TPU v7x, 512 devices: a whole 4x4x16 slice. The times are simulated.
512 devices in a mesh: sp: 32 (over z, core), tp: 16 (over y, x).
Axes of the slice: x: 4, y: 4, z: 16, core: 2. Of those that a mesh axis runs over, the one named last changes fastest.
Arguments:
- residual_in: bfloat16 [4096, 2048], P('sp'), may hold values from -6 to 6
- queries: bfloat16 [4096, 2048], P('sp', 'tp'), may hold values from -6 to 6
- keys: bfloat16 [4096, 2048], P('sp', 'tp'), may hold values from -6 to 6
- values: bfloat16 [4096, 2048], P('sp', 'tp'), may hold values from -6 to 6
- out_gate: bfloat16 [4096, 2048], P('sp', 'tp'), may hold values from -6 to 6
- beta_logit: bfloat16 [16, 4096], P('tp', 'sp'), may hold values from -6 to -2
- decay_logit: bfloat16 [16, 4096], P('tp', 'sp'), may hold values from -4.5 to 4.5
- decay_log: float32 [16], P('tp'), may hold values from -11 to -3.2
- head_gain: float32 [128], replicated, may hold values from 0.1 to 1.9
- out_weight: bfloat16 [2048, 2048], P('tp'), may hold values from -0.125 to 0.125
- norm_gain: float32 [2048], replicated, may hold values from 0.1 to 1.9
- final_gain: float32 [2048], replicated, may hold values from 0.1 to 1.9
- expert_index: int32 [4096, 2], P('sp'), may hold values from 0 to 31, all different within a row; in each aligned block of 8 rows (0 to 7, 8 to 15, ...) no two rows name the same one
- route_weights: float32 [4096, 2], P('sp'), may hold values from 0.2 to 1
- expert_gate: bfloat16 [32, 2048, 6144], P('sp', None, 'tp'), may hold values from -0.125 to 0.125
- expert_up: bfloat16 [32, 2048, 6144], P('sp', None, 'tp'), may hold values from -0.125 to 0.125
- expert_down: bfloat16 [32, 6144, 2048], P('sp', 'tp'), may hold values from -0.078125 to 0.078125
Outputs:
- layer_out: bfloat16 [4096, 2048], P('sp')
Inputs may be any that keep to these rules, and one draw needn't show every extreme that they name: `expert_index`: in each aligned block of 8 rows no expert is named by more than 1 row, a bound that some block reaches; a row names 2 different experts.
All inputs are finite; a program needn't handle non-finite values.
Results may differ from a plain program's by a relative error of at most 0.015.
Values may be sent and summed in bfloat16 or wider, within the bound.
No kernel may reach another device: no remote copies, remote signals or barrier semaphores. Data moves between devices by JAX's collectives and lax.ppermute only.
A program may use at most 64 MiB of HBM per device.

v0:
```python
import jax
import jax.numpy as jnp
from jax import lax
from jax.sharding import Mesh
from jax.sharding import PartitionSpec as P

HEAD_FEATURES = 128
TOP = 2
BLOCK = 64
SP = ("sp_0", "sp_1")


highest_precision = lax.Precision.HIGHEST
residual_scale = 2.0**0.5


def nothing_yet(x, identity):
    return jax.tree.map(
        lambda part, zero: jnp.zeros_like(part) + jnp.asarray(zero, part.dtype), x, identity
    )


def entering(x, axes, combine, identity):
    before = start = nothing_yet(x, identity)
    total = x
    for axis in reversed(axes):
        length, here = (lax.axis_size(axis), lax.axis_index(axis))
        pieces = jax.tree.map(
            lambda part, kind: lax.all_gather(part.astype(kind), axis),
            total,
            (jnp.bfloat16, jnp.bfloat16),
        )
        inside, total = (start, start)
        for k in range(length):
            passed = k < here
            total = combine(
                total, jax.tree.map(lambda part, own: part[k].astype(own.dtype), pieces, x)
            )
            inside = jax.tree.map(lambda new, old: jnp.where(passed, new, old), total, inside)
        before = combine(inside, before)
    return before


def in_blocks(x, dim, length):
    shape = x.shape
    blocks = x.reshape(*shape[:dim], length, shape[dim] // length, *shape[dim + 1 :])
    return jnp.moveaxis(blocks, dim, 0)


def sum_at_owner(x, axis, dim):
    length = lax.axis_size(axis)
    blocks = lax.all_to_all(in_blocks(x, dim, length), axis, 0, 0, tiled=True)
    return jnp.sum(blocks.astype(jnp.float32), axis=0)


def copy_for_each(x, axis):
    length = lax.axis_size(axis)
    return lax.all_to_all(jnp.broadcast_to(x[None], (length, *x.shape)), axis, 0, 0, tiled=True)


def in_order(blocks, dim):
    shape = list(blocks.shape[1:])
    shape[dim] *= blocks.shape[0]
    return jnp.moveaxis(blocks, 0, dim).reshape(shape)


def collect(x, axis, dim):
    blocks = copy_for_each(x, axis)
    return in_order(blocks, dim)


def unit_rows(data):
    return data * lax.rsqrt(jnp.sum(data * data, -1, keepdims=True) + 1e-06)


def layer_norm(data, gain):
    center = data - jnp.mean(data, -1, keepdims=True)
    return center * lax.rsqrt(jnp.mean(center * center, -1, keepdims=True) + 1e-05) * gain


def block_terms(query, key, beta, decay):
    heads, length, width = query.shape
    count = length // BLOCK
    shape = (heads, count, BLOCK, width)
    query = query.reshape(shape)
    key = key.reshape(shape)
    beta = beta.reshape(heads, count, BLOCK)
    running = jnp.cumsum(decay.reshape(heads, count, BLOCK), axis=-1)
    causal = jnp.tril(jnp.ones((BLOCK, BLOCK), bool))
    strict = jnp.tril(jnp.ones((BLOCK, BLOCK), bool), -1)
    within = jnp.exp(jnp.where(causal, running[..., :, None] - running[..., None, :], -jnp.inf))
    key_beta = key * beta[..., None]
    lower = jnp.where(
        strict,
        jnp.einsum("hnid,hnjd->hnij", key_beta, key, precision=highest_precision) * within,
        0.0,
    )
    system = jnp.eye(BLOCK, dtype=jnp.float32) + lower
    weighted = jax.scipy.linalg.solve_triangular(
        system, key_beta * jnp.exp(running)[..., None], lower=True, unit_diagonal=True
    )
    scores = jnp.einsum("hnid,hnjd->hnij", query, key, precision=highest_precision) * within
    query_decayed = query * jnp.exp(running)[..., None]
    key_decayed = key * jnp.exp(running[..., -1:] - running)[..., None]
    block_decay = jnp.exp(running[..., -1])
    return (system, beta, weighted, query_decayed, key_decayed, scores, block_decay)


def run_blocks(terms, value, start):
    system, beta, weighted, query_decayed, key_decayed, scores, block_decay = terms
    heads, count = (beta.shape[0], beta.shape[1])
    fresh = jax.scipy.linalg.solve_triangular(
        system,
        value.reshape(heads, count, BLOCK, -1) * beta[..., None],
        lower=True,
        unit_diagonal=True,
    )
    missing = start.shape[-1] - fresh.shape[-1]
    fresh = jnp.concatenate([fresh, jnp.zeros(fresh.shape[:-1] + (missing,), jnp.float32)], -1)

    def advance(recurrent_state, inputs):
        (
            fresh_value_block,
            block_weighted_values,
            block_queries,
            block_keys,
            block_scores,
            block_decay_factor,
        ) = inputs
        corrected_value = fresh_value_block - jnp.einsum(
            "nya,nag->nyg", block_weighted_values, recurrent_state, precision=highest_precision
        )
        state_next = block_decay_factor[:, None, None] * recurrent_state + jnp.einsum(
            "iyp,iyu->ipu", block_keys, corrected_value, precision=highest_precision
        )
        final_output = jnp.einsum(
            "nya,nag->nyg", block_queries, recurrent_state, precision=highest_precision
        ) + jnp.einsum("emp,epk->emk", block_scores, corrected_value, precision=highest_precision)
        return (state_next, final_output)

    inputs = tuple(
        (
            jnp.moveaxis(item, 1, 0)
            for item in (fresh, weighted, query_decayed, key_decayed, scores, block_decay)
        )
    )
    final, output_list = lax.scan(advance, start, inputs)
    return (jnp.moveaxis(output_list, 0, 1).reshape(heads, count * BLOCK, -1), final)


def compose(earlier, later):
    return (
        jnp.einsum("hij,hjk->hik", later[0], earlier[0], precision=highest_precision),
        jnp.einsum("hij,hjk->hik", later[0], earlier[1], precision=highest_precision) + later[1],
    )


def slot_places(routes, groups, capacity, experts):
    rows, picks = routes.shape
    flat = routes.reshape(groups, rows // groups * picks)
    matches = (flat[..., None] == jnp.arange(experts, dtype=jnp.int32)).astype(jnp.int32)
    before = jnp.cumsum(matches, axis=1) - matches
    rank = jnp.sum(before * matches, -1)
    group = jnp.arange(groups, dtype=jnp.int32)[:, None]
    return ((flat * groups + group) * capacity + rank).reshape(rows, picks)


def per_device(
    residual_in,
    queries,
    keys,
    values,
    out_gate,
    beta_logit,
    decay_logit,
    decay_log,
    head_gain,
    out_weight,
    norm_gain,
    final_gain,
    expert_index,
    route_weights,
    expert_gate,
    expert_up,
    expert_down,
):
    length, width = residual_in.shape
    heads = beta_logit.shape[0]

    def split_heads(data):
        return data.astype(jnp.float32).reshape(length, heads, HEAD_FEATURES).transpose(1, 0, 2)

    query = unit_rows(split_heads(queries)) * HEAD_FEATURES ** (-0.5)
    key = unit_rows(split_heads(keys))
    value = split_heads(values)
    beta = jax.nn.sigmoid(beta_logit.astype(jnp.float32))
    decay = -jnp.exp(decay_log)[:, None] * jax.nn.softplus(decay_logit.astype(jnp.float32))
    terms = block_terms(query, key, beta, decay)
    identity_map = jnp.broadcast_to(
        jnp.eye(HEAD_FEATURES, dtype=jnp.float32), (heads, HEAD_FEATURES, HEAD_FEATURES)
    )
    blank = jnp.zeros((heads, HEAD_FEATURES, HEAD_FEATURES), jnp.float32)
    extended = jnp.concatenate([blank, identity_map], -1)
    output_list, final = run_blocks(terms, value, extended)
    prefix = entering(
        (final[..., HEAD_FEATURES:], final[..., :HEAD_FEATURES]), SP, compose, (identity_map, blank)
    )
    entry_value = prefix[1]
    mixed = output_list[..., :HEAD_FEATURES] + jnp.einsum(
        "apj,ajz->apz", output_list[..., HEAD_FEATURES:], entry_value, precision=highest_precision
    )
    normalized = mixed * lax.rsqrt(jnp.mean(mixed * mixed, -1, keepdims=True) + 1e-06) * head_gain
    gated = (
        (normalized * jax.nn.silu(split_heads(out_gate)))
        .transpose(1, 0, 2)
        .reshape(length, heads * HEAD_FEATURES)
        .astype(jnp.bfloat16)
    )
    split_count = lax.axis_size("tp")
    expert_count = lax.axis_size(SP) * expert_gate.shape[0]
    rows = length // split_count
    first = lax.axis_index("tp") * rows
    projected = sum_at_owner(
        jnp.dot(gated, out_weight, preferred_element_type=jnp.float32).astype(jnp.bfloat16), "tp", 0
    )
    residual = lax.dynamic_slice_in_dim(residual_in, first, rows, 0)
    routes = lax.dynamic_slice_in_dim(expert_index, first, rows, 0)
    weights = lax.dynamic_slice_in_dim(route_weights, first, rows, 0)
    groups = 1
    capacity = 2 * TOP * (length // split_count) // expert_count
    hidden_in = layer_norm(
        residual_scale * residual.astype(jnp.float32) + projected, norm_gain
    ).astype(jnp.bfloat16)
    places = slot_places(routes, groups, capacity, expert_count)
    slots = expert_count * groups * capacity
    table = (places[:, :, None] == jnp.arange(slots, dtype=jnp.int32)).astype(jnp.bfloat16)
    send = jnp.einsum(
        "rs,rd->sd", jnp.sum(table, 1), hidden_in, preferred_element_type=jnp.float32
    ).astype(jnp.bfloat16)
    arrived = lax.all_to_all(
        send.reshape(expert_count, groups * capacity, width),
        SP,
        split_axis=0,
        concat_axis=0,
        tiled=True,
    ).reshape(slots, width)
    gate_matrix, up_matrix, down_matrix = (expert_gate[0], expert_up[0], expert_down[0])
    piece = collect(arrived, "tp", 0)
    gate = jnp.dot(piece, gate_matrix, preferred_element_type=jnp.float32)
    up = jnp.dot(piece, up_matrix, preferred_element_type=jnp.float32)
    inner = (jax.nn.silu(gate) * up).astype(jnp.bfloat16)
    partial_value = jnp.dot(inner, down_matrix, preferred_element_type=jnp.float32)
    result = sum_at_owner(partial_value.astype(jnp.bfloat16), "tp", 0)
    back = lax.all_to_all(
        result.astype(jnp.bfloat16).reshape(expert_count, groups * capacity, width),
        SP,
        split_axis=0,
        concat_axis=0,
        tiled=True,
    ).reshape(slots, width)
    gathered = jnp.einsum("rks,sd->rkd", table, back, preferred_element_type=jnp.float32)
    routed = jnp.sum(weights[..., None] * gathered, 1)
    layer_out = layer_norm(
        residual_scale * hidden_in.astype(jnp.float32) + routed, final_gain
    ).astype(jnp.bfloat16)
    layer_out = collect(layer_out, "tp", 0)
    return layer_out


def solution(mesh):
    split = Mesh(mesh.devices.reshape(16, 2, mesh.shape["tp"]), ("sp_0", "sp_1", "tp"))
    placed = (
        P(SP, None),
        P(SP, "tp"),
        P(SP, "tp"),
        P(SP, "tp"),
        P(SP, "tp"),
        P("tp", SP),
        P("tp", SP),
        P("tp"),
        P(),
        P("tp", None),
        P(),
        P(),
        P(SP, None),
        P(SP, None),
        P(SP, None, "tp"),
        P(SP, None, "tp"),
        P(SP, "tp", None),
    )
    return jax.shard_map(
        per_device, mesh=split, in_specs=placed, out_specs=P(SP, None), check_vma=False
    )
```

profile of v0, /device:TPU:1, one launch (start us, length us, event | category | flops | bytes accessed | tf_op | source)
XLA Modules:
  0.0 266.3 jit_solution(16867856148266013828)
XLA Ops:
  1.6 0.9 fusion.52
  4.3 9.8 %custom-call.4 = f32[2,1,64,64]{2,3,1,0:T(8,128)S(1)} custom-call(f32[2,1,64,64]{3,2,1,0:T(8,128)S(1)} %fusion.40), custom_call_target="InvertDiagBlocksLowerTriangular" | custom-call | tf_op jit(solution)/shard_map/jit(_solve_triangular)/vmap()/triangular_solve | solution.py:112
  14.2 1.1 convolution_bitcast_fusion.3
  15.3 0.9 fusion.53
  17.8 4.7 %while.12 = (s32[]{:T(128)}, f32[1,128,256]{2,1,0:T(8,128)S(1)}, f32[2,1,64,256]{3,2,1,0:T(8,128)S(1)}, f32[2,1]{0,1:T(1,128)S(1)}, f32[2,1,64,128]{3,2,1,0:T(8,...) while((s32[]{:T(128)}, f32[1,128,256]{2,1,0:T(8,128)S(1)}, ...), condition=%wide.region_4.6_spmd, body=%wide.region_3.5_spmd.sunk | while | flops 88178688 | bytes 1116285 | solution.py:147
  19.1 1.0 fusion.176
  21.5 1.0 fusion.176
  22.6 8.3 %all-gather = bf16[2,128,128]{2,1,0:T(8,128)(2,1)S(1)} all-gather(bf16[1,128,128]{2,1,0:T(8,128)(2,1)S(1)} %get-tuple-element.113), channel_id=2, replica_groups=mesh['sp_0'=16,'sp_1'=2,'tp'=16] {'sp_1'}, dimensions={0}, use_global_device_ids=true | all-gather | bytes 98304 | tf_op jit(solution)/shard_map/all_gather | solution.py:29
  31.0 1.8 all-gather.2
  33.9 26.1 %all-gather.3 = bf16[2048,128]{1,0:T(8,128)(2,1)S(1)} all-gather(bf16[128,128]{1,0:T(8,128)(2,1)S(1)} %get-tuple-element.116), channel_id=5, replica_groups=mesh['sp_0'=16,'sp_1'=2,'tp'=16] {'sp_0'}, dimensions={0}, use_global_device_ids=true | all-gather | bytes 557056 | tf_op jit(solution)/shard_map/all_gather | solution.py:29
  60.8 22.2 %all-gather.1 = bf16[2048,128]{1,0:T(8,128)(2,1)S(1)} all-gather(bf16[128,128]{1,0:T(8,128)(2,1)S(1)} %get-tuple-element.118), channel_id=3, replica_groups=mesh['sp_0'=16,'sp_1'=2,'tp'=16] {'sp_0'}, dimensions={0}, use_global_device_ids=true | all-gather | bytes 557056 | tf_op jit(solution)/shard_map/all_gather | solution.py:29
  86.4 1.5 slice.207
  87.9 1.6 copy.66
  89.6 1.1 fusion.32
  91.0 1.0 convolution_add_fusion.1
  92.1 1.2 multiply_reduce_fusion.2
  93.3 0.9 copy.56
  94.1 2.2 fusion.18
  96.4 6.8 %all-to-all-start = ((bf16[16,8,2048]{2,1,0:T(8,128)(2,1)}), bf16[16,8,2048]{2,1,0:T(8,128)(2,1)S(1)}, u32[]{:S(2)}, u32[]{:S(2)}) async-start(bf16[16,8,2048]{2,1,0:T(8,128)(2,1)} %fusion.18), calls=%async_computation | async-start | bytes 1048576 | tf_op jit(solution)/shard_map/all_to_all | solution.py:52
  103.9 8.2 %all-to-all-done = bf16[16,8,2048]{2,1,0:T(8,128)(2,1)S(1)} async-done(((bf16[16,8,2048]{2,1,0:T(8,128)(2,1)}), bf16[16,8,2048]{2,1,0:T(8,128)(2,1)S(1)}, u32[]{:S(2)}, u32[]{:S(2)}) %all-to-all-start) | async-done | bytes 524320 | tf_op jit(solution)/shard_map/all_to_all | solution.py:52
  112.2 0.9 fusion.111
  113.1 1.0 multiply_reduce_fusion.1
  116.4 38.0 %all_to_all.30 = bf16[32,2,1024]{2,1,0:T(2,128)(2,1)S(1)} all-to-all(bf16[32,2,1024]{2,1,0:T(2,128)(2,1)S(1)} %reshape.862), channel_id=1, replica_groups=mesh['sp_0'=16,'sp_1'=2,'tp'=16] {'sp_0','sp_1'}, dimensions={0} | all-to-all | bytes 262144 | tf_op jit(solution)/shard_map/all_to_all | solution.py:240
  154.8 29.7 %all_to_all.31 = bf16[16,32,2048]{2,1,0:T(8,128)(2,1)S(1)} all-to-all(bf16[16,32,2048]{2,1,0:T(8,128)(2,1)S(1)} %broadcast_in_dim.43), channel_id=1, replica_groups=mesh['sp_0'=16,'sp_1'=2,'tp'=16] {'tp'}, dimensions={0} | all-to-all | bytes 4194304 | tf_op jit(solution)/shard_map/all_to_all | solution.py:58
  184.5 1.3 copy-done.1
  185.8 1.3 fusion.23
  187.1 5.8 %convolution_convert_fusion = bf16[512,2048]{1,0:T(8,128)(2,1)} fusion(bf16[1,384,2048]{2,1,0:T(8,128)(2,1)S(1)} %copy-done, bf16[512,2048]{1,0:T(8,128)(2,1)} %bitcast.212, bf16[1,2048,384]{2,1,0:T(8,128)(2,1)} %param.36, f32[512,384]{1,0:T(8,128)S(1)} %fusion.23), kind=kOutput, calls=%fused_computation.22 | convolution fusion | flops 1612840960 | bytes 8126464 | tf_op jit(solution)/shard_map/dot_general | solution.py:252
  192.8 30.4 %all_to_all.32 = bf16[16,32,2048]{2,1,0:T(8,128)(2,1)} all-to-all(bf16[16,32,2048]{2,1,0:T(8,128)(2,1)} %bitcast.213), channel_id=1, replica_groups=mesh['sp_0'=16,'sp_1'=2,'tp'=16] {'tp'}, dimensions={0} | all-to-all | bytes 4194304 | tf_op jit(solution)/shard_map/all_to_all | solution.py:52
  223.3 2.0 reduce_sum.125
  226.7 9.4 %all-to-all-start.4 = ((bf16[32,2,1024]{2,1,0:T(2,128)(2,1)}), bf16[32,2,1024]{2,1,0:T(2,128)(2,1)S(1)}, u32[]{:S(2)}, u32[]{:S(2)}) async-start(bf16[32,2,1024]{2,1,0:T(2,128)(2,1)} %reshape.864), calls=%async_computation.4 | async-start | bytes 262144 | tf_op jit(solution)/shard_map/all_to_all | solution.py:254
  236.2 15.8 %all-to-all-done.4 = bf16[32,2,1024]{2,1,0:T(2,128)(2,1)S(1)} async-done(((bf16[32,2,1024]{2,1,0:T(2,128)(2,1)}), bf16[32,2,1024]{2,1,0:T(2,128)(2,1)S(1)}, u32[]{:S(2)}, u32[]{:S(2)}) %all-to-all-start.4) | async-done | bytes 131104 | tf_op jit(solution)/shard_map/all_to_all | solution.py:254
  252.8 12.7 %all_to_all.33 = bf16[16,8,2048]{2,1,0:T(8,128)(2,1)S(1)} all-to-all(bf16[16,8,2048]{2,1,0:T(8,128)(2,1)S(1)} %broadcast_in_dim.44), channel_id=1, replica_groups=mesh['sp_0'=16,'sp_1'=2,'tp'=16] {'tp'}, dimensions={0} | all-to-all | bytes 1048576 | tf_op jit(solution)/shard_map/all_to_all | solution.py:58
  (108 shorter events, 19.2 us)
Async XLA Ops:
  0.0 187.1 %copy-start = (bf16[1,384,2048]{2,1,0:T(8,128)(2,1)S(1)}, bf16[1,384,2048]{2,1,0:T(8,128)(2,1)}, u32[]{:S(2)}) copy-start(bf16[1,384,2048]{2,1,0:T(8,128)(2,1)} %param.37) | copy-start | bytes 4718596
  22.6 38.2 %copy-start.4 = (f32[2,1,64,256]{3,2,1,0:T(8,128)}, f32[2,1,64,256]{3,2,1,0:T(8,128)S(1)}, u32[]{:S(2)}) copy-start(f32[2,1,64,256]{3,2,1,0:T(8,128)S(1)} %get-tuple-element.54) | copy-start | bytes 393220
  33.1 27.7 %copy-start.3 = (f32[128,128]{1,0:T(8,128)}, f32[128,128]{1,0:T(8,128)S(1)}, u32[]{:S(2)}) copy-start(f32[128,128]{1,0:T(8,128)S(1)} %convolution_add_fusion.18) | copy-start | bytes 196612
  83.1 2.1 copy-start.2
  84.1 10.0 %copy-start.9 = (f32[128]{0:T(128)S(1)}, f32[128]{0:T(128)}, u32[]{:S(2)}) copy-start(f32[128]{0:T(128)} %param.29) | copy-start | bytes 1540
  89.6 13.5 %copy-start.7 = (s32[128,2]{0,1:T(2,128)S(1)}, s32[128,2]{0,1:T(2,128)}, u32[]{:S(2)}) copy-start(s32[128,2]{0,1:T(2,128)} %param.33) | copy-start | bytes 3076
  90.8 23.3 %copy-start.5 = (f32[2048]{0:T(1024)S(1)}, f32[2048]{0:T(1024)}, u32[]{:S(2)}) copy-start(f32[2048]{0:T(1024)} %param.31) | copy-start | bytes 24580
  96.4 15.7 %all-to-all-start = ((bf16[16,8,2048]{2,1,0:T(8,128)(2,1)}), bf16[16,8,2048]{2,1,0:T(8,128)(2,1)S(1)}, u32[]{:S(2)}, u32[]{:S(2)}) async-start(bf16[16,8,2048]{2,1,0:T(8,128)(2,1)} %fusion.18), calls=%async_computation | async-start | bytes 1048576 | tf_op jit(solution)/shard_map/all_to_all | solution.py:52
  154.8 31.0 %copy-start.10 = (bf16[1,2048,384]{2,1,0:T(8,128)(2,1)S(1)}, bf16[1,2048,384]{2,1,0:T(8,128)(2,1)}, u32[]{:S(2)}) copy-start(bf16[1,2048,384]{2,1,0:T(8,128)(2,1)} %param.35) | copy-start | bytes 4718596
  184.5 1.3 copy-start.1
  223.3 12.9 %copy-start.8 = (f32[128,2]{0,1:T(2,128)S(1)}, f32[128,2]{0,1:T(2,128)}, u32[]{:S(2)}) copy-start(f32[128,2]{0,1:T(2,128)} %param.34) | copy-start | bytes 3076
  223.3 29.4 %copy-start.6 = (f32[2048]{0:T(1024)S(1)}, f32[2048]{0:T(1024)}, u32[]{:S(2)}) copy-start(f32[2048]{0:T(1024)} %param.32) | copy-start | bytes 24580
  226.7 25.3 %all-to-all-start.4 = ((bf16[32,2,1024]{2,1,0:T(2,128)(2,1)}), bf16[32,2,1024]{2,1,0:T(2,128)(2,1)S(1)}, u32[]{:S(2)}, u32[]{:S(2)}) async-start(bf16[32,2,1024]{2,1,0:T(2,128)(2,1)} %reshape.864), calls=%async_computation.4 | async-start | bytes 262144 | tf_op jit(solution)/shard_map/all_to_all | solution.py:254
where the time goes:
time: 268 us; the launch traced here: 266 us
  blocking collectives  169 us (63%)
  matrix products  23.9 us (9%)
  waiting for transfers between devices  23.9 us (9%)
  other arithmetic  21.5 us (8%)
  starting transfers between devices  16.2 us (6%)
  local copies, waits for them, and re-layouts  10.1 us (4%)
    all_gather x4, blocking collectives, entering(): lax.all_gather(part.astype(kind), axis)  58.4 us
    all_to_all x2, blocking collectives, copy_for_each(): lax.all_to_all(jnp.broadcast_to(x[None], (length, *x.shape)), axis, 0, 0,...  42.4 us
    all_to_all x1, blocking collectives, per_device(): lax.all_to_all(send.reshape(expert_count, groups * capacity, width), SP,...  38 us
    all_to_all x1, blocking collectives, sum_at_owner(): blocks = lax.all_to_all(in_blocks(x, dim, length), axis, 0, 0, tiled=True)  30.4 us
    all_to_all x1, waiting for transfers between devices, per_device(): lax.all_to_all(result.astype(jnp.bfloat16).reshape(expert_count, groups *...  15.8 us
    another operation x3, other arithmetic, run_blocks(): jax.scipy.linalg.solve_triangular(system, value.reshape(heads, count, BLO...  9.92 us
    all_to_all x1, starting transfers between devices, per_device(): lax.all_to_all(result.astype(jnp.bfloat16).reshape(expert_count, groups *...  9.45 us
    all_to_all x1, waiting for transfers between devices, sum_at_owner(): blocks = lax.all_to_all(in_blocks(x, dim, length), axis, 0, 0, tiled=True)  8.19 us
  transfers between devices with their start and end apart: 2, of which 2 were waited for; matrix products, arithmetic and copies ran while one was open for 0% of the time, Pallas kernels for 0%

commit v1 on v0

--- a/solution.py
+++ b/solution.py
@@ -7,38 +7,45 @@
 HEAD_FEATURES = 128
 TOP = 2
 BLOCK = 64
-SP = ("sp_0", "sp_1")
+Z = ("zh", "zl")
+SP = ("zh", "zl", "c")
+PLANE = ("c", "tp")
 
 
 highest_precision = lax.Precision.HIGHEST
 residual_scale = 2.0**0.5
 
 
-def nothing_yet(x, identity):
-    return jax.tree.map(
-        lambda part, zero: jnp.zeros_like(part) + jnp.asarray(zero, part.dtype), x, identity
-    )
-
-
-def entering(x, axes, combine, identity):
-    before = start = nothing_yet(x, identity)
-    total = x
-    for axis in reversed(axes):
-        length, here = (lax.axis_size(axis), lax.axis_index(axis))
-        pieces = jax.tree.map(
-            lambda part, kind: lax.all_gather(part.astype(kind), axis),
-            total,
-            (jnp.bfloat16, jnp.bfloat16),
-        )
-        inside, total = (start, start)
-        for k in range(length):
-            passed = k < here
-            total = combine(
-                total, jax.tree.map(lambda part, own: part[k].astype(own.dtype), pieces, x)
-            )
-            inside = jax.tree.map(lambda new, old: jnp.where(passed, new, old), total, inside)
-        before = combine(inside, before)
-    return before
+def mm(a, b):
+    return jnp.dot(a, b, precision=highest_precision)
+
+
+def entering(map_here, state_here):
+    kind = jnp.bfloat16
+    zh, zl, c = (lax.axis_index(axis) for axis in SP)
+    own = jnp.concatenate([map_here, state_here], 0).astype(kind)
+    near = lax.all_gather(own, ("zl", "c")).astype(jnp.float32)
+    width = map_here.shape[-1]
+    map_in, state_in = (jnp.eye(width, dtype=jnp.float32), jnp.zeros((width, width), jnp.float32))
+    map_all, state_all = (near[0, :width], near[0, width:])
+    for k in range(1, 4):
+        inside = k == 2 * zl + c
+        map_in = jnp.where(inside, map_all, map_in)
+        state_in = jnp.where(inside, state_all, state_in)
+        map_k, state_k = (near[k, :width], near[k, width:])
+        state_all = mm(map_k, state_all) + state_k
+        map_all = mm(map_k, map_all)
+    group = jnp.concatenate([map_all, state_all], 0).astype(kind)
+    quarter = lax.dynamic_slice_in_dim(group, (2 * zl + c) * (width // 2), width // 2, 0)
+    count = lax.axis_size(Z)
+    far = lax.all_to_all(jnp.broadcast_to(quarter[None], (count, *quarter.shape)), Z, 0, 0, tiled=True)
+    far = lax.all_gather(far, "c")
+    far = far.reshape(2, count // 2, 2, width // 2, width).transpose(1, 2, 0, 3, 4)
+    far = far.reshape(count // 2, 2 * width, width).astype(jnp.float32)
+    state = jnp.zeros((width, width), jnp.float32)
+    for k in range(count // 2 - 1):
+        state = jnp.where(k < zh, mm(far[k, :width], state) + far[k, width:], state)
+    return mm(map_in, state) + state_in
 
 
 def in_blocks(x, dim, length):
@@ -146,23 +153,6 @@
     )
     final, output_list = lax.scan(advance, start, inputs)
     return (jnp.moveaxis(output_list, 0, 1).reshape(heads, count * BLOCK, -1), final)
-
-
-def compose(earlier, later):
-    return (
-        jnp.einsum("hij,hjk->hik", later[0], earlier[0], precision=highest_precision),
-        jnp.einsum("hij,hjk->hik", later[0], earlier[1], precision=highest_precision) + later[1],
-    )
-
-
-def slot_places(routes, groups, capacity, experts):
-    rows, picks = routes.shape
-    flat = routes.reshape(groups, rows // groups * picks)
-    matches = (flat[..., None] == jnp.arange(experts, dtype=jnp.int32)).astype(jnp.int32)
-    before = jnp.cumsum(matches, axis=1) - matches
-    rank = jnp.sum(before * matches, -1)
-    group = jnp.arange(groups, dtype=jnp.int32)[:, None]
-    return ((flat * groups + group) * capacity + rank).reshape(rows, picks)
 
 
 def per_device(
@@ -202,10 +192,7 @@
     blank = jnp.zeros((heads, HEAD_FEATURES, HEAD_FEATURES), jnp.float32)
     extended = jnp.concatenate([blank, identity_map], -1)
     output_list, final = run_blocks(terms, value, extended)
-    prefix = entering(
-        (final[..., HEAD_FEATURES:], final[..., :HEAD_FEATURES]), SP, compose, (identity_map, blank)
-    )
-    entry_value = prefix[1]
+    entry_value = entering(final[0, :, HEAD_FEATURES:], final[0, :, :HEAD_FEATURES])[None]
     mixed = output_list[..., :HEAD_FEATURES] + jnp.einsum(
         "apj,ajz->apz", output_list[..., HEAD_FEATURES:], entry_value, precision=highest_precision
     )
@@ -226,38 +213,34 @@
     residual = lax.dynamic_slice_in_dim(residual_in, first, rows, 0)
     routes = lax.dynamic_slice_in_dim(expert_index, first, rows, 0)
     weights = lax.dynamic_slice_in_dim(route_weights, first, rows, 0)
-    groups = 1
-    capacity = 2 * TOP * (length // split_count) // expert_count
     hidden_in = layer_norm(
         residual_scale * residual.astype(jnp.float32) + projected, norm_gain
     ).astype(jnp.bfloat16)
-    places = slot_places(routes, groups, capacity, expert_count)
-    slots = expert_count * groups * capacity
-    table = (places[:, :, None] == jnp.arange(slots, dtype=jnp.int32)).astype(jnp.bfloat16)
+    chips = lax.axis_size(Z)
+    table = (routes[:, :, None] == jnp.arange(expert_count, dtype=jnp.int32)).astype(jnp.bfloat16)
     send = jnp.einsum(
         "rs,rd->sd", jnp.sum(table, 1), hidden_in, preferred_element_type=jnp.float32
     ).astype(jnp.bfloat16)
-    arrived = lax.all_to_all(
-        send.reshape(expert_count, groups * capacity, width),
-        SP,
-        split_axis=0,
-        concat_axis=0,
-        tiled=True,
-    ).reshape(slots, width)
+
+    def along_z(x):
+        out = lax.all_to_all(x.reshape(chips, 16, width // 8), Z, 0, 0, tiled=True)
+        return out.reshape(chips, 2, width)
+
+    def in_plane(x):
+        return lax.all_to_all(x, PLANE, 0, 0, tiled=True)
+
+    arrived = along_z(send).transpose(1, 0, 2)
+    arrived = jnp.broadcast_to(arrived[:, None], (2, split_count, chips, width))
+    piece = in_plane(arrived.reshape(2 * split_count, chips, width)).reshape(-1, width)
     gate_matrix, up_matrix, down_matrix = (expert_gate[0], expert_up[0], expert_down[0])
-    piece = collect(arrived, "tp", 0)
     gate = jnp.dot(piece, gate_matrix, preferred_element_type=jnp.float32)
     up = jnp.dot(piece, up_matrix, preferred_element_type=jnp.float32)
     inner = (jax.nn.silu(gate) * up).astype(jnp.bfloat16)
     partial_value = jnp.dot(inner, down_matrix, preferred_element_type=jnp.float32)
-    result = sum_at_owner(partial_value.astype(jnp.bfloat16), "tp", 0)
-    back = lax.all_to_all(
-        result.astype(jnp.bfloat16).reshape(expert_count, groups * capacity, width),
-        SP,
-        split_axis=0,
-        concat_axis=0,
-        tiled=True,
-    ).reshape(slots, width)
+    parts = in_plane(partial_value.astype(jnp.bfloat16).reshape(2 * split_count, chips, width))
+    parts = parts.reshape(2, split_count, chips, width)
+    result = jnp.sum(parts.astype(jnp.float32), axis=1).astype(jnp.bfloat16)
+    back = along_z(result.transpose(1, 0, 2)).reshape(expert_count, width)
     gathered = jnp.einsum("rks,sd->rkd", table, back, preferred_element_type=jnp.float32)
     routed = jnp.sum(weights[..., None] * gathered, 1)
     layer_out = layer_norm(
@@ -268,7 +251,9 @@
 
 
 def solution(mesh):
-    split = Mesh(mesh.devices.reshape(16, 2, mesh.shape["tp"]), ("sp_0", "sp_1", "tp"))
+    split = Mesh(
+        mesh.devices.reshape(8, 2, 2, mesh.shape["tp"]), ("zh", "zl", "c", "tp")
+    )
     placed = (
         P(SP, None),
         P(SP, "tp"),

time: 268 us -> 222 us (0.83); the launches traced: 266 us -> 218 us
  blocking collectives: 169 us -> 118 us
  waiting for transfers between devices: 23.9 us -> 36.3 us
  matrix products: 23.9 us -> 17.2 us
  local copies, waits for them, and re-layouts: 10.1 us -> 6.43 us
  starting transfers between devices: 16.2 us -> 19.8 us
  other arithmetic: 21.5 us -> 18.4 us
    all_gather x4 -> x2, blocking collectives: 58.4 us -> 19.2 us  [the longest x1 12.5 us: entering(): near = lax.all_gather(own, ('zl', 'c')).astype(jnp.float32)]
    all_to_all x2 -> x1, blocking collectives: 42.4 us -> 13 us  [copy_for_each(): lax.all_to_all(jnp.broadcast_to(x[None], (length, *x.shape)), axis, 0, 0,...]
    all_to_all x2 -> x3, blocking collectives: 68.4 us -> 85.7 us  [the longest x2 68.3 us: in_plane(): return lax.all_to_all(x, PLANE, 0, 0, tiled=True)]
    all_to_all x1 -> x2, waiting for transfers between devices: 15.8 us -> 25.7 us  [the longest x1 13.9 us: entering(): lax.all_to_all(jnp.broadcast_to(quarter[None], (count, *quarter.shape)),...]
    dot_general x23 -> x14, matrix products: 7.78 us -> 2.46 us  [mm(): return jnp.dot(a, b, precision=highest_precision)]
    all_to_all x1 -> x2, starting transfers between devices: 9.45 us -> 13.1 us  [the longest x1 9.57 us: entering(): lax.all_to_all(jnp.broadcast_to(quarter[None], (count, *quarter.shape)),...]
    unnamed x31 -> x25, local copies, waits for them, and re-layouts: 5.74 us -> 2.4 us
  transfers between devices with their start and end apart: 2 -> 3, of which waited for: 2 -> 3; matrix products, arithmetic and copies ran while one was open for 0% -> 0% of each run, Pallas kernels for 0% -> 0%
where the time goes in v1:
time: 222 us; the launch traced here: 218 us
  blocking collectives  118 us (53%)
  waiting for transfers between devices  36.3 us (16%)
  starting transfers between devices  19.8 us (9%)
  other arithmetic  18.4 us (8%)
  matrix products  17.2 us (8%)
  local copies, waits for them, and re-layouts  6.43 us (3%)
    all_to_all x2, blocking collectives, in_plane(): return lax.all_to_all(x, PLANE, 0, 0, tiled=True)  68.3 us
    all_to_all x1, blocking collectives, along_z(): out = lax.all_to_all(x.reshape(chips, 16, width // 8), Z, 0, 0, tiled=True)  17.4 us
    all_to_all x1, waiting for transfers between devices, entering(): lax.all_to_all(jnp.broadcast_to(quarter[None], (count, *quarter.shape)),...  13.9 us
    all_to_all x1, blocking collectives, copy_for_each(): lax.all_to_all(jnp.broadcast_to(x[None], (length, *x.shape)), axis, 0, 0,...  13 us
    all_gather x1, blocking collectives, entering(): near = lax.all_gather(own, ('zl', 'c')).astype(jnp.float32)  12.5 us
    all_to_all x1, waiting for transfers between devices, along_z(): out = lax.all_to_all(x.reshape(chips, 16, width // 8), Z, 0, 0, tiled=True)  11.8 us
    all_to_all x1, waiting for transfers between devices, sum_at_owner(): blocks = lax.all_to_all(in_blocks(x, dim, length), axis, 0, 0, tiled=True)  10.6 us
    another operation x3, other arithmetic, run_blocks(): jax.scipy.linalg.solve_triangular(system, value.reshape(heads, count, BLO...  9.92 us
  transfers between devices with their start and end apart: 3, of which 3 were waited for; matrix products, arithmetic and copies ran while one was open for 0% of the time, Pallas kernels for 0%

profile of v1, /device:TPU:1, one launch (start us, length us, event | category | flops | bytes accessed | tf_op | source)
XLA Modules:
  0.0 217.6 jit_solution(7074667725620606729)
XLA Ops:
  0.8 0.7 divide_reduce_fusion
  1.6 0.9 fusion.56
  2.5 0.8 convert_multiply_fusion.3
  4.3 9.8 %custom-call.4 = f32[2,1,64,64]{2,3,1,0:T(8,128)S(1)} custom-call(f32[2,1,64,64]{3,2,1,0:T(8,128)S(1)} %fusion.46), custom_call_target="InvertDiagBlocksLowerTriangular" | custom-call | tf_op jit(solution)/shard_map/jit(_solve_triangular)/vmap()/triangular_solve | solution.py:119
  14.2 1.1 convolution_bitcast_fusion.3
  15.3 0.9 fusion.57
  16.2 0.8 fusion.58
  17.8 4.7 %while.12 = (s32[]{:T(128)}, f32[1,128,256]{2,1,0:T(8,128)S(1)}, f32[2,1,64,256]{3,2,1,0:T(8,128)S(1)}, f32[2,1]{0,1:T(1,128)S(1)}, f32[2,1,64,128]{3,2,1,0:T(8,...) while((s32[]{:T(128)}, f32[1,128,256]{2,1,0:T(8,128)S(1)}, ...), condition=%wide.region_4.6_spmd, body=%wide.region_3.5_spmd.sunk | while | flops 88178688 | bytes 1116285 | solution.py:154
  19.1 1.0 fusion.151
  21.5 1.0 fusion.151
  22.6 12.5 %all_gather.10 = bf16[4,256,128]{2,1,0:T(8,128)(2,1)S(1)} all-gather(bf16[1,256,128]{2,1,0:T(8,128)(2,1)S(1)} %pad_maximum_fusion), channel_id=1, replica_groups=mesh['zh'=8,'zl'=2,'c'=2,'tp'=16] {'zl','c'}, dimensions={0}, use_global_device_ids=true | all-gather | bytes 327680 | tf_op jit(solution)/shard_map/all_gather | solution.py:27
  36.2 0.8 broadcast_in_dim.39
  37.0 9.6 %all-to-all-start = ((bf16[16,64,128]{2,1,0:T(8,128)(2,1)}), bf16[16,64,128]{2,1,0:T(8,128)(2,1)S(1)}, u32[]{:S(2)}, u32[]{:S(2)}) async-start(bf16[16,64,128]{2,1,0:T(8,128)(2,1)} %broadcast_in_dim.39), calls=%async_computation | async-start | bytes 524288 | tf_op jit(solution)/shard_map/all_to_all | solution.py:41
  46.8 13.9 %all-to-all-done = bf16[16,64,128]{2,1,0:T(8,128)(2,1)S(1)} async-done(((bf16[16,64,128]{2,1,0:T(8,128)(2,1)}), bf16[16,64,128]{2,1,0:T(8,128)(2,1)S(1)}, u32[]{:S(2)}, u32[]{:S(2)}) %all-to-all-start) | async-done | bytes 262176 | tf_op jit(solution)/shard_map/all_to_all | solution.py:41
  60.7 6.8 %all-gather = bf16[32,64,128]{2,1,0:T(8,128)(2,1)S(1)} all-gather(bf16[16,64,128]{2,1,0:T(8,128)(2,1)S(1)} %all-to-all-done), channel_id=2, replica_groups=mesh['zh'=8,'zl'=2,'c'=2,'tp'=16] {'c'}, dimensions={0}, use_global_device_ids=true | all-gather | bytes 786432 | tf_op jit(solution)/shard_map/all_gather | solution.py:42
  69.6 1.2 fusion.18
  70.8 6.8 %all-to-all-start.1 = ((bf16[16,8,2048]{2,1,0:T(8,128)(2,1)}), bf16[16,8,2048]{2,1,0:T(8,128)(2,1)S(1)}, u32[]{:S(2)}, u32[]{:S(2)}) async-start(bf16[16,8,2048]{2,1,0:T(8,128)(2,1)} %fusion.18), calls=%async_computation.1 | async-start | bytes 1048576 | tf_op jit(solution)/shard_map/all_to_all | solution.py:59
  77.7 10.6 %all-to-all-done.1 = bf16[16,8,2048]{2,1,0:T(8,128)(2,1)S(1)} async-done(((bf16[16,8,2048]{2,1,0:T(8,128)(2,1)}), bf16[16,8,2048]{2,1,0:T(8,128)(2,1)S(1)}, u32[]{:S(2)}, u32[]{:S(2)}) %all-to-all-start.1) | async-done | bytes 524320 | tf_op jit(solution)/shard_map/all_to_all | solution.py:59
  88.3 0.9 fusion.99
  89.2 1.0 multiply_reduce_fusion.1
  90.2 0.8 multiply_convert_fusion.1
  91.4 17.4 %all_to_all.35 = bf16[16,16,256]{2,1,0:T(8,128)(2,1)S(1)} all-to-all(bf16[16,16,256]{2,1,0:T(8,128)(2,1)S(1)} %reshape.383), channel_id=1, replica_groups=mesh['zh'=8,'zl'=2,'c'=2,'tp'=16] {'zh','zl'}, dimensions={0} | all-to-all | bytes 262144 | tf_op jit(solution)/shard_map/all_to_all | solution.py:226
  109.2 35.3 %all_to_all.36 = bf16[32,16,2048]{2,1,0:T(8,128)(2,1)S(1)} all-to-all(bf16[32,16,2048]{2,1,0:T(8,128)(2,1)S(1)} %bitcast.275), channel_id=1, replica_groups=mesh['zh'=8,'zl'=2,'c'=2,'tp'=16] {'c','tp'}, dimensions={0} | all-to-all | bytes 4194304 | tf_op jit(solution)/shard_map/all_to_all | solution.py:230
  144.4 1.3 copy-done.1
  145.8 2.1 fusion.22
  147.9 5.4 %convolution_convert_fusion = bf16[512,2048]{1,0:T(8,128)(2,1)} fusion(bf16[1,384,2048]{2,1,0:T(8,128)(2,1)S(1)} %copy-done, bf16[512,2048]{1,0:T(8,128)(2,1)} %bitcast.288, bf16[1,2048,384]{2,1,0:T(8,128)(2,1)S(1)} %copy-done.10, f32[512,384]{1,0:T(8,128)} %fusion.22), kind=kOutput, calls=%fused_computation.22 | convolution fusion | flops 1612840960 | bytes 8126464 | tf_op jit(solution)/shard_map/dot_general | solution.py:239
  153.4 33.0 %all_to_all.37 = bf16[32,16,2048]{2,1,0:T(8,128)(2,1)S(1)} all-to-all(bf16[32,16,2048]{2,1,0:T(8,128)(2,1)} %bitcast.289), channel_id=1, replica_groups=mesh['zh'=8,'zl'=2,'c'=2,'tp'=16] {'c','tp'}, dimensions={0} | all-to-all | bytes 4194304 | tf_op jit(solution)/shard_map/all_to_all | solution.py:230
  186.9 0.7 reshape.389
  187.6 3.5 %all-to-all-start.5 = ((bf16[16,16,256]{2,1,0:T(8,128)(2,1)}), bf16[16,16,256]{2,1,0:T(8,128)(2,1)S(1)}, u32[]{:S(2)}, u32[]{:S(2)}) async-start(bf16[16,16,256]{2,1,0:T(8,128)(2,1)} %reshape.389), calls=%async_computation.5 | async-start | bytes 262144 | tf_op jit(solution)/shard_map/all_to_all | solution.py:226
  191.2 11.8 %all-to-all-done.5 = bf16[16,16,256]{2,1,0:T(8,128)(2,1)S(1)} async-done(((bf16[16,16,256]{2,1,0:T(8,128)(2,1)}), bf16[16,16,256]{2,1,0:T(8,128)(2,1)S(1)}, u32[]{:S(2)}, u32[]{:S(2)}) %all-to-all-start.5) | async-done | bytes 131104 | tf_op jit(solution)/shard_map/all_to_all | solution.py:226
  203.8 13.0 %all_to_all.38 = bf16[16,8,2048]{2,1,0:T(8,128)(2,1)S(1)} all-to-all(bf16[16,8,2048]{2,1,0:T(8,128)(2,1)S(1)} %broadcast_in_dim.41), channel_id=1, replica_groups=mesh['zh'=8,'zl'=2,'c'=2,'tp'=16] {'tp'}, dimensions={0} | all-to-all | bytes 1048576 | tf_op jit(solution)/shard_map/all_to_all | solution.py:65
  216.8 0.8 copy.73
  (95 shorter events, 9.9 us)
Async XLA Ops:
  0.0 147.9 %copy-start = (bf16[1,384,2048]{2,1,0:T(8,128)(2,1)S(1)}, bf16[1,384,2048]{2,1,0:T(8,128)(2,1)}, u32[]{:S(2)}) copy-start(bf16[1,384,2048]{2,1,0:T(8,128)(2,1)} %param.37) | copy-start | bytes 4718596
  22.6 24.1 %copy-start.3 = (bf16[128,128]{1,0:T(8,128)(2,1)S(1)}, bf16[128,128]{1,0:T(8,128)(2,1)}, u32[]{:S(2)}) copy-start(bf16[128,128]{1,0:T(8,128)(2,1)} %param.25) | copy-start | bytes 98308
  37.0 23.7 %all-to-all-start = ((bf16[16,64,128]{2,1,0:T(8,128)(2,1)}), bf16[16,64,128]{2,1,0:T(8,128)(2,1)S(1)}, u32[]{:S(2)}, u32[]{:S(2)}) async-start(bf16[16,64,128]{2,1,0:T(8,128)(2,1)} %broadcast_in_dim.39), calls=%async_computation | async-start | bytes 524288 | tf_op jit(solution)/shard_map/all_to_all | solution.py:41
  67.5 2.0 copy-start.2
  67.6 2.0 copy-start.8
  68.0 9.5 %copy-start.6 = (s32[128,2]{0,1:T(2,128)S(1)}, s32[128,2]{0,1:T(2,128)}, u32[]{:S(2)}) copy-start(s32[128,2]{0,1:T(2,128)} %param.33) | copy-start | bytes 3076
  68.6 21.6 %copy-start.4 = (f32[2048]{0:T(1024)S(1)}, f32[2048]{0:T(1024)}, u32[]{:S(2)}) copy-start(f32[2048]{0:T(1024)} %param.31) | copy-start | bytes 24580
  70.8 17.5 %all-to-all-start.1 = ((bf16[16,8,2048]{2,1,0:T(8,128)(2,1)}), bf16[16,8,2048]{2,1,0:T(8,128)(2,1)S(1)}, u32[]{:S(2)}, u32[]{:S(2)}) async-start(bf16[16,8,2048]{2,1,0:T(8,128)(2,1)} %fusion.18), calls=%async_computation.1 | async-start | bytes 1048576 | tf_op jit(solution)/shard_map/all_to_all | solution.py:59
  109.1 36.6 %copy-start.9 = (bf16[1,2048,384]{2,1,0:T(8,128)(2,1)S(1)}, bf16[1,2048,384]{2,1,0:T(8,128)(2,1)}, u32[]{:S(2)}) copy-start(bf16[1,2048,384]{2,1,0:T(8,128)(2,1)} %param.35) | copy-start | bytes 4718596
  144.4 1.4 copy-start.1
  145.8 2.2 copy-start.10
  186.4 4.8 %copy-start.7 = (f32[128,2]{0,1:T(2,128)S(1)}, f32[128,2]{0,1:T(2,128)}, u32[]{:S(2)}) copy-start(f32[128,2]{0,1:T(2,128)} %param.34) | copy-start | bytes 3076
  186.4 17.3 %copy-start.5 = (f32[2048]{0:T(1024)S(1)}, f32[2048]{0:T(1024)}, u32[]{:S(2)}) copy-start(f32[2048]{0:T(1024)} %param.32) | copy-start | bytes 24580
  187.6 15.4 %all-to-all-start.5 = ((bf16[16,16,256]{2,1,0:T(8,128)(2,1)}), bf16[16,16,256]{2,1,0:T(8,128)(2,1)S(1)}, u32[]{:S(2)}, u32[]{:S(2)}) async-start(bf16[16,16,256]{2,1,0:T(8,128)(2,1)} %reshape.389), calls=%async_computation.5 | async-start | bytes 262144 | tf_op jit(solution)/shard_map/all_to_all | solution.py:226

commit v2 on v1

--- a/solution.py
+++ b/solution.py
@@ -1,12 +1,13 @@
 import jax
 import jax.numpy as jnp
 from jax import lax
+from jax.experimental import pallas as pl
+from jax.experimental.pallas import tpu as pltpu
 from jax.sharding import Mesh
 from jax.sharding import PartitionSpec as P
 
 HEAD_FEATURES = 128
 TOP = 2
-BLOCK = 64
 Z = ("zh", "zl")
 SP = ("zh", "zl", "c")
 PLANE = ("c", "tp")
@@ -20,12 +21,11 @@
     return jnp.dot(a, b, precision=highest_precision)
 
 
-def entering(map_here, state_here):
+def entering(own):
     kind = jnp.bfloat16
     zh, zl, c = (lax.axis_index(axis) for axis in SP)
-    own = jnp.concatenate([map_here, state_here], 0).astype(kind)
     near = lax.all_gather(own, ("zl", "c")).astype(jnp.float32)
-    width = map_here.shape[-1]
+    width = own.shape[-1]
     map_in, state_in = (jnp.eye(width, dtype=jnp.float32), jnp.zeros((width, width), jnp.float32))
     map_all, state_all = (near[0, :width], near[0, width:])
     for k in range(1, 4):
@@ -76,83 +76,65 @@
     return in_order(blocks, dim)
 
 
-def unit_rows(data):
-    return data * lax.rsqrt(jnp.sum(data * data, -1, keepdims=True) + 1e-06)
-
-
 def layer_norm(data, gain):
     center = data - jnp.mean(data, -1, keepdims=True)
     return center * lax.rsqrt(jnp.mean(center * center, -1, keepdims=True) + 1e-05) * gain
 
 
-def block_terms(query, key, beta, decay):
-    heads, length, width = query.shape
-    count = length // BLOCK
-    shape = (heads, count, BLOCK, width)
-    query = query.reshape(shape)
-    key = key.reshape(shape)
-    beta = beta.reshape(heads, count, BLOCK)
-    running = jnp.cumsum(decay.reshape(heads, count, BLOCK), axis=-1)
-    causal = jnp.tril(jnp.ones((BLOCK, BLOCK), bool))
-    strict = jnp.tril(jnp.ones((BLOCK, BLOCK), bool), -1)
-    within = jnp.exp(jnp.where(causal, running[..., :, None] - running[..., None, :], -jnp.inf))
-    key_beta = key * beta[..., None]
+def local_span(q_ref, k_ref, v_ref, beta_ref, decay_ref, rate_ref, both_ref, mix_ref, out_ref):
+    size = HEAD_FEATURES
+    row = lax.broadcasted_iota(jnp.int32, (size, size), 0)
+    col = lax.broadcasted_iota(jnp.int32, (size, size), 1)
+    eye = row == col
+    causal = col <= row
+
+    def to_column(data):
+        return jnp.sum(jnp.where(eye, data, 0.0), 1, keepdims=True)
+
+    def to_row(data):
+        return jnp.sum(jnp.where(eye, data, 0.0), 0, keepdims=True)
+
+    def dot(a, b, dims=((1,), (0,))):
+        return lax.dot_general(
+            a.astype(jnp.bfloat16),
+            b.astype(jnp.bfloat16),
+            (dims, ((), ())),
+            preferred_element_type=jnp.float32,
+        )
+
+    beta = to_column(jax.nn.sigmoid(beta_ref[...].astype(jnp.float32)))
+    logit = decay_ref[...].astype(jnp.float32)
+    softplus = jnp.maximum(logit, 0.0) + jnp.log(1.0 + jnp.exp(-jnp.abs(logit)))
+    decay = -jnp.exp(jnp.full((1, size), rate_ref[0], jnp.float32)) * softplus
+    running = jnp.sum(jnp.where(causal, decay, 0.0), 1, keepdims=True)
+    last = jnp.sum(decay, 1, keepdims=True)
+    within = jnp.exp(jnp.where(causal, running - to_row(running), -1e30))
+    query = q_ref[...].astype(jnp.float32)
+    key = k_ref[...].astype(jnp.float32)
+    value = v_ref[...].astype(jnp.float32)
+    query_scale = lax.rsqrt(jnp.sum(query * query, 1, keepdims=True) + 1e-06) * size ** (-0.5)
+    key_scale = lax.rsqrt(jnp.sum(key * key, 1, keepdims=True) + 1e-06)
+    key_scale_row = to_row(key_scale)
+    across = within * key_scale_row
     lower = jnp.where(
-        strict,
-        jnp.einsum("hnid,hnjd->hnij", key_beta, key, precision=highest_precision) * within,
-        0.0,
-    )
-    system = jnp.eye(BLOCK, dtype=jnp.float32) + lower
-    weighted = jax.scipy.linalg.solve_triangular(
-        system, key_beta * jnp.exp(running)[..., None], lower=True, unit_diagonal=True
-    )
-    scores = jnp.einsum("hnid,hnjd->hnij", query, key, precision=highest_precision) * within
-    query_decayed = query * jnp.exp(running)[..., None]
-    key_decayed = key * jnp.exp(running[..., -1:] - running)[..., None]
-    block_decay = jnp.exp(running[..., -1])
-    return (system, beta, weighted, query_decayed, key_decayed, scores, block_decay)
-
-
-def run_blocks(terms, value, start):
-    system, beta, weighted, query_decayed, key_decayed, scores, block_decay = terms
-    heads, count = (beta.shape[0], beta.shape[1])
-    fresh = jax.scipy.linalg.solve_triangular(
-        system,
-        value.reshape(heads, count, BLOCK, -1) * beta[..., None],
-        lower=True,
-        unit_diagonal=True,
-    )
-    missing = start.shape[-1] - fresh.shape[-1]
-    fresh = jnp.concatenate([fresh, jnp.zeros(fresh.shape[:-1] + (missing,), jnp.float32)], -1)
-
-    def advance(recurrent_state, inputs):
-        (
-            fresh_value_block,
-            block_weighted_values,
-            block_queries,
-            block_keys,
-            block_scores,
-            block_decay_factor,
-        ) = inputs
-        corrected_value = fresh_value_block - jnp.einsum(
-            "nya,nag->nyg", block_weighted_values, recurrent_state, precision=highest_precision
-        )
-        state_next = block_decay_factor[:, None, None] * recurrent_state + jnp.einsum(
-            "iyp,iyu->ipu", block_keys, corrected_value, precision=highest_precision
-        )
-        final_output = jnp.einsum(
-            "nya,nag->nyg", block_queries, recurrent_state, precision=highest_precision
-        ) + jnp.einsum("emp,epk->emk", block_scores, corrected_value, precision=highest_precision)
-        return (state_next, final_output)
-
-    inputs = tuple(
-        (
-            jnp.moveaxis(item, 1, 0)
-            for item in (fresh, weighted, query_decayed, key_decayed, scores, block_decay)
-        )
-    )
-    final, output_list = lax.scan(advance, start, inputs)
-    return (jnp.moveaxis(output_list, 0, 1).reshape(heads, count * BLOCK, -1), final)
+        col < row, dot(k_ref[...], k_ref[...], ((1,), (1,))) * across * (beta * key_scale), 0.0
+    )
+    scores = dot(q_ref[...], k_ref[...], ((1,), (1,))) * across * query_scale
+    differ = row ^ col
+    inverse = jnp.where(eye, 1.0, 0.0) - jnp.where(differ == 1, lower, 0.0)
+    for level in range(1, 7):
+        part = jnp.where((differ >> level) == 1, lower, 0.0)
+        inverse = inverse - dot(dot(inverse, part), inverse)
+    grown = jnp.exp(running)
+    key = key * key_scale
+    right = jnp.concatenate([key * (beta * grown), value * beta], 1)
+    solved = dot(inverse, right)
+    leaving = dot(key * jnp.exp(last - running), solved, ((0,), (0,)))
+    passed = jnp.where(eye, jnp.exp(last), 0.0) - leaving[:, :size]
+    both_ref[...] = jnp.concatenate([passed, leaving[:, size:]], 0).astype(both_ref.dtype)
+    seen = dot(scores, solved)
+    mix_ref[...] = query * (query_scale * grown) - seen[:, :size]
+    out_ref[...] = seen[:, size:]
 
 
 def per_device(
@@ -175,34 +157,22 @@
     expert_down,
 ):
     length, width = residual_in.shape
-    heads = beta_logit.shape[0]
-
-    def split_heads(data):
-        return data.astype(jnp.float32).reshape(length, heads, HEAD_FEATURES).transpose(1, 0, 2)
-
-    query = unit_rows(split_heads(queries)) * HEAD_FEATURES ** (-0.5)
-    key = unit_rows(split_heads(keys))
-    value = split_heads(values)
-    beta = jax.nn.sigmoid(beta_logit.astype(jnp.float32))
-    decay = -jnp.exp(decay_log)[:, None] * jax.nn.softplus(decay_logit.astype(jnp.float32))
-    terms = block_terms(query, key, beta, decay)
-    identity_map = jnp.broadcast_to(
-        jnp.eye(HEAD_FEATURES, dtype=jnp.float32), (heads, HEAD_FEATURES, HEAD_FEATURES)
-    )
-    blank = jnp.zeros((heads, HEAD_FEATURES, HEAD_FEATURES), jnp.float32)
-    extended = jnp.concatenate([blank, identity_map], -1)
-    output_list, final = run_blocks(terms, value, extended)
-    entry_value = entering(final[0, :, HEAD_FEATURES:], final[0, :, :HEAD_FEATURES])[None]
-    mixed = output_list[..., :HEAD_FEATURES] + jnp.einsum(
-        "apj,ajz->apz", output_list[..., HEAD_FEATURES:], entry_value, precision=highest_precision
-    )
+
+    vmem = pl.BlockSpec(memory_space=pltpu.VMEM)
+    both, mix, local = pl.pallas_call(
+        local_span,
+        out_shape=(
+            jax.ShapeDtypeStruct((2 * HEAD_FEATURES, HEAD_FEATURES), jnp.bfloat16),
+            jax.ShapeDtypeStruct((length, HEAD_FEATURES), jnp.float32),
+            jax.ShapeDtypeStruct((length, HEAD_FEATURES), jnp.float32),
+        ),
+        in_specs=[vmem] * 5 + [pl.BlockSpec(memory_space=pltpu.SMEM)],
+        out_specs=(vmem,) * 3,
+        name="local_span",
+    )(queries, keys, values, beta_logit, decay_logit, decay_log)
+    mixed = local + mm(mix, entering(both))
     normalized = mixed * lax.rsqrt(jnp.mean(mixed * mixed, -1, keepdims=True) + 1e-06) * head_gain
-    gated = (
-        (normalized * jax.nn.silu(split_heads(out_gate)))
-        .transpose(1, 0, 2)
-        .reshape(length, heads * HEAD_FEATURES)
-        .astype(jnp.bfloat16)
-    )
+    gated = (normalized * jax.nn.silu(out_gate.astype(jnp.float32))).astype(jnp.bfloat16)
     split_count = lax.axis_size("tp")
     expert_count = lax.axis_size(SP) * expert_gate.shape[0]
     rows = length // split_count

time: 222 us -> 203 us (0.914)
  other arithmetic: 18.4 us -> 3.86 us
  matrix products: 17.2 us -> 11.9 us
  Pallas kernels: 0 us -> 3.4 us
    another operation x5 -> x0, other arithmetic: 10.2 us -> none  [the longest x3 9.92 us: run_blocks(): jax.scipy.linalg.solve_triangular(system, value.reshape(heads, count, BLO...]
    dot_general x11 -> x0, matrix products: 4.17 us -> none  [the longest x2 2.1 us: advance(): jnp.einsum('iyp,iyu->ipu', block_keys, corrected_value, precision=highest...]
    pallas_call x0 -> x1, Pallas kernels: none -> 3.4 us  [per_device(): pl.pallas_call(local_span, out_shape=(jax.ShapeDtypeStruct((2 * HEAD_FEAT...]
where the time goes in v2:
time: 203 us; the launch traced here: 199 us
  blocking collectives  118 us (58%)
  waiting for transfers between devices  36.5 us (18%)
  starting transfers between devices  19.8 us (10%)
  matrix products  11.9 us (6%)
  local copies, waits for them, and re-layouts  4.52 us (2%)
  other arithmetic  3.86 us (2%)
  Pallas kernels  3.4 us (2%)
    all_to_all x2, blocking collectives, in_plane(): return lax.all_to_all(x, PLANE, 0, 0, tiled=True)  68.3 us
    all_to_all x1, blocking collectives, along_z(): out = lax.all_to_all(x.reshape(chips, 16, width // 8), Z, 0, 0, tiled=True)  17.5 us
    all_to_all x1, waiting for transfers between devices, entering(): lax.all_to_all(jnp.broadcast_to(quarter[None], (count, *quarter.shape)),...  14.1 us
    all_to_all x1, blocking collectives, copy_for_each(): lax.all_to_all(jnp.broadcast_to(x[None], (length, *x.shape)), axis, 0, 0,...  13 us
    all_gather x1, blocking collectives, entering(): near = lax.all_gather(own, ('zl', 'c')).astype(jnp.float32)  12.7 us
    all_to_all x1, waiting for transfers between devices, along_z(): out = lax.all_to_all(x.reshape(chips, 16, width // 8), Z, 0, 0, tiled=True)  11.8 us
    all_to_all x1, waiting for transfers between devices, sum_at_owner(): blocks = lax.all_to_all(in_blocks(x, dim, length), axis, 0, 0, tiled=True)  10.6 us
    all_to_all x1, starting transfers between devices, entering(): lax.all_to_all(jnp.broadcast_to(quarter[None], (count, *quarter.shape)),...  9.57 us
  transfers between devices with their start and end apart: 3, of which 3 were waited for; matrix products, arithmetic and copies ran while one was open for 0% of the time, Pallas kernels for 0%

profile of v2, /device:TPU:1, one launch (start us, length us, event | category | flops | bytes accessed | tf_op | source)
XLA Modules:
  0.0 199.4 jit_solution(3178505045244934397)
XLA Ops:
  0.8 3.4 %local_span.1 = (bf16[256,128]{1,0:T(8,128)(2,1)}, f32[128,128]{1,0:T(8,128)}, f32[128,128]{1,0:T(8,128)}) custom-call(bf16[128,128]{1,0:T(8,128)(2,1)} %q_ref.1, bf16[128,128]{1,0:T(8,128)(2,1)} %k_ref.1, bf16[128,128]{1,0:T(8,128)(2,1)} %v_ref.1, bf16[1,128]{1,0:T(2,128)(2,1)} %beta_ref.1, bf16[1,128]{1,0:T(2,128)(2,1)} %decay_ref.1, f32[1]{0:T(128)S(6)} %copy.32.rate_ref), custom_call_target="tpu_custom_call" | custom-call | tf_op jit(solution)/shard_map/local_span/pallas_call | solution.py:162
  4.2 12.7 %all-gather = bf16[1024,128]{1,0:T(8,128)(2,1)S(1)} all-gather(bf16[256,128]{1,0:T(8,128)(2,1)} %get-tuple-element.10), channel_id=2, replica_groups=mesh['zh'=8,'zl'=2,'c'=2,'tp'=16] {'zl','c'}, dimensions={0}, use_global_device_ids=true | all-gather | bytes 327680 | tf_op jit(solution)/shard_map/all_gather | solution.py:27
  17.1 0.2 convolution_add_fusion.10
  18.0 0.8 broadcast_in_dim.6
  18.7 9.6 %all-to-all-start = ((bf16[16,64,128]{2,1,0:T(8,128)(2,1)}), bf16[16,64,128]{2,1,0:T(8,128)(2,1)S(1)}, u32[]{:S(2)}, u32[]{:S(2)}) async-start(bf16[16,64,128]{2,1,0:T(8,128)(2,1)} %broadcast_in_dim.6), calls=%async_computation | async-start | bytes 524288 | tf_op jit(solution)/shard_map/all_to_all | solution.py:41
  28.4 14.1 %all-to-all-done = bf16[16,64,128]{2,1,0:T(8,128)(2,1)S(1)} async-done(((bf16[16,64,128]{2,1,0:T(8,128)(2,1)}), bf16[16,64,128]{2,1,0:T(8,128)(2,1)S(1)}, u32[]{:S(2)}, u32[]{:S(2)}) %all-to-all-start) | async-done | bytes 262176 | tf_op jit(solution)/shard_map/all_to_all | solution.py:41
  42.5 6.8 %all-gather.1 = bf16[32,64,128]{2,1,0:T(8,128)(2,1)S(1)} all-gather(bf16[16,64,128]{2,1,0:T(8,128)(2,1)S(1)} %all-to-all-done), channel_id=3, replica_groups=mesh['zh'=8,'zl'=2,'c'=2,'tp'=16] {'c'}, dimensions={0}, use_global_device_ids=true | all-gather | bytes 786432 | tf_op jit(solution)/shard_map/all_gather | solution.py:42
  50.0 0.2 fusion.16
  50.8 0.2 convolution_add_fusion.1
  51.0 0.3 multiply_reduce_fusion.2
  51.4 1.1 fusion
  52.5 6.8 %all-to-all-start.1 = ((bf16[16,8,2048]{2,1,0:T(8,128)(2,1)}), bf16[16,8,2048]{2,1,0:T(8,128)(2,1)S(1)}, u32[]{:S(2)}, u32[]{:S(2)}) async-start(bf16[16,8,2048]{2,1,0:T(8,128)(2,1)} %fusion), calls=%async_computation.1 | async-start | bytes 1048576 | tf_op jit(solution)/shard_map/all_to_all | solution.py:59
  59.4 10.6 %all-to-all-done.1 = bf16[16,8,2048]{2,1,0:T(8,128)(2,1)S(1)} async-done(((bf16[16,8,2048]{2,1,0:T(8,128)(2,1)}), bf16[16,8,2048]{2,1,0:T(8,128)(2,1)S(1)}, u32[]{:S(2)}, u32[]{:S(2)}) %all-to-all-start.1) | async-done | bytes 524320 | tf_op jit(solution)/shard_map/all_to_all | solution.py:59
  70.1 0.9 fusion.54
  71.0 1.0 multiply_reduce_fusion.1
  71.9 0.8 multiply_convert_fusion.1
  72.8 0.2 convolution_convert_fusion.2
  73.1 17.5 %all_to_all.35 = bf16[16,16,256]{2,1,0:T(8,128)(2,1)S(1)} all-to-all(bf16[16,16,256]{2,1,0:T(8,128)(2,1)S(1)} %reshape.79), channel_id=1, replica_groups=mesh['zh'=8,'zl'=2,'c'=2,'tp'=16] {'zh','zl'}, dimensions={0} | all-to-all | bytes 262144 | tf_op jit(solution)/shard_map/all_to_all | solution.py:196
  90.6 0.2 broadcast_in_dim.7
  90.9 35.3 %all_to_all.36 = bf16[32,16,2048]{2,1,0:T(8,128)(2,1)S(1)} all-to-all(bf16[32,16,2048]{2,1,0:T(8,128)(2,1)S(1)} %bitcast.146), channel_id=1, replica_groups=mesh['zh'=8,'zl'=2,'c'=2,'tp'=16] {'c','tp'}, dimensions={0} | all-to-all | bytes 4194304 | tf_op jit(solution)/shard_map/all_to_all | solution.py:200
  126.2 1.3 copy-done.1
  127.5 2.2 %fusion.4 = f32[512,384]{1,0:T(8,128)} fusion(bf16[512,2048]{1,0:T(8,128)(2,1)S(1)} %bitcast.161, bf16[1,2048,384]{2,1,0:T(8,128)(2,1)S(1)} %copy-done.11), kind=kOutput, calls=%fused_computation.9 | convolution fusion | flops 805306368 | bytes 4456448 | tf_op jit(solution)/shard_map/dot_general | solution.py:206
  129.7 5.4 %convolution_convert_fusion = bf16[512,2048]{1,0:T(8,128)(2,1)} fusion(bf16[1,384,2048]{2,1,0:T(8,128)(2,1)S(1)} %copy-done, bf16[512,2048]{1,0:T(8,128)(2,1)} %bitcast.162, bf16[1,2048,384]{2,1,0:T(8,128)(2,1)S(1)} %copy-done.12, f32[512,384]{1,0:T(8,128)} %fusion.4), kind=kOutput, calls=%fused_computation | convolution fusion | flops 1612840960 | bytes 8126464 | tf_op jit(solution)/shard_map/dot_general | solution.py:209
  135.1 33.0 %all_to_all.37 = bf16[32,16,2048]{2,1,0:T(8,128)(2,1)S(1)} all-to-all(bf16[32,16,2048]{2,1,0:T(8,128)(2,1)} %bitcast.163), channel_id=1, replica_groups=mesh['zh'=8,'zl'=2,'c'=2,'tp'=16] {'c','tp'}, dimensions={0} | all-to-all | bytes 4194304 | tf_op jit(solution)/shard_map/all_to_all | solution.py:200
  168.1 0.3 bitcast_reduce_fusion
  168.6 0.7 reshape.85
  169.4 3.5 %all-to-all-start.5 = ((bf16[16,16,256]{2,1,0:T(8,128)(2,1)}), bf16[16,16,256]{2,1,0:T(8,128)(2,1)S(1)}, u32[]{:S(2)}, u32[]{:S(2)}) async-start(bf16[16,16,256]{2,1,0:T(8,128)(2,1)} %reshape.85), calls=%async_computation.5 | async-start | bytes 262144 | tf_op jit(solution)/shard_map/all_to_all | solution.py:196
  173.0 11.8 %all-to-all-done.5 = bf16[16,16,256]{2,1,0:T(8,128)(2,1)S(1)} async-done(((bf16[16,16,256]{2,1,0:T(8,128)(2,1)}), bf16[16,16,256]{2,1,0:T(8,128)(2,1)S(1)}, u32[]{:S(2)}, u32[]{:S(2)}) %all-to-all-start.5) | async-done | bytes 131104 | tf_op jit(solution)/shard_map/all_to_all | solution.py:196
  184.9 0.2 fusion.12
  185.2 0.2 multiply_reduce_fusion
  185.6 13.0 %all_to_all.38 = bf16[16,8,2048]{2,1,0:T(8,128)(2,1)S(1)} all-to-all(bf16[16,8,2048]{2,1,0:T(8,128)(2,1)S(1)} %broadcast_in_dim.8), channel_id=1, replica_groups=mesh['zh'=8,'zl'=2,'c'=2,'tp'=16] {'tp'}, dimensions={0} | all-to-all | bytes 1048576 | tf_op jit(solution)/shard_map/all_to_all | solution.py:65
  198.6 0.8 copy.33
  (57 shorter events, 3.1 us)
Async XLA Ops:
  0.0 129.7 %copy-start = (bf16[1,384,2048]{2,1,0:T(8,128)(2,1)S(1)}, bf16[1,384,2048]{2,1,0:T(8,128)(2,1)}, u32[]{:S(2)}) copy-start(bf16[1,384,2048]{2,1,0:T(8,128)(2,1)} %param.33) | copy-start | bytes 4718596
  18.7 23.7 %all-to-all-start = ((bf16[16,64,128]{2,1,0:T(8,128)(2,1)}), bf16[16,64,128]{2,1,0:T(8,128)(2,1)S(1)}, u32[]{:S(2)}, u32[]{:S(2)}) async-start(bf16[16,64,128]{2,1,0:T(8,128)(2,1)} %broadcast_in_dim.6), calls=%async_computation | async-start | bytes 524288 | tf_op jit(solution)/shard_map/all_to_all | solution.py:41
  49.3 1.7 copy-start.3
  49.3 1.8 copy-start.4
  49.3 2.0 %copy-start.2 = (bf16[128,2048]{1,0:T(8,128)(2,1)S(1)}, bf16[128,2048]{1,0:T(8,128)(2,1)}, u32[]{:S(2)}) copy-start(bf16[128,2048]{1,0:T(8,128)(2,1)} %param.26) | copy-start | bytes 1572868
  49.3 2.0 %copy-start.5 = (bf16[128,128]{1,0:T(8,128)(2,1)S(1)}, bf16[128,128]{1,0:T(8,128)(2,1)}, u32[]{:S(2)}) copy-start(bf16[128,128]{1,0:T(8,128)(2,1)} %param.21) | copy-start | bytes 98308
  49.3 2.0 %copy-start.10 = (f32[128]{0:T(128)S(1)}, f32[128]{0:T(128)}, u32[]{:S(2)}) copy-start(f32[128]{0:T(128)} %param.25) | copy-start | bytes 1540
  49.8 9.5 %copy-start.8 = (s32[128,2]{0,1:T(2,128)S(1)}, s32[128,2]{0,1:T(2,128)}, u32[]{:S(2)}) copy-start(s32[128,2]{0,1:T(2,128)} %param.29) | copy-start | bytes 3076
  50.4 21.5 %copy-start.6 = (f32[2048]{0:T(1024)S(1)}, f32[2048]{0:T(1024)}, u32[]{:S(2)}) copy-start(f32[2048]{0:T(1024)} %param.27) | copy-start | bytes 24580
  52.5 17.5 %all-to-all-start.1 = ((bf16[16,8,2048]{2,1,0:T(8,128)(2,1)}), bf16[16,8,2048]{2,1,0:T(8,128)(2,1)S(1)}, u32[]{:S(2)}, u32[]{:S(2)}) async-start(bf16[16,8,2048]{2,1,0:T(8,128)(2,1)} %fusion), calls=%async_computation.1 | async-start | bytes 1048576 | tf_op jit(solution)/shard_map/all_to_all | solution.py:59
  90.9 36.6 %copy-start.11 = (bf16[1,2048,384]{2,1,0:T(8,128)(2,1)S(1)}, bf16[1,2048,384]{2,1,0:T(8,128)(2,1)}, u32[]{:S(2)}) copy-start(bf16[1,2048,384]{2,1,0:T(8,128)(2,1)} %param.31) | copy-start | bytes 4718596
  126.2 1.4 copy-start.1
  127.5 2.2 %copy-start.12 = (bf16[1,2048,384]{2,1,0:T(8,128)(2,1)S(1)}, bf16[1,2048,384]{2,1,0:T(8,128)(2,1)}, u32[]{:S(2)}) copy-start(bf16[1,2048,384]{2,1,0:T(8,128)(2,1)} %param.32) | copy-start | bytes 4718596
  168.1 4.8 %copy-start.9 = (f32[128,2]{0,1:T(2,128)S(1)}, f32[128,2]{0,1:T(2,128)}, u32[]{:S(2)}) copy-start(f32[128,2]{0,1:T(2,128)} %param.30) | copy-start | bytes 3076
  168.1 17.3 %copy-start.7 = (f32[2048]{0:T(1024)S(1)}, f32[2048]{0:T(1024)}, u32[]{:S(2)}) copy-start(f32[2048]{0:T(1024)} %param.28) | copy-start | bytes 24580
  169.4 15.4 %all-to-all-start.5 = ((bf16[16,16,256]{2,1,0:T(8,128)(2,1)}), bf16[16,16,256]{2,1,0:T(8,128)(2,1)S(1)}, u32[]{:S(2)}, u32[]{:S(2)}) async-start(bf16[16,16,256]{2,1,0:T(8,128)(2,1)} %reshape.85), calls=%async_computation.5 | async-start | bytes 262144 | tf_op jit(solution)/shard_map/all_to_all | solution.py:196

commit v3 on v2

--- a/solution.py
+++ b/solution.py
@@ -6,8 +6,8 @@
 from jax.sharding import Mesh
 from jax.sharding import PartitionSpec as P
 
+
 HEAD_FEATURES = 128
-TOP = 2
 Z = ("zh", "zl")
 SP = ("zh", "zl", "c")
 PLANE = ("c", "tp")
@@ -17,11 +17,57 @@
 residual_scale = 2.0**0.5
 
 
+def held(x):
+    return pltpu.with_memory_space_constraint(x, pltpu.VMEM)
+
+
 def mm(a, b):
     return jnp.dot(a, b, precision=highest_precision)
 
 
-def entering(own):
+def pack_thirds(gate_ref, up_ref, down_ref, first_ref, second_ref, third_ref, sems):
+    share = down_ref.shape[0] // 3
+    copies = []
+    for part, ref in enumerate((first_ref, second_ref, third_ref)):
+        cut = pl.ds(part * share, share)
+        moves = [(gate_ref.at[:, cut], ref.at[:, pl.ds(0, share)])]
+        moves.append((up_ref.at[:, cut], ref.at[:, pl.ds(share, share)]))
+        for k in range(0, ref.shape[0], share):
+            source = down_ref.at[cut, pl.ds(k, share)]
+            moves.append((source, ref.at[pl.ds(k, share), pl.ds(2 * share, share)]))
+        copies += moves
+    copies = [pltpu.make_async_copy(x, y, sems.at[k]) for k, (x, y) in enumerate(copies)]
+    for copy in copies:
+        copy.start()
+    for copy in copies:
+        copy.wait()
+
+
+def spread(gate, up, down, side):
+    width, share = gate.shape
+    share //= 3
+    packed = jax.ShapeDtypeStruct((width, 3 * share), gate.dtype)
+    anywhere = pl.BlockSpec(memory_space=pl.ANY)
+    thirds = pl.pallas_call(
+        pack_thirds,
+        out_shape=(packed,) * 3,
+        in_specs=[anywhere] * 3,
+        out_specs=(anywhere,) * 3,
+        scratch_shapes=[pltpu.SemaphoreType.DMA((3 * (2 + width // share),))],
+        name="pack_thirds",
+    )(gate, up, down)
+    out = []
+    for third, (dy, dx) in zip(thirds, ((0, 1), (0, side - 1), (1, 0))):
+        pairs = [
+            (y * side + x, (y + dy) % side * side + (x + dx) % side)
+            for y in range(side)
+            for x in range(side)
+        ]
+        out.append(lax.ppermute(third, "tp", pairs))
+    return out
+
+
+def entering(own, weights, side):
     kind = jnp.bfloat16
     zh, zl, c = (lax.axis_index(axis) for axis in SP)
     near = lax.all_gather(own, ("zl", "c")).astype(jnp.float32)
@@ -38,14 +84,17 @@
     group = jnp.concatenate([map_all, state_all], 0).astype(kind)
     quarter = lax.dynamic_slice_in_dim(group, (2 * zl + c) * (width // 2), width // 2, 0)
     count = lax.axis_size(Z)
-    far = lax.all_to_all(jnp.broadcast_to(quarter[None], (count, *quarter.shape)), Z, 0, 0, tiled=True)
+    quarter, weights = lax.optimization_barrier((quarter, weights))
+    thirds = spread(*weights, side)
+    far = jnp.broadcast_to(quarter[None], (count, *quarter.shape))
+    far = lax.all_to_all(far, Z, 0, 0, tiled=True)
     far = lax.all_gather(far, "c")
     far = far.reshape(2, count // 2, 2, width // 2, width).transpose(1, 2, 0, 3, 4)
     far = far.reshape(count // 2, 2 * width, width).astype(jnp.float32)
     state = jnp.zeros((width, width), jnp.float32)
     for k in range(count // 2 - 1):
         state = jnp.where(k < zh, mm(far[k, :width], state) + far[k, width:], state)
-    return mm(map_in, state) + state_in
+    return mm(map_in, state) + state_in, thirds
 
 
 def in_blocks(x, dim, length):
@@ -137,6 +186,33 @@
     out_ref[...] = seen[:, size:]
 
 
+def run_experts(rows_ref, *refs):
+    out_ref, bufs, sems = refs[6], refs[7:13], refs[13]
+    copies = [pltpu.make_async_copy(refs[k], bufs[k], sems.at[k]) for k in range(6)]
+    for copy in copies:
+        copy.start()
+    gate_ref, up_ref, down_ref = bufs[:3]
+    rows = rows_ref[...]
+    share = bufs[3].shape[1] // 3
+
+    def dot(a, b):
+        return jnp.dot(a, b, preferred_element_type=jnp.float32)
+
+    copies[0].wait()
+    gate = dot(rows, gate_ref[...])
+    copies[1].wait()
+    inner = (jax.nn.silu(gate) * dot(rows, up_ref[...])).astype(jnp.bfloat16)
+    copies[2].wait()
+    total = dot(inner, down_ref[...])
+    for copy, ref in zip(copies[3:], bufs[3:]):
+        copy.wait()
+        both = dot(rows, ref[:, : 2 * share])
+        inner = (jax.nn.silu(both[:, :share]) * both[:, share:]).astype(jnp.bfloat16)
+        down = [ref[k : k + share, 2 * share :] for k in range(0, ref.shape[0], share)]
+        total = total + dot(inner, jnp.concatenate(down, 1))
+    out_ref[...] = total.astype(out_ref.dtype)
+
+
 def per_device(
     residual_in,
     queries,
@@ -162,18 +238,21 @@
     both, mix, local = pl.pallas_call(
         local_span,
         out_shape=(
-            jax.ShapeDtypeStruct((2 * HEAD_FEATURES, HEAD_FEATURES), jnp.bfloat16),
-            jax.ShapeDtypeStruct((length, HEAD_FEATURES), jnp.float32),
-            jax.ShapeDtypeStruct((length, HEAD_FEATURES), jnp.float32),
+            pltpu.VMEM((2 * HEAD_FEATURES, HEAD_FEATURES), jnp.bfloat16),
+            pltpu.VMEM((length, HEAD_FEATURES), jnp.float32),
+            pltpu.VMEM((length, HEAD_FEATURES), jnp.float32),
         ),
         in_specs=[vmem] * 5 + [pl.BlockSpec(memory_space=pltpu.SMEM)],
         out_specs=(vmem,) * 3,
         name="local_span",
     )(queries, keys, values, beta_logit, decay_logit, decay_log)
-    mixed = local + mm(mix, entering(both))
+    split_count = lax.axis_size("tp")
+    side = round(split_count**0.5)
+    gate_matrix, up_matrix, down_matrix = (expert_gate[0], expert_up[0], expert_down[0])
+    state, thirds = entering(both, (gate_matrix, up_matrix, down_matrix), side)
+    mixed = local + mm(mix, state)
     normalized = mixed * lax.rsqrt(jnp.mean(mixed * mixed, -1, keepdims=True) + 1e-06) * head_gain
     gated = (normalized * jax.nn.silu(out_gate.astype(jnp.float32))).astype(jnp.bfloat16)
-    split_count = lax.axis_size("tp")
     expert_count = lax.axis_size(SP) * expert_gate.shape[0]
     rows = length // split_count
     first = lax.axis_index("tp") * rows
@@ -199,17 +278,27 @@
     def in_plane(x):
         return lax.all_to_all(x, PLANE, 0, 0, tiled=True)
 
-    arrived = along_z(send).transpose(1, 0, 2)
-    arrived = jnp.broadcast_to(arrived[:, None], (2, split_count, chips, width))
-    piece = in_plane(arrived.reshape(2 * split_count, chips, width)).reshape(-1, width)
-    gate_matrix, up_matrix, down_matrix = (expert_gate[0], expert_up[0], expert_down[0])
-    gate = jnp.dot(piece, gate_matrix, preferred_element_type=jnp.float32)
-    up = jnp.dot(piece, up_matrix, preferred_element_type=jnp.float32)
-    inner = (jax.nn.silu(gate) * up).astype(jnp.bfloat16)
-    partial_value = jnp.dot(inner, down_matrix, preferred_element_type=jnp.float32)
-    parts = in_plane(partial_value.astype(jnp.bfloat16).reshape(2 * split_count, chips, width))
-    parts = parts.reshape(2, split_count, chips, width)
-    result = jnp.sum(parts.astype(jnp.float32), axis=1).astype(jnp.bfloat16)
+    half = chips // 2
+    arrived = along_z(send).transpose(1, 0, 2).reshape(2, 2, half, width)
+    swapped = arrived[:, ::-1]
+    turns = jnp.stack([arrived, swapped], 1)[:, None, :, None]
+    turns = jnp.broadcast_to(turns, (2, side // 2, 2, side // 2, 2, half, width))
+    piece = in_plane(turns.reshape(2 * split_count, half, width)).reshape(-1, width)
+    tables = (gate_matrix, up_matrix, down_matrix, *thirds)
+    partial_value = pl.pallas_call(
+        run_experts,
+        out_shape=pltpu.VMEM(piece.shape, jnp.bfloat16),
+        in_specs=[vmem] + [pl.BlockSpec(memory_space=pl.ANY)] * 6,
+        out_specs=vmem,
+        scratch_shapes=[pltpu.VMEM(x.shape, x.dtype) for x in tables]
+        + [pltpu.SemaphoreType.DMA((6,))],
+        name="run_experts",
+    )(held(piece), *tables)
+    parts = in_plane(partial_value.reshape(2 * split_count, half, width))
+    parts = parts.reshape(2, side // 2, 2, side // 2, 2, half, width).astype(jnp.float32)
+    parts = jnp.sum(parts, axis=(1, 3))
+    result = jnp.stack([parts[:, 0, 0] + parts[:, 1, 1], parts[:, 0, 1] + parts[:, 1, 0]], 1)
+    result = result.reshape(2, chips, width).astype(jnp.bfloat16)
     back = along_z(result.transpose(1, 0, 2)).reshape(expert_count, width)
     gathered = jnp.einsum("rks,sd->rkd", table, back, preferred_element_type=jnp.float32)
     routed = jnp.sum(weights[..., None] * gathered, 1)
@@ -243,6 +332,5 @@
         P(SP, None, "tp"),
         P(SP, "tp", None),
     )
-    return jax.shard_map(
-        per_device, mesh=split, in_specs=placed, out_specs=P(SP, None), check_vma=False
-    )
+
+    return jax.shard_map(per_device, mesh=split, in_specs=placed, out_specs=P(SP, None), check_vma=False)

time: 203 us -> 352 us (1.73)
  Pallas kernels: 3.4 us -> 156 us
  blocking collectives: 118 us -> 52.7 us
  waiting for transfers between devices: 36.5 us -> 76.5 us
  starting transfers between devices: 19.8 us -> 49.2 us
  matrix products: 11.9 us -> 4.32 us
    pallas_call x1 -> x3, Pallas kernels: 3.4 us -> 156 us  [the longest x1 145 us: spread(): pl.pallas_call(pack_thirds, out_shape=(packed,) * 3, in_specs=[anywhere]...]
    all_to_all x2 -> x1, blocking collectives: 68.3 us -> 20.3 us  [in_plane(): return lax.all_to_all(x, PLANE, 0, 0, tiled=True)]
    ppermute x0 -> x3, waiting for transfers between devices: none -> 34.7 us  [spread(): out.append(lax.ppermute(third, 'tp', pairs))]
    all_to_all x1 -> x0, blocking collectives: 17.5 us -> none  [along_z(): out = lax.all_to_all(x.reshape(chips, 16, width // 8), Z, 0, 0, tiled=True)]
    all_to_all x1 -> x2, starting transfers between devices: 3.51 us -> 17.1 us  [along_z(): out = lax.all_to_all(x.reshape(chips, 16, width // 8), Z, 0, 0, tiled=True)]
    ppermute x0 -> x3, starting transfers between devices: none -> 8.42 us  [spread(): out.append(lax.ppermute(third, 'tp', pairs))]
    dot_general x2 -> x0, matrix products: 7.57 us -> none  [the longest x1 5.42 us: per_device(): jnp.dot(inner, down_matrix, preferred_element_type=jnp.float32)]
    all_to_all x1 -> x2, starting transfers between devices: 9.57 us -> 16.8 us  [the longest x1 9.57 us: entering(): far = lax.all_to_all(far, Z, 0, 0, tiled=True)]
  transfers between devices with their start and end apart: 3 -> 8, of which waited for: 3 -> 7; matrix products, arithmetic and copies ran while one was open for 0% -> 0% of each run, Pallas kernels for 0% -> 42%
where the time goes in v3:
time: 352 us; the launch traced here: 348 us
  Pallas kernels  156 us (44%)
  waiting for transfers between devices  76.5 us (22%)
  blocking collectives  52.7 us (15%)
  starting transfers between devices  49.2 us (14%)
  local copies, waits for them, and re-layouts  4.71 us (1%)
  matrix products  4.32 us (1%)
  other arithmetic  3.74 us (1%)
    pallas_call x1, Pallas kernels, spread(): pl.pallas_call(pack_thirds, out_shape=(packed,) * 3, in_specs=[anywhere]...  145 us
    ppermute x3, waiting for transfers between devices, spread(): out.append(lax.ppermute(third, 'tp', pairs))  34.7 us
    all_to_all x1, blocking collectives, in_plane(): return lax.all_to_all(x, PLANE, 0, 0, tiled=True)  20.3 us
    all_to_all x2, starting transfers between devices, along_z(): out = lax.all_to_all(x.reshape(chips, 16, width // 8), Z, 0, 0, tiled=True)  17.1 us
    all_to_all x1, waiting for transfers between devices, entering(): far = lax.all_to_all(far, Z, 0, 0, tiled=True)  14.1 us
    all_to_all x1, blocking collectives, copy_for_each(): lax.all_to_all(jnp.broadcast_to(x[None], (length, *x.shape)), axis, 0, 0,...  13.1 us
    all_gather x1, blocking collectives, entering(): near = lax.all_gather(own, ('zl', 'c')).astype(jnp.float32)  12.5 us
    all_to_all x2, waiting for transfers between devices, along_z(): out = lax.all_to_all(x.reshape(chips, 16, width // 8), Z, 0, 0, tiled=True)  11.9 us
  transfers between devices with their start and end apart: 8, of which 7 were waited for; matrix products, arithmetic and copies ran while one was open for 0% of the time, Pallas kernels for 42%

profile of v3, /device:TPU:1, one launch (start us, length us, event | category | flops | bytes accessed | tf_op | source)
XLA Modules:
  0.0 348.0 jit_solution(8276141538149250780)
XLA Ops:
  0.7 2.7 local_span.1
  3.4 12.5 %all-gather = bf16[1024,128]{1,0:T(8,128)(2,1)S(1)} all-gather(bf16[256,128]{1,0:T(8,128)(2,1)S(1)} %get-tuple-element.17), channel_id=2, replica_groups=mesh['zh'=8,'zl'=2,'c'=2,'tp'=16] {'zl','c'}, dimensions={0}, use_global_device_ids=true | all-gather | bytes 327680 | tf_op jit(solution)/shard_map/all_gather | solution.py:73
  17.1 0.8 broadcast_in_dim.6
  17.8 9.6 %all-to-all-start = ((bf16[16,64,128]{2,1,0:T(8,128)(2,1)}), bf16[16,64,128]{2,1,0:T(8,128)(2,1)S(1)}, u32[]{:S(2)}, u32[]{:S(2)}) async-start(bf16[16,64,128]{2,1,0:T(8,128)(2,1)} %broadcast_in_dim.6), calls=%async_computation | async-start | bytes 524288 | tf_op jit(solution)/shard_map/all_to_all | solution.py:90
  27.4 14.1 %all-to-all-done = bf16[16,64,128]{2,1,0:T(8,128)(2,1)S(1)} async-done(((bf16[16,64,128]{2,1,0:T(8,128)(2,1)}), bf16[16,64,128]{2,1,0:T(8,128)(2,1)S(1)}, u32[]{:S(2)}, u32[]{:S(2)}) %all-to-all-start) | async-done | bytes 262176 | tf_op jit(solution)/shard_map/all_to_all | solution.py:90
  41.5 6.8 %all-gather.1 = bf16[32,64,128]{2,1,0:T(8,128)(2,1)S(1)} all-gather(bf16[16,64,128]{2,1,0:T(8,128)(2,1)S(1)} %all-to-all-done), channel_id=3, replica_groups=mesh['zh'=8,'zl'=2,'c'=2,'tp'=16] {'c'}, dimensions={0}, use_global_device_ids=true | all-gather | bytes 786432 | tf_op jit(solution)/shard_map/all_gather | solution.py:91
  50.1 0.3 multiply_reduce_fusion.2
  50.4 1.1 fusion
  51.5 6.8 %all-to-all-start.1 = ((bf16[16,8,2048]{2,1,0:T(8,128)(2,1)}), bf16[16,8,2048]{2,1,0:T(8,128)(2,1)S(1)}, u32[]{:S(2)}, u32[]{:S(2)}) async-start(bf16[16,8,2048]{2,1,0:T(8,128)(2,1)} %fusion), calls=%async_computation.1 | async-start | bytes 1048576 | tf_op jit(solution)/shard_map/all_to_all | solution.py:108
  58.5 10.6 %all-to-all-done.1 = bf16[16,8,2048]{2,1,0:T(8,128)(2,1)S(1)} async-done(((bf16[16,8,2048]{2,1,0:T(8,128)(2,1)}), bf16[16,8,2048]{2,1,0:T(8,128)(2,1)S(1)}, u32[]{:S(2)}, u32[]{:S(2)}) %all-to-all-start.1) | async-done | bytes 524320 | tf_op jit(solution)/shard_map/all_to_all | solution.py:108
  69.1 0.9 fusion.40
  70.0 1.0 multiply_reduce_fusion.1
  71.0 0.8 multiply_convert_fusion.1
  72.0 0.7 reshape.122
  72.8 5.7 %all-to-all-start.2 = ((bf16[16,16,256]{2,1,0:T(8,128)(2,1)}), bf16[16,16,256]{2,1,0:T(8,128)(2,1)S(1)}, u32[]{:S(2)}, u32[]{:S(2)}) async-start(bf16[16,16,256]{2,1,0:T(8,128)(2,1)} %reshape.122), calls=%async_computation.2 | async-start | bytes 262144 | tf_op jit(solution)/shard_map/all_to_all | solution.py:275
  78.5 144.5 %pack_thirds.1 = (bf16[2048,384]{1,0:T(8,128)(2,1)}, bf16[2048,384]{1,0:T(8,128)(2,1)}, bf16[2048,384]{1,0:T(8,128)(2,1)}) custom-call(bf16[2048,384]{1,0:T(8,128)(2,1)} %bitcast.161, bf16[2048,384]{1,0:T(8,128)(2,1)} %bitcast.163, bf16[384,2048]{1,0:T(8,128)(2,1)} %bitcast.165), custom_call_target="tpu_custom_call" | custom-call | tf_op jit(solution)/shard_map/pack_thirds/pallas_call | solution.py:51
  223.0 2.2 collective-permute-start
  225.2 4.3 %collective-permute-start.1 = (bf16[2048,384]{1,0:T(8,128)(2,1)}, bf16[2048,384]{1,0:T(8,128)(2,1)}, u32[]{:S(2)}, u32[]{:S(2)}) collective-permute-start(bf16[2048,384]{1,0:T(8,128)(2,1)} %get-tuple-element.23), channel_id=1, source_target_pairs={{0,3},{1,0},{2,1},{3,2},{4,7},{5,4},{6,5},{7,6},{8,11},{9,8},{10,9... | collective-permute-start | bytes 4718600 | tf_op jit(solution)/shard_map/ppermute | solution.py:66
  229.5 1.9 collective-permute-start.2
  231.6 1.1 broadcast_in_dim.7
  232.7 7.3 %all-to-all-start.3 = ((bf16[32,8,2048]{2,1,0:T(8,128)(2,1)}), bf16[32,8,2048]{2,1,0:T(8,128)(2,1)S(1)}, u32[]{:S(2)}, u32[]{:S(2)}) async-start(bf16[32,8,2048]{2,1,0:T(8,128)(2,1)} %bitcast.36), calls=%async_computation.3 | async-start | bytes 2097152 | tf_op jit(solution)/shard_map/all_to_all | solution.py:279
  240.0 20.7 %collective-permute-done.refs_3_ = bf16[2048,384]{1,0:T(8,128)(2,1)} collective-permute-done((bf16[2048,384]{1,0:T(8,128)(2,1)}, bf16[2048,384]{1,0:T(8,128)(2,1)}, u32[]{:S(2)}, u32[]{:S(2)}) %collective-permute-start) | collective-permute-done | bytes 1572896 | tf_op jit(solution)/shard_map/ppermute | solution.py:66
  260.7 0.6 collective-permute-done.1.refs_4_
  261.2 13.5 %collective-permute-done.2.refs_5_ = bf16[2048,384]{1,0:T(8,128)(2,1)} collective-permute-done((bf16[2048,384]{1,0:T(8,128)(2,1)}, bf16[2048,384]{1,0:T(8,128)(2,1)}, u32[]{:S(2)}, u32[]{:S(2)}) %collective-permute-start.2) | collective-permute-done | bytes 1572896 | tf_op jit(solution)/shard_map/ppermute | solution.py:66
  274.7 5.2 %all-to-all-done.3 = bf16[32,8,2048]{2,1,0:T(8,128)(2,1)S(1)} async-done(((bf16[32,8,2048]{2,1,0:T(8,128)(2,1)}), bf16[32,8,2048]{2,1,0:T(8,128)(2,1)S(1)}, u32[]{:S(2)}, u32[]{:S(2)}) %all-to-all-start.3) | async-done | bytes 1048608 | tf_op jit(solution)/shard_map/all_to_all | solution.py:279
  279.9 8.5 %run_experts.1 = bf16[256,2048]{1,0:T(8,128)(2,1)S(1)} custom-call(bf16[256,2048]{1,0:T(8,128)(2,1)S(1)} %bitcast.159, bf16[2048,384]{1,0:T(8,128)(2,1)} %bitcast.162, bf16[2048,384]{1,0:T(8,128)(2,1)} %bitcast.164, bf16[384,2048]{1,0:T(8,128)(2,1)} %bitcast.166, bf16[2048,384]{1,0:T(8,128)(2,1)} %collective-permute-done.refs_3_, ...), custom_call_target="tpu_custom_call" | custom-call | tf_op jit(solution)/shard_map/run_experts/pallas_call | solution.py:288
  288.4 20.3 %all_to_all.35 = bf16[32,8,2048]{2,1,0:T(8,128)(2,1)S(1)} all-to-all(bf16[32,8,2048]{2,1,0:T(8,128)(2,1)S(1)} %bitcast.160), channel_id=1, replica_groups=mesh['zh'=8,'zl'=2,'c'=2,'tp'=16] {'c','tp'}, dimensions={0} | all-to-all | bytes 2097152 | tf_op jit(solution)/shard_map/all_to_all | solution.py:279
  309.1 0.7 reshape.128
  309.8 11.5 %all-to-all-start.5 = ((bf16[16,16,256]{2,1,0:T(8,128)(2,1)}), bf16[16,16,256]{2,1,0:T(8,128)(2,1)S(1)}, u32[]{:S(2)}, u32[]{:S(2)}) async-start(bf16[16,16,256]{2,1,0:T(8,128)(2,1)} %reshape.128), calls=%async_computation.5 | async-start | bytes 262144 | tf_op jit(solution)/shard_map/all_to_all | solution.py:275
  321.4 11.9 %all-to-all-done.5 = bf16[16,16,256]{2,1,0:T(8,128)(2,1)S(1)} async-done(((bf16[16,16,256]{2,1,0:T(8,128)(2,1)}), bf16[16,16,256]{2,1,0:T(8,128)(2,1)S(1)}, u32[]{:S(2)}, u32[]{:S(2)}) %all-to-all-start.5) | async-done | bytes 131104 | tf_op jit(solution)/shard_map/all_to_all | solution.py:275
  334.1 13.1 %all_to_all.36 = bf16[16,8,2048]{2,1,0:T(8,128)(2,1)S(1)} all-to-all(bf16[16,8,2048]{2,1,0:T(8,128)(2,1)S(1)} %broadcast_in_dim.8), channel_id=1, replica_groups=mesh['zh'=8,'zl'=2,'c'=2,'tp'=16] {'tp'}, dimensions={0} | all-to-all | bytes 1048576 | tf_op jit(solution)/shard_map/all_to_all | solution.py:114
  347.2 0.8 copy.52
  (59 shorter events, 4.5 us)
Async XLA Ops:
  0.0 50.4 %copy-start = (bf16[128,2048]{1,0:T(8,128)(2,1)S(1)}, bf16[128,2048]{1,0:T(8,128)(2,1)}, u32[]{:S(2)}) copy-start(bf16[128,2048]{1,0:T(8,128)(2,1)} %param.26) | copy-start | bytes 1572868
  17.8 23.7 %all-to-all-start = ((bf16[16,64,128]{2,1,0:T(8,128)(2,1)}), bf16[16,64,128]{2,1,0:T(8,128)(2,1)S(1)}, u32[]{:S(2)}, u32[]{:S(2)}) async-start(bf16[16,64,128]{2,1,0:T(8,128)(2,1)} %broadcast_in_dim.6), calls=%async_computation | async-start | bytes 524288 | tf_op jit(solution)/shard_map/all_to_all | solution.py:90
  48.4 2.0 copy-start.1
  48.4 2.0 copy-start.6
  49.6 8.7 %copy-start.4 = (s32[128,2]{0,1:T(2,128)S(1)}, s32[128,2]{0,1:T(2,128)}, u32[]{:S(2)}) copy-start(s32[128,2]{0,1:T(2,128)} %param.29) | copy-start | bytes 3076
  50.0 20.9 %copy-start.2 = (f32[2048]{0:T(1024)S(1)}, f32[2048]{0:T(1024)}, u32[]{:S(2)}) copy-start(f32[2048]{0:T(1024)} %param.27) | copy-start | bytes 24580
  51.5 17.5 %all-to-all-start.1 = ((bf16[16,8,2048]{2,1,0:T(8,128)(2,1)}), bf16[16,8,2048]{2,1,0:T(8,128)(2,1)S(1)}, u32[]{:S(2)}, u32[]{:S(2)}) async-start(bf16[16,8,2048]{2,1,0:T(8,128)(2,1)} %fusion), calls=%async_computation.1 | async-start | bytes 1048576 | tf_op jit(solution)/shard_map/all_to_all | solution.py:108
  72.8 158.7 %all-to-all-start.2 = ((bf16[16,16,256]{2,1,0:T(8,128)(2,1)}), bf16[16,16,256]{2,1,0:T(8,128)(2,1)S(1)}, u32[]{:S(2)}, u32[]{:S(2)}) async-start(bf16[16,16,256]{2,1,0:T(8,128)(2,1)} %reshape.122), calls=%async_computation.2 | async-start | bytes 262144 | tf_op jit(solution)/shard_map/all_to_all | solution.py:275
  223.0 37.7 %collective-permute-start = (bf16[2048,384]{1,0:T(8,128)(2,1)}, bf16[2048,384]{1,0:T(8,128)(2,1)}, u32[]{:S(2)}, u32[]{:S(2)}) collective-permute-start(bf16[2048,384]{1,0:T(8,128)(2,1)} %get-tuple-element.22), channel_id=1, source_target_pairs={{0,1},{1,2},{2,3},{3,0},{4,5},{5,6},{6,7},{7,4},{8,9},{9,10},{10,1... | collective-permute-start | bytes 4718600 | tf_op jit(solution)/shard_map/ppermute | solution.py:66
  225.2 36.0 %collective-permute-start.1 = (bf16[2048,384]{1,0:T(8,128)(2,1)}, bf16[2048,384]{1,0:T(8,128)(2,1)}, u32[]{:S(2)}, u32[]{:S(2)}) collective-permute-start(bf16[2048,384]{1,0:T(8,128)(2,1)} %get-tuple-element.23), channel_id=1, source_target_pairs={{0,3},{1,0},{2,1},{3,2},{4,7},{5,4},{6,5},{7,6},{8,11},{9,8},{10,9... | collective-permute-start | bytes 4718600 | tf_op jit(solution)/shard_map/ppermute | solution.py:66
  229.5 45.2 %collective-permute-start.2 = (bf16[2048,384]{1,0:T(8,128)(2,1)}, bf16[2048,384]{1,0:T(8,128)(2,1)}, u32[]{:S(2)}, u32[]{:S(2)}) collective-permute-start(bf16[2048,384]{1,0:T(8,128)(2,1)} %get-tuple-element.24), channel_id=1, source_target_pairs={{0,4},{1,5},{2,6},{3,7},{4,8},{5,9},{6,10},{7,11},{8,12},{9,13},{1... | collective-permute-start | bytes 4718600 | tf_op jit(solution)/shard_map/ppermute | solution.py:66
  232.7 47.1 %all-to-all-start.3 = ((bf16[32,8,2048]{2,1,0:T(8,128)(2,1)}), bf16[32,8,2048]{2,1,0:T(8,128)(2,1)S(1)}, u32[]{:S(2)}, u32[]{:S(2)}) async-start(bf16[32,8,2048]{2,1,0:T(8,128)(2,1)} %bitcast.36), calls=%async_computation.3 | async-start | bytes 2097152 | tf_op jit(solution)/shard_map/all_to_all | solution.py:279
  308.7 12.6 %copy-start.5 = (f32[128,2]{0,1:T(2,128)S(1)}, f32[128,2]{0,1:T(2,128)}, u32[]{:S(2)}) copy-start(f32[128,2]{0,1:T(2,128)} %param.30) | copy-start | bytes 3076
  308.9 25.1 %copy-start.3 = (f32[2048]{0:T(1024)S(1)}, f32[2048]{0:T(1024)}, u32[]{:S(2)}) copy-start(f32[2048]{0:T(1024)} %param.28) | copy-start | bytes 24580
  309.8 23.5 %all-to-all-start.5 = ((bf16[16,16,256]{2,1,0:T(8,128)(2,1)}), bf16[16,16,256]{2,1,0:T(8,128)(2,1)S(1)}, u32[]{:S(2)}, u32[]{:S(2)}) async-start(bf16[16,16,256]{2,1,0:T(8,128)(2,1)} %reshape.128), calls=%async_computation.5 | async-start | bytes 262144 | tf_op jit(solution)/shard_map/all_to_all | solution.py:275

commit v4 on v3

--- a/solution.py
+++ b/solution.py
@@ -25,35 +25,36 @@
     return jnp.dot(a, b, precision=highest_precision)
 
 
-def pack_thirds(gate_ref, up_ref, down_ref, first_ref, second_ref, third_ref, sems):
-    share = down_ref.shape[0] // 3
-    copies = []
-    for part, ref in enumerate((first_ref, second_ref, third_ref)):
-        cut = pl.ds(part * share, share)
-        moves = [(gate_ref.at[:, cut], ref.at[:, pl.ds(0, share)])]
-        moves.append((up_ref.at[:, cut], ref.at[:, pl.ds(share, share)]))
-        for k in range(0, ref.shape[0], share):
-            source = down_ref.at[cut, pl.ds(k, share)]
-            moves.append((source, ref.at[pl.ds(k, share), pl.ds(2 * share, share)]))
-        copies += moves
-    copies = [pltpu.make_async_copy(x, y, sems.at[k]) for k, (x, y) in enumerate(copies)]
+def pack_thirds(gate_ref, up_ref, down_ref, *refs):
+    outs, bufs, sems = refs[:3], refs[3:6], refs[6]
+    copies = [
+        pltpu.make_async_copy(x, y, sems.at[k])
+        for k, (x, y) in enumerate(zip((gate_ref, up_ref, down_ref), bufs))
+    ]
     for copy in copies:
         copy.start()
-    for copy in copies:
+    share = down_ref.shape[0] // 3
+    for kind, (copy, buf) in enumerate(zip(copies, bufs)):
         copy.wait()
+        for part, out in enumerate(outs):
+            cut = slice(part * share, (part + 1) * share)
+            rows = slice(kind * share, (kind + 1) * share)
+            if kind == 2:
+                out[rows] = buf[cut]
+            else:
+                for k in range(0, buf.shape[0], share):
+                    out[rows, k : k + share] = buf[k : k + share, cut]
 
 
 def spread(gate, up, down, side):
-    width, share = gate.shape
-    share //= 3
-    packed = jax.ShapeDtypeStruct((width, 3 * share), gate.dtype)
-    anywhere = pl.BlockSpec(memory_space=pl.ANY)
+    packed = jax.ShapeDtypeStruct(down.shape, down.dtype)
     thirds = pl.pallas_call(
         pack_thirds,
         out_shape=(packed,) * 3,
-        in_specs=[anywhere] * 3,
-        out_specs=(anywhere,) * 3,
-        scratch_shapes=[pltpu.SemaphoreType.DMA((3 * (2 + width // share),))],
+        in_specs=[pl.BlockSpec(memory_space=pl.ANY)] * 3,
+        out_specs=(pl.BlockSpec(memory_space=pltpu.VMEM),) * 3,
+        scratch_shapes=[pltpu.VMEM(x.shape, x.dtype) for x in (gate, up, down)]
+        + [pltpu.SemaphoreType.DMA((3,))],
         name="pack_thirds",
     )(gate, up, down)
     out = []
@@ -193,7 +194,8 @@
         copy.start()
     gate_ref, up_ref, down_ref = bufs[:3]
     rows = rows_ref[...]
-    share = bufs[3].shape[1] // 3
+    share = down_ref.shape[0] // 3
+    width = rows.shape[1]
 
     def dot(a, b):
         return jnp.dot(a, b, preferred_element_type=jnp.float32)
@@ -201,16 +203,22 @@
     copies[0].wait()
     gate = dot(rows, gate_ref[...])
     copies[1].wait()
-    inner = (jax.nn.silu(gate) * dot(rows, up_ref[...])).astype(jnp.bfloat16)
-    copies[2].wait()
-    total = dot(inner, down_ref[...])
+    inners = [(jax.nn.silu(gate) * dot(rows, up_ref[...])).astype(jnp.bfloat16)]
     for copy, ref in zip(copies[3:], bufs[3:]):
         copy.wait()
-        both = dot(rows, ref[:, : 2 * share])
-        inner = (jax.nn.silu(both[:, :share]) * both[:, share:]).astype(jnp.bfloat16)
-        down = [ref[k : k + share, 2 * share :] for k in range(0, ref.shape[0], share)]
-        total = total + dot(inner, jnp.concatenate(down, 1))
-    out_ref[...] = total.astype(out_ref.dtype)
+        both = [
+            jnp.concatenate([ref[:share, k : k + share], ref[share : 2 * share, k : k + share]], 1)
+            for k in range(0, width, share)
+        ]
+        both = dot(rows, jnp.concatenate(both, 0))
+        inners.append((jax.nn.silu(both[:, :share]) * both[:, share:]).astype(jnp.bfloat16))
+    copies[2].wait()
+    step = 2 * share
+    for k in range(0, width, step):
+        total = dot(inners[0], down_ref[:, k : k + step])
+        for inner, ref in zip(inners[1:], bufs[3:]):
+            total = total + dot(inner, ref[2 * share :, k : k + step])
+        out_ref[:, k : k + step] = total.astype(out_ref.dtype)
 
 
 def per_device(

time: 352 us -> 211 us (0.60)
  Pallas kernels: 156 us -> 14.3 us
    pallas_call x1, Pallas kernels: 145 us -> 4.67 us  [spread(): pl.pallas_call(pack_thirds, out_shape=(packed,) * 3, in_specs=[pl.BlockSp...]
  transfers between devices with their start and end apart: 8 -> 8, of which waited for: 7 -> 7; matrix products, arithmetic and copies ran while one was open for 0% -> 1% of each run, Pallas kernels for 42% -> 2%
where the time goes in v4:
time: 211 us; the launch traced here: 207 us
  waiting for transfers between devices  76.5 us (36%)
  blocking collectives  52.7 us (25%)
  starting transfers between devices  49.2 us (23%)
  Pallas kernels  14.3 us (7%)
  local copies, waits for them, and re-layouts  4.71 us (2%)
  matrix products  4.32 us (2%)
  other arithmetic  3.74 us (2%)
    ppermute x3, waiting for transfers between devices, spread(): out.append(lax.ppermute(third, 'tp', pairs))  34.7 us
    all_to_all x1, blocking collectives, in_plane(): return lax.all_to_all(x, PLANE, 0, 0, tiled=True)  20.3 us
    all_to_all x2, starting transfers between devices, along_z(): out = lax.all_to_all(x.reshape(chips, 16, width // 8), Z, 0, 0, tiled=True)  17.1 us
    all_to_all x1, waiting for transfers between devices, entering(): far = lax.all_to_all(far, Z, 0, 0, tiled=True)  14.1 us
    all_to_all x1, blocking collectives, copy_for_each(): lax.all_to_all(jnp.broadcast_to(x[None], (length, *x.shape)), axis, 0, 0,...  13.1 us
    all_gather x1, blocking collectives, entering(): near = lax.all_gather(own, ('zl', 'c')).astype(jnp.float32)  12.5 us
    all_to_all x2, waiting for transfers between devices, along_z(): out = lax.all_to_all(x.reshape(chips, 16, width // 8), Z, 0, 0, tiled=True)  11.9 us
    all_to_all x1, waiting for transfers between devices, sum_at_owner(): blocks = lax.all_to_all(in_blocks(x, dim, length), axis, 0, 0, tiled=True)  10.6 us
  transfers between devices with their start and end apart: 8, of which 7 were waited for; matrix products, arithmetic and copies ran while one was open for 1% of the time, Pallas kernels for 2%

profile of v4, /device:TPU:1, one launch (start us, length us, event | category | flops | bytes accessed | tf_op | source)
XLA Modules:
  0.0 206.5 jit_solution(9878841247999306506)
XLA Ops:
  0.7 2.7 %local_span.1 = (bf16[256,128]{1,0:T(8,128)(2,1)S(1)}, f32[128,128]{1,0:T(8,128)S(1)}, f32[128,128]{1,0:T(8,128)S(1)}) custom-call(bf16[128,128]{1,0:T(8,128)(2,1)} %q_ref.1, bf16[128,128]{1,0:T(8,128)(2,1)} %k_ref.1, bf16[128,128]{1,0:T(8,128)(2,1)} %v_ref.1, bf16[1,128]{1,0:T(2,128)(2,1)} %beta_ref.1, bf16[1,128]{1,0:T(2,128)(2,1)} %decay_ref.1, ...), custom_call_target="tpu_custom_call" | custom-call | tf_op jit(solution)/shard_map/local_span/pallas_call | solution.py:246
  3.4 12.5 %all-gather = bf16[1024,128]{1,0:T(8,128)(2,1)S(1)} all-gather(bf16[256,128]{1,0:T(8,128)(2,1)S(1)} %get-tuple-element.17), channel_id=2, replica_groups=mesh['zh'=8,'zl'=2,'c'=2,'tp'=16] {'zl','c'}, dimensions={0}, use_global_device_ids=true | all-gather | bytes 327680 | tf_op jit(solution)/shard_map/all_gather | solution.py:74
  17.1 0.8 broadcast_in_dim.6
  17.8 9.6 %all-to-all-start = ((bf16[16,64,128]{2,1,0:T(8,128)(2,1)}), bf16[16,64,128]{2,1,0:T(8,128)(2,1)S(1)}, u32[]{:S(2)}, u32[]{:S(2)}) async-start(bf16[16,64,128]{2,1,0:T(8,128)(2,1)} %broadcast_in_dim.6), calls=%async_computation | async-start | bytes 524288 | tf_op jit(solution)/shard_map/all_to_all | solution.py:91
  27.4 14.1 %all-to-all-done = bf16[16,64,128]{2,1,0:T(8,128)(2,1)S(1)} async-done(((bf16[16,64,128]{2,1,0:T(8,128)(2,1)}), bf16[16,64,128]{2,1,0:T(8,128)(2,1)S(1)}, u32[]{:S(2)}, u32[]{:S(2)}) %all-to-all-start) | async-done | bytes 262176 | tf_op jit(solution)/shard_map/all_to_all | solution.py:91
  41.5 6.8 %all-gather.1 = bf16[32,64,128]{2,1,0:T(8,128)(2,1)S(1)} all-gather(bf16[16,64,128]{2,1,0:T(8,128)(2,1)S(1)} %all-to-all-done), channel_id=3, replica_groups=mesh['zh'=8,'zl'=2,'c'=2,'tp'=16] {'c'}, dimensions={0}, use_global_device_ids=true | all-gather | bytes 786432 | tf_op jit(solution)/shard_map/all_gather | solution.py:92
  50.1 0.3 multiply_reduce_fusion.2
  50.4 1.1 fusion
  51.5 6.8 %all-to-all-start.1 = ((bf16[16,8,2048]{2,1,0:T(8,128)(2,1)}), bf16[16,8,2048]{2,1,0:T(8,128)(2,1)S(1)}, u32[]{:S(2)}, u32[]{:S(2)}) async-start(bf16[16,8,2048]{2,1,0:T(8,128)(2,1)} %fusion), calls=%async_computation.1 | async-start | bytes 1048576 | tf_op jit(solution)/shard_map/all_to_all | solution.py:109
  58.5 10.6 %all-to-all-done.1 = bf16[16,8,2048]{2,1,0:T(8,128)(2,1)S(1)} async-done(((bf16[16,8,2048]{2,1,0:T(8,128)(2,1)}), bf16[16,8,2048]{2,1,0:T(8,128)(2,1)S(1)}, u32[]{:S(2)}, u32[]{:S(2)}) %all-to-all-start.1) | async-done | bytes 524320 | tf_op jit(solution)/shard_map/all_to_all | solution.py:109
  69.1 0.9 fusion.40
  70.0 1.0 multiply_reduce_fusion.1
  71.0 0.8 multiply_convert_fusion.1
  72.0 0.7 reshape.122
  72.8 5.7 %all-to-all-start.2 = ((bf16[16,16,256]{2,1,0:T(8,128)(2,1)}), bf16[16,16,256]{2,1,0:T(8,128)(2,1)S(1)}, u32[]{:S(2)}, u32[]{:S(2)}) async-start(bf16[16,16,256]{2,1,0:T(8,128)(2,1)} %reshape.122), calls=%async_computation.2 | async-start | bytes 262144 | tf_op jit(solution)/shard_map/all_to_all | solution.py:283
  78.5 4.7 %pack_thirds.1 = (bf16[384,2048]{1,0:T(8,128)(2,1)}, bf16[384,2048]{1,0:T(8,128)(2,1)}, bf16[384,2048]{1,0:T(8,128)(2,1)}) custom-call(bf16[2048,384]{1,0:T(8,128)(2,1)} %bitcast.161, bf16[2048,384]{1,0:T(8,128)(2,1)} %bitcast.163, bf16[384,2048]{1,0:T(8,128)(2,1)} %bitcast.165), custom_call_target="tpu_custom_call" | custom-call | tf_op jit(solution)/shard_map/pack_thirds/pallas_call | solution.py:51
  83.2 2.2 %collective-permute-start = (bf16[384,2048]{1,0:T(8,128)(2,1)}, bf16[384,2048]{1,0:T(8,128)(2,1)}, u32[]{:S(2)}, u32[]{:S(2)}) collective-permute-start(bf16[384,2048]{1,0:T(8,128)(2,1)} %get-tuple-element.22), channel_id=1, source_target_pairs={{0,1},{1,2},{2,3},{3,0},{4,5},{5,6},{6,7},{7,4},{8,9},{9,10},{10,1... | collective-permute-start | bytes 4718600 | tf_op jit(solution)/shard_map/ppermute | solution.py:67
  85.4 4.3 %collective-permute-start.1 = (bf16[384,2048]{1,0:T(8,128)(2,1)}, bf16[384,2048]{1,0:T(8,128)(2,1)}, u32[]{:S(2)}, u32[]{:S(2)}) collective-permute-start(bf16[384,2048]{1,0:T(8,128)(2,1)} %get-tuple-element.23), channel_id=1, source_target_pairs={{0,3},{1,0},{2,1},{3,2},{4,7},{5,4},{6,5},{7,6},{8,11},{9,8},{10,9... | collective-permute-start | bytes 4718600 | tf_op jit(solution)/shard_map/ppermute | solution.py:67
  89.7 1.9 collective-permute-start.2
  91.8 1.1 broadcast_in_dim.7
  92.9 7.3 %all-to-all-start.3 = ((bf16[32,8,2048]{2,1,0:T(8,128)(2,1)}), bf16[32,8,2048]{2,1,0:T(8,128)(2,1)S(1)}, u32[]{:S(2)}, u32[]{:S(2)}) async-start(bf16[32,8,2048]{2,1,0:T(8,128)(2,1)} %bitcast.36), calls=%async_computation.3 | async-start | bytes 2097152 | tf_op jit(solution)/shard_map/all_to_all | solution.py:287
  100.2 20.7 %collective-permute-done.refs_3_ = bf16[384,2048]{1,0:T(8,128)(2,1)} collective-permute-done((bf16[384,2048]{1,0:T(8,128)(2,1)}, bf16[384,2048]{1,0:T(8,128)(2,1)}, u32[]{:S(2)}, u32[]{:S(2)}) %collective-permute-start) | collective-permute-done | bytes 1572896 | tf_op jit(solution)/shard_map/ppermute | solution.py:67
  120.8 0.6 collective-permute-done.1.refs_4_
  121.4 13.5 %collective-permute-done.2.refs_5_ = bf16[384,2048]{1,0:T(8,128)(2,1)} collective-permute-done((bf16[384,2048]{1,0:T(8,128)(2,1)}, bf16[384,2048]{1,0:T(8,128)(2,1)}, u32[]{:S(2)}, u32[]{:S(2)}) %collective-permute-start.2) | collective-permute-done | bytes 1572896 | tf_op jit(solution)/shard_map/ppermute | solution.py:67
  134.9 5.2 %all-to-all-done.3 = bf16[32,8,2048]{2,1,0:T(8,128)(2,1)S(1)} async-done(((bf16[32,8,2048]{2,1,0:T(8,128)(2,1)}), bf16[32,8,2048]{2,1,0:T(8,128)(2,1)S(1)}, u32[]{:S(2)}, u32[]{:S(2)}) %all-to-all-start.3) | async-done | bytes 1048608 | tf_op jit(solution)/shard_map/all_to_all | solution.py:287
  140.0 6.9 %run_experts.1 = bf16[256,2048]{1,0:T(8,128)(2,1)S(1)} custom-call(bf16[256,2048]{1,0:T(8,128)(2,1)S(1)} %bitcast.159, bf16[2048,384]{1,0:T(8,128)(2,1)} %bitcast.162, bf16[2048,384]{1,0:T(8,128)(2,1)} %bitcast.164, bf16[384,2048]{1,0:T(8,128)(2,1)} %bitcast.166, bf16[384,2048]{1,0:T(8,128)(2,1)} %collective-permute-done.refs_3_, ...), custom_call_target="tpu_custom_call" | custom-call | tf_op jit(solution)/shard_map/run_experts/pallas_call | solution.py:296
  146.9 20.3 %all_to_all.35 = bf16[32,8,2048]{2,1,0:T(8,128)(2,1)S(1)} all-to-all(bf16[32,8,2048]{2,1,0:T(8,128)(2,1)S(1)} %bitcast.160), channel_id=1, replica_groups=mesh['zh'=8,'zl'=2,'c'=2,'tp'=16] {'c','tp'}, dimensions={0} | all-to-all | bytes 2097152 | tf_op jit(solution)/shard_map/all_to_all | solution.py:287
  167.6 0.7 reshape.128
  168.4 11.5 %all-to-all-start.5 = ((bf16[16,16,256]{2,1,0:T(8,128)(2,1)}), bf16[16,16,256]{2,1,0:T(8,128)(2,1)S(1)}, u32[]{:S(2)}, u32[]{:S(2)}) async-start(bf16[16,16,256]{2,1,0:T(8,128)(2,1)} %reshape.128), calls=%async_computation.5 | async-start | bytes 262144 | tf_op jit(solution)/shard_map/all_to_all | solution.py:283
  179.9 11.9 %all-to-all-done.5 = bf16[16,16,256]{2,1,0:T(8,128)(2,1)S(1)} async-done(((bf16[16,16,256]{2,1,0:T(8,128)(2,1)}), bf16[16,16,256]{2,1,0:T(8,128)(2,1)S(1)}, u32[]{:S(2)}, u32[]{:S(2)}) %all-to-all-start.5) | async-done | bytes 131104 | tf_op jit(solution)/shard_map/all_to_all | solution.py:283
  192.6 13.1 %all_to_all.36 = bf16[16,8,2048]{2,1,0:T(8,128)(2,1)S(1)} all-to-all(bf16[16,8,2048]{2,1,0:T(8,128)(2,1)S(1)} %broadcast_in_dim.8), channel_id=1, replica_groups=mesh['zh'=8,'zl'=2,'c'=2,'tp'=16] {'tp'}, dimensions={0} | all-to-all | bytes 1048576 | tf_op jit(solution)/shard_map/all_to_all | solution.py:115
  205.8 0.8 copy.52
  (59 shorter events, 4.5 us)
Async XLA Ops:
  0.0 50.4 %copy-start = (bf16[128,2048]{1,0:T(8,128)(2,1)S(1)}, bf16[128,2048]{1,0:T(8,128)(2,1)}, u32[]{:S(2)}) copy-start(bf16[128,2048]{1,0:T(8,128)(2,1)} %param.26) | copy-start | bytes 1572868
  17.8 23.7 %all-to-all-start = ((bf16[16,64,128]{2,1,0:T(8,128)(2,1)}), bf16[16,64,128]{2,1,0:T(8,128)(2,1)S(1)}, u32[]{:S(2)}, u32[]{:S(2)}) async-start(bf16[16,64,128]{2,1,0:T(8,128)(2,1)} %broadcast_in_dim.6), calls=%async_computation | async-start | bytes 524288 | tf_op jit(solution)/shard_map/all_to_all | solution.py:91
  48.4 2.0 copy-start.1
  48.4 2.0 copy-start.6
  49.6 8.7 %copy-start.4 = (s32[128,2]{0,1:T(2,128)S(1)}, s32[128,2]{0,1:T(2,128)}, u32[]{:S(2)}) copy-start(s32[128,2]{0,1:T(2,128)} %param.29) | copy-start | bytes 3076
  50.0 20.9 %copy-start.2 = (f32[2048]{0:T(1024)S(1)}, f32[2048]{0:T(1024)}, u32[]{:S(2)}) copy-start(f32[2048]{0:T(1024)} %param.27) | copy-start | bytes 24580
  51.5 17.5 %all-to-all-start.1 = ((bf16[16,8,2048]{2,1,0:T(8,128)(2,1)}), bf16[16,8,2048]{2,1,0:T(8,128)(2,1)S(1)}, u32[]{:S(2)}, u32[]{:S(2)}) async-start(bf16[16,8,2048]{2,1,0:T(8,128)(2,1)} %fusion), calls=%async_computation.1 | async-start | bytes 1048576 | tf_op jit(solution)/shard_map/all_to_all | solution.py:109
  72.8 18.8 %all-to-all-start.2 = ((bf16[16,16,256]{2,1,0:T(8,128)(2,1)}), bf16[16,16,256]{2,1,0:T(8,128)(2,1)S(1)}, u32[]{:S(2)}, u32[]{:S(2)}) async-start(bf16[16,16,256]{2,1,0:T(8,128)(2,1)} %reshape.122), calls=%async_computation.2 | async-start | bytes 262144 | tf_op jit(solution)/shard_map/all_to_all | solution.py:283
  83.2 37.7 %collective-permute-start = (bf16[384,2048]{1,0:T(8,128)(2,1)}, bf16[384,2048]{1,0:T(8,128)(2,1)}, u32[]{:S(2)}, u32[]{:S(2)}) collective-permute-start(bf16[384,2048]{1,0:T(8,128)(2,1)} %get-tuple-element.22), channel_id=1, source_target_pairs={{0,1},{1,2},{2,3},{3,0},{4,5},{5,6},{6,7},{7,4},{8,9},{9,10},{10,1... | collective-permute-start | bytes 4718600 | tf_op jit(solution)/shard_map/ppermute | solution.py:67
  85.4 36.0 %collective-permute-start.1 = (bf16[384,2048]{1,0:T(8,128)(2,1)}, bf16[384,2048]{1,0:T(8,128)(2,1)}, u32[]{:S(2)}, u32[]{:S(2)}) collective-permute-start(bf16[384,2048]{1,0:T(8,128)(2,1)} %get-tuple-element.23), channel_id=1, source_target_pairs={{0,3},{1,0},{2,1},{3,2},{4,7},{5,4},{6,5},{7,6},{8,11},{9,8},{10,9... | collective-permute-start | bytes 4718600 | tf_op jit(solution)/shard_map/ppermute | solution.py:67
  89.7 45.2 %collective-permute-start.2 = (bf16[384,2048]{1,0:T(8,128)(2,1)}, bf16[384,2048]{1,0:T(8,128)(2,1)}, u32[]{:S(2)}, u32[]{:S(2)}) collective-permute-start(bf16[384,2048]{1,0:T(8,128)(2,1)} %get-tuple-element.24), channel_id=1, source_target_pairs={{0,4},{1,5},{2,6},{3,7},{4,8},{5,9},{6,10},{7,11},{8,12},{9,13},{1... | collective-permute-start | bytes 4718600 | tf_op jit(solution)/shard_map/ppermute | solution.py:67
  92.9 47.1 %all-to-all-start.3 = ((bf16[32,8,2048]{2,1,0:T(8,128)(2,1)}), bf16[32,8,2048]{2,1,0:T(8,128)(2,1)S(1)}, u32[]{:S(2)}, u32[]{:S(2)}) async-start(bf16[32,8,2048]{2,1,0:T(8,128)(2,1)} %bitcast.36), calls=%async_computation.3 | async-start | bytes 2097152 | tf_op jit(solution)/shard_map/all_to_all | solution.py:287
  167.3 12.6 %copy-start.5 = (f32[128,2]{0,1:T(2,128)S(1)}, f32[128,2]{0,1:T(2,128)}, u32[]{:S(2)}) copy-start(f32[128,2]{0,1:T(2,128)} %param.30) | copy-start | bytes 3076
  167.4 25.1 %copy-start.3 = (f32[2048]{0:T(1024)S(1)}, f32[2048]{0:T(1024)}, u32[]{:S(2)}) copy-start(f32[2048]{0:T(1024)} %param.28) | copy-start | bytes 24580
  168.4 23.5 %all-to-all-start.5 = ((bf16[16,16,256]{2,1,0:T(8,128)(2,1)}), bf16[16,16,256]{2,1,0:T(8,128)(2,1)S(1)}, u32[]{:S(2)}, u32[]{:S(2)}) async-start(bf16[16,16,256]{2,1,0:T(8,128)(2,1)} %reshape.128), calls=%async_computation.5 | async-start | bytes 262144 | tf_op jit(solution)/shard_map/all_to_all | solution.py:283

commit v5 on v3

--- a/solution.py
+++ b/solution.py
@@ -8,6 +8,7 @@
 
 
 HEAD_FEATURES = 128
+LANES = 128
 Z = ("zh", "zl")
 SP = ("zh", "zl", "c")
 PLANE = ("c", "tp")
@@ -25,49 +26,45 @@
     return jnp.dot(a, b, precision=highest_precision)
 
 
-def pack_thirds(gate_ref, up_ref, down_ref, first_ref, second_ref, third_ref, sems):
-    share = down_ref.shape[0] // 3
-    copies = []
-    for part, ref in enumerate((first_ref, second_ref, third_ref)):
-        cut = pl.ds(part * share, share)
-        moves = [(gate_ref.at[:, cut], ref.at[:, pl.ds(0, share)])]
-        moves.append((up_ref.at[:, cut], ref.at[:, pl.ds(share, share)]))
-        for k in range(0, ref.shape[0], share):
-            source = down_ref.at[cut, pl.ds(k, share)]
-            moves.append((source, ref.at[pl.ds(k, share), pl.ds(2 * share, share)]))
-        copies += moves
-    copies = [pltpu.make_async_copy(x, y, sems.at[k]) for k, (x, y) in enumerate(copies)]
-    for copy in copies:
-        copy.start()
-    for copy in copies:
-        copy.wait()
-
-
-def spread(gate, up, down, side):
-    width, share = gate.shape
-    share //= 3
-    packed = jax.ShapeDtypeStruct((width, 3 * share), gate.dtype)
-    anywhere = pl.BlockSpec(memory_space=pl.ANY)
-    thirds = pl.pallas_call(
-        pack_thirds,
-        out_shape=(packed,) * 3,
-        in_specs=[anywhere] * 3,
-        out_specs=(anywhere,) * 3,
-        scratch_shapes=[pltpu.SemaphoreType.DMA((3 * (2 + width // share),))],
-        name="pack_thirds",
-    )(gate, up, down)
+def regroup(lanes):
+    row = lax.broadcasted_iota(jnp.int32, (16 * lanes, 16 * lanes), 0)
+    col = lax.broadcasted_iota(jnp.int32, (16 * lanes, 16 * lanes), 1)
+    row_kind, row_part = (row // (4 * lanes), row // lanes % 4)
+    col_part, col_kind = (col // (4 * lanes), col // lanes % 4)
+    same = (row_kind == col_kind) & (row_part == col_part) & (row % lanes == col % lanes)
+    return jnp.where(same, 1.0, 0.0).astype(jnp.bfloat16)
+
+
+def pack_parts(gate_ref, up_ref, down_ref, outs):
+    depth, hidden = gate_ref.shape
+    half, lanes = (depth // 2, LANES // 4)
+    order = regroup(lanes)
+    for block in range(hidden // LANES):
+        cut = slice(block * LANES, (block + 1) * LANES)
+        kinds = [ref[k : k + half, cut] for ref in (gate_ref, up_ref) for k in (0, half)]
+        parts = jnp.dot(jnp.concatenate(kinds, 1), order, preferred_element_type=jnp.float32)
+        parts = parts.astype(jnp.bfloat16)
+        for part, out in enumerate(outs):
+            out[block * half : (block + 1) * half] = parts[:, part * LANES : (part + 1) * LANES]
+            first = block * LANES + part * lanes
+            for k in range(depth // LANES):
+                row = hidden // LANES * (half + k * lanes) + block * lanes
+                out[row : row + lanes] = down_ref[first : first + lanes, k * LANES : (k + 1) * LANES]
+
+
+def spread(parts, side):
     out = []
-    for third, (dy, dx) in zip(thirds, ((0, 1), (0, side - 1), (1, 0))):
+    for part, (dy, dx) in zip(parts, ((0, 1), (0, side - 1), (1, 0), (side - 1, 0))):
         pairs = [
             (y * side + x, (y + dy) % side * side + (x + dx) % side)
             for y in range(side)
             for x in range(side)
         ]
-        out.append(lax.ppermute(third, "tp", pairs))
+        out.append(lax.ppermute(part, "tp", pairs))
     return out
 
 
-def entering(own, weights, side):
+def entering(own, parts, side):
     kind = jnp.bfloat16
     zh, zl, c = (lax.axis_index(axis) for axis in SP)
     near = lax.all_gather(own, ("zl", "c")).astype(jnp.float32)
@@ -84,8 +81,8 @@
     group = jnp.concatenate([map_all, state_all], 0).astype(kind)
     quarter = lax.dynamic_slice_in_dim(group, (2 * zl + c) * (width // 2), width // 2, 0)
     count = lax.axis_size(Z)
-    quarter, weights = lax.optimization_barrier((quarter, weights))
-    thirds = spread(*weights, side)
+    quarter, parts = lax.optimization_barrier((quarter, parts))
+    parts = spread(parts, side)
     far = jnp.broadcast_to(quarter[None], (count, *quarter.shape))
     far = lax.all_to_all(far, Z, 0, 0, tiled=True)
     far = lax.all_gather(far, "c")
@@ -94,7 +91,7 @@
     state = jnp.zeros((width, width), jnp.float32)
     for k in range(count // 2 - 1):
         state = jnp.where(k < zh, mm(far[k, :width], state) + far[k, width:], state)
-    return mm(map_in, state) + state_in, thirds
+    return mm(map_in, state) + state_in, parts
 
 
 def in_blocks(x, dim, length):
@@ -130,7 +127,12 @@
     return center * lax.rsqrt(jnp.mean(center * center, -1, keepdims=True) + 1e-05) * gain
 
 
-def local_span(q_ref, k_ref, v_ref, beta_ref, decay_ref, rate_ref, both_ref, mix_ref, out_ref):
+def local_span(q_ref, k_ref, v_ref, beta_ref, decay_ref, rate_ref, *refs):
+    tables, (both_ref, mix_ref, out_ref), outs = refs[:3], refs[3:6], refs[6:10]
+    bufs, part_bufs, sems = refs[10:13], refs[13:17], refs[17]
+    copies = [pltpu.make_async_copy(x, y, sems.at[k]) for k, (x, y) in enumerate(zip(tables, bufs))]
+    for copy in copies:
+        copy.start()
     size = HEAD_FEATURES
     row = lax.broadcasted_iota(jnp.int32, (size, size), 0)
     col = lax.broadcasted_iota(jnp.int32, (size, size), 1)
@@ -169,6 +171,14 @@
         col < row, dot(k_ref[...], k_ref[...], ((1,), (1,))) * across * (beta * key_scale), 0.0
     )
     scores = dot(q_ref[...], k_ref[...], ((1,), (1,))) * across * query_scale
+    for copy in copies:
+        copy.wait()
+    pack_parts(*bufs, part_bufs)
+    copies = [
+        pltpu.make_async_copy(x, y, sems.at[3 + k]) for k, (x, y) in enumerate(zip(part_bufs, outs))
+    ]
+    for copy in copies:
+        copy.start()
     differ = row ^ col
     inverse = jnp.where(eye, 1.0, 0.0) - jnp.where(differ == 1, lower, 0.0)
     for level in range(1, 7):
@@ -184,16 +194,19 @@
     seen = dot(scores, solved)
     mix_ref[...] = query * (query_scale * grown) - seen[:, :size]
     out_ref[...] = seen[:, size:]
+    for copy in copies:
+        copy.wait()
 
 
 def run_experts(rows_ref, *refs):
-    out_ref, bufs, sems = refs[6], refs[7:13], refs[13]
-    copies = [pltpu.make_async_copy(refs[k], bufs[k], sems.at[k]) for k in range(6)]
-    for copy in copies:
+    out_ref, bufs, sems = refs[7], refs[8:15], refs[15]
+    copies = [pltpu.make_async_copy(refs[k], bufs[k], sems.at[k]) for k in range(7)]
+    for copy in (*copies[:2], *copies[3:], copies[2]):
         copy.start()
     gate_ref, up_ref, down_ref = bufs[:3]
     rows = rows_ref[...]
-    share = bufs[3].shape[1] // 3
+    width = rows.shape[1]
+    half, lanes, blocks = (width // 2, LANES // 4, down_ref.shape[0] // LANES)
 
     def dot(a, b):
         return jnp.dot(a, b, preferred_element_type=jnp.float32)
@@ -202,15 +215,31 @@
     gate = dot(rows, gate_ref[...])
     copies[1].wait()
     inner = (jax.nn.silu(gate) * dot(rows, up_ref[...])).astype(jnp.bfloat16)
+    place = lax.broadcasted_iota(jnp.int32, (rows.shape[0], LANES), 1) // lanes
+    arrived = [jnp.zeros((rows.shape[0], LANES), jnp.float32)] * blocks
+    for part, (copy, ref) in enumerate(zip(copies[3:], bufs[3:])):
+        copy.wait()
+        table = jnp.concatenate([ref[k * half : (k + 1) * half] for k in range(blocks)], 1)
+        low, high = (dot(rows[:, :half], table), dot(rows[:, half:], table))
+        for k in range(blocks):
+            cut = slice(k * LANES, (k + 1) * LANES)
+            sums = low[:, cut] + pltpu.roll(high[:, cut], LANES - lanes, 1)
+            acts = jax.nn.silu(sums) * pltpu.roll(sums, LANES - 2 * lanes, 1)
+            if part > 0:
+                acts = pltpu.roll(acts, part * lanes, 1)
+            arrived[k] = jnp.where(place == part, acts, arrived[k])
+    arrived = jnp.concatenate(arrived, 1).astype(jnp.bfloat16)
     copies[2].wait()
-    total = dot(inner, down_ref[...])
-    for copy, ref in zip(copies[3:], bufs[3:]):
-        copy.wait()
-        both = dot(rows, ref[:, : 2 * share])
-        inner = (jax.nn.silu(both[:, :share]) * both[:, share:]).astype(jnp.bfloat16)
-        down = [ref[k : k + share, 2 * share :] for k in range(0, ref.shape[0], share)]
-        total = total + dot(inner, jnp.concatenate(down, 1))
-    out_ref[...] = total.astype(out_ref.dtype)
+
+    def down_block(k):
+        row = blocks * (half + k * lanes)
+        runs = [ref[row + b * lanes : row + (b + 1) * lanes] for b in range(blocks) for ref in bufs[3:]]
+        return jnp.concatenate(runs, 0)
+
+    for k in range(0, width // LANES, 2):
+        cut = slice(k * LANES, (k + 2) * LANES)
+        other = jnp.concatenate([down_block(k), down_block(k + 1)], 1)
+        out_ref[:, cut] = (dot(inner, down_ref[:, cut]) + dot(arrived, other)).astype(out_ref.dtype)
 
 
 def per_device(
@@ -235,21 +264,27 @@
     length, width = residual_in.shape
 
     vmem = pl.BlockSpec(memory_space=pltpu.VMEM)
-    both, mix, local = pl.pallas_call(
+    anywhere = pl.BlockSpec(memory_space=pl.ANY)
+    split_count = lax.axis_size("tp")
+    side = round(split_count**0.5)
+    tables = (expert_gate[0], expert_up[0], expert_down[0])
+    packed = (3 * tables[0].size // 4 // LANES, LANES)
+    both, mix, local, *parts = pl.pallas_call(
         local_span,
         out_shape=(
             pltpu.VMEM((2 * HEAD_FEATURES, HEAD_FEATURES), jnp.bfloat16),
             pltpu.VMEM((length, HEAD_FEATURES), jnp.float32),
             pltpu.VMEM((length, HEAD_FEATURES), jnp.float32),
-        ),
-        in_specs=[vmem] * 5 + [pl.BlockSpec(memory_space=pltpu.SMEM)],
-        out_specs=(vmem,) * 3,
+        )
+        + (jax.ShapeDtypeStruct(packed, jnp.bfloat16),) * 4,
+        in_specs=[vmem] * 5 + [pl.BlockSpec(memory_space=pltpu.SMEM)] + [anywhere] * 3,
+        out_specs=(vmem,) * 3 + (anywhere,) * 4,
+        scratch_shapes=[pltpu.VMEM(x.shape, x.dtype) for x in tables]
+        + [pltpu.VMEM(packed, jnp.bfloat16)] * 4
+        + [pltpu.SemaphoreType.DMA((7,))],
         name="local_span",
-    )(queries, keys, values, beta_logit, decay_logit, decay_log)
-    split_count = lax.axis_size("tp")
-    side = round(split_count**0.5)
-    gate_matrix, up_matrix, down_matrix = (expert_gate[0], expert_up[0], expert_down[0])
-    state, thirds = entering(both, (gate_matrix, up_matrix, down_matrix), side)
+    )(queries, keys, values, beta_logit, decay_logit, decay_log, *tables)
+    state, parts = entering(both, parts, side)
     mixed = local + mm(mix, state)
     normalized = mixed * lax.rsqrt(jnp.mean(mixed * mixed, -1, keepdims=True) + 1e-06) * head_gain
     gated = (normalized * jax.nn.silu(out_gate.astype(jnp.float32))).astype(jnp.bfloat16)
@@ -284,20 +319,20 @@
     turns = jnp.stack([arrived, swapped], 1)[:, None, :, None]
     turns = jnp.broadcast_to(turns, (2, side // 2, 2, side // 2, 2, half, width))
     piece = in_plane(turns.reshape(2 * split_count, half, width)).reshape(-1, width)
-    tables = (gate_matrix, up_matrix, down_matrix, *thirds)
+    tables += tuple(parts)
     partial_value = pl.pallas_call(
         run_experts,
         out_shape=pltpu.VMEM(piece.shape, jnp.bfloat16),
-        in_specs=[vmem] + [pl.BlockSpec(memory_space=pl.ANY)] * 6,
+        in_specs=[vmem] + [anywhere] * 7,
         out_specs=vmem,
         scratch_shapes=[pltpu.VMEM(x.shape, x.dtype) for x in tables]
-        + [pltpu.SemaphoreType.DMA((6,))],
+        + [pltpu.SemaphoreType.DMA((7,))],
         name="run_experts",
     )(held(piece), *tables)
-    parts = in_plane(partial_value.reshape(2 * split_count, half, width))
-    parts = parts.reshape(2, side // 2, 2, side // 2, 2, half, width).astype(jnp.float32)
-    parts = jnp.sum(parts, axis=(1, 3))
-    result = jnp.stack([parts[:, 0, 0] + parts[:, 1, 1], parts[:, 0, 1] + parts[:, 1, 0]], 1)
+    shares = in_plane(partial_value.reshape(2 * split_count, half, width))
+    shares = shares.reshape(2, side // 2, 2, side // 2, 2, half, width).astype(jnp.float32)
+    shares = jnp.sum(shares, axis=(1, 3))
+    result = jnp.stack([shares[:, 0, 0] + shares[:, 1, 1], shares[:, 0, 1] + shares[:, 1, 0]], 1)
     result = result.reshape(2, chips, width).astype(jnp.bfloat16)
     back = along_z(result.transpose(1, 0, 2)).reshape(expert_count, width)
     gathered = jnp.einsum("rks,sd->rkd", table, back, preferred_element_type=jnp.float32)

time: 352 us -> 207 us (0.59)
  Pallas kernels: 156 us -> 16.8 us
  waiting for transfers between devices: 76.5 us -> 64.5 us
  starting transfers between devices: 49.2 us -> 53.4 us
    pallas_call x1 -> x0, Pallas kernels: 145 us -> none  [spread(): pl.pallas_call(pack_thirds, out_shape=(packed,) * 3, in_specs=[anywhere]...]
    ppermute x3 -> x4, waiting for transfers between devices: 34.7 us -> 23.2 us  [spread(): out.append(lax.ppermute(part, 'tp', pairs))]
    pallas_call x1, Pallas kernels: 2.73 us -> 8.73 us  [per_device(): pl.pallas_call(local_span, out_shape=(pltpu.VMEM((2 * HEAD_FEATURES, HEAD...]
    ppermute x3 -> x4, starting transfers between devices: 8.42 us -> 13 us  [spread(): out.append(lax.ppermute(part, 'tp', pairs))]
  transfers between devices with their start and end apart: 8 -> 9, of which waited for: 7 -> 8; matrix products, arithmetic and copies ran while one was open for 0% -> 1% of each run, Pallas kernels for 42% -> 0%
where the time goes in v5:
time: 207 us; the launch traced here: 204 us
  waiting for transfers between devices  64.5 us (31%)
  blocking collectives  55 us (27%)
  starting transfers between devices  53.4 us (26%)
  Pallas kernels  16.8 us (8%)
  local copies, waits for them, and re-layouts  4.72 us (2%)
  matrix products  4.31 us (2%)
  other arithmetic  3.74 us (2%)
    ppermute x4, waiting for transfers between devices, spread(): out.append(lax.ppermute(part, 'tp', pairs))  23.2 us
    all_to_all x1, blocking collectives, in_plane(): return lax.all_to_all(x, PLANE, 0, 0, tiled=True)  22.7 us
    all_to_all x2, starting transfers between devices, along_z(): out = lax.all_to_all(x.reshape(chips, 16, width // 8), Z, 0, 0, tiled=True)  17.1 us
    all_to_all x1, waiting for transfers between devices, entering(): far = lax.all_to_all(far, Z, 0, 0, tiled=True)  14.1 us
    all_to_all x1, blocking collectives, copy_for_each(): lax.all_to_all(jnp.broadcast_to(x[None], (length, *x.shape)), axis, 0, 0,...  13 us
    ppermute x4, starting transfers between devices, spread(): out.append(lax.ppermute(part, 'tp', pairs))  13 us
    all_gather x1, blocking collectives, entering(): near = lax.all_gather(own, ('zl', 'c')).astype(jnp.float32)  12.5 us
    all_to_all x2, waiting for transfers between devices, along_z(): out = lax.all_to_all(x.reshape(chips, 16, width // 8), Z, 0, 0, tiled=True)  11.9 us
  transfers between devices with their start and end apart: 9, of which 8 were waited for; matrix products, arithmetic and copies ran while one was open for 1% of the time, Pallas kernels for 0%

profile of v5, /device:TPU:1, one launch (start us, length us, event | category | flops | bytes accessed | tf_op | source)
XLA Modules:
  0.0 203.6 jit_solution(15930417846904111177)
XLA Ops:
  0.7 8.7 %local_span.1 = (bf16[256,128]{1,0:T(8,128)(2,1)S(1)}, f32[128,128]{1,0:T(8,128)S(1)}, f32[128,128]{1,0:T(8,128)S(1)}, bf16[4608,128]{1,0:T(8,128)(2,1)}, bf16[4...) custom-call(bf16[128,128]{1,0:T(8,128)(2,1)} %q_ref.1, bf16[128,128]{1,0:T(8,128)(2,1)} %k_ref.1, ...), custom_call_target="tpu_custom_call" | custom-call | tf_op jit(solution)/shard_map/local_span/pallas_call | solution.py:272
  9.5 12.5 %all-gather = bf16[1024,128]{1,0:T(8,128)(2,1)S(1)} all-gather(bf16[256,128]{1,0:T(8,128)(2,1)S(1)} %get-tuple-element.19), channel_id=2, replica_groups=mesh['zh'=8,'zl'=2,'c'=2,'tp'=16] {'zl','c'}, dimensions={0}, use_global_device_ids=true | all-gather | bytes 327680 | tf_op jit(solution)/shard_map/all_gather | solution.py:70
  23.1 0.8 broadcast_in_dim.6
  23.8 9.6 %all-to-all-start = ((bf16[16,64,128]{2,1,0:T(8,128)(2,1)}), bf16[16,64,128]{2,1,0:T(8,128)(2,1)S(1)}, u32[]{:S(2)}, u32[]{:S(2)}) async-start(bf16[16,64,128]{2,1,0:T(8,128)(2,1)} %broadcast_in_dim.6), calls=%async_computation | async-start | bytes 524288 | tf_op jit(solution)/shard_map/all_to_all | solution.py:87
  33.4 14.1 %all-to-all-done = bf16[16,64,128]{2,1,0:T(8,128)(2,1)S(1)} async-done(((bf16[16,64,128]{2,1,0:T(8,128)(2,1)}), bf16[16,64,128]{2,1,0:T(8,128)(2,1)S(1)}, u32[]{:S(2)}, u32[]{:S(2)}) %all-to-all-start) | async-done | bytes 262176 | tf_op jit(solution)/shard_map/all_to_all | solution.py:87
  47.6 6.8 %all-gather.1 = bf16[32,64,128]{2,1,0:T(8,128)(2,1)S(1)} all-gather(bf16[16,64,128]{2,1,0:T(8,128)(2,1)S(1)} %all-to-all-done), channel_id=3, replica_groups=mesh['zh'=8,'zl'=2,'c'=2,'tp'=16] {'c'}, dimensions={0}, use_global_device_ids=true | all-gather | bytes 786432 | tf_op jit(solution)/shard_map/all_gather | solution.py:88
  56.4 1.1 fusion
  57.5 6.9 %all-to-all-start.1 = ((bf16[16,8,2048]{2,1,0:T(8,128)(2,1)}), bf16[16,8,2048]{2,1,0:T(8,128)(2,1)S(1)}, u32[]{:S(2)}, u32[]{:S(2)}) async-start(bf16[16,8,2048]{2,1,0:T(8,128)(2,1)} %fusion), calls=%async_computation.1 | async-start | bytes 1048576 | tf_op jit(solution)/shard_map/all_to_all | solution.py:105
  64.6 10.6 %all-to-all-done.1 = bf16[16,8,2048]{2,1,0:T(8,128)(2,1)S(1)} async-done(((bf16[16,8,2048]{2,1,0:T(8,128)(2,1)}), bf16[16,8,2048]{2,1,0:T(8,128)(2,1)S(1)}, u32[]{:S(2)}, u32[]{:S(2)}) %all-to-all-start.1) | async-done | bytes 524320 | tf_op jit(solution)/shard_map/all_to_all | solution.py:105
  75.2 0.9 fusion.40
  76.1 1.0 multiply_reduce_fusion.1
  77.1 0.8 multiply_convert_fusion.1
  78.2 0.7 reshape.122
  78.9 5.7 %all-to-all-start.2 = ((bf16[16,16,256]{2,1,0:T(8,128)(2,1)}), bf16[16,16,256]{2,1,0:T(8,128)(2,1)S(1)}, u32[]{:S(2)}, u32[]{:S(2)}) async-start(bf16[16,16,256]{2,1,0:T(8,128)(2,1)} %reshape.122), calls=%async_computation.2 | async-start | bytes 262144 | tf_op jit(solution)/shard_map/all_to_all | solution.py:310
  84.6 2.2 %collective-permute-start = (bf16[4608,128]{1,0:T(8,128)(2,1)}, bf16[4608,128]{1,0:T(8,128)(2,1)}, u32[]{:S(2)}, u32[]{:S(2)}) collective-permute-start(bf16[4608,128]{1,0:T(8,128)(2,1)} %get-tuple-element.25), channel_id=1, source_target_pairs={{0,1},{1,2},{2,3},{3,0},{4,5},{5,6},{6,7},{7,4},{8,9},{9,10},{10,1... | collective-permute-start | bytes 3538952 | tf_op jit(solution)/shard_map/ppermute | solution.py:63
  86.8 4.3 %collective-permute-start.1 = (bf16[4608,128]{1,0:T(8,128)(2,1)}, bf16[4608,128]{1,0:T(8,128)(2,1)}, u32[]{:S(2)}, u32[]{:S(2)}) collective-permute-start(bf16[4608,128]{1,0:T(8,128)(2,1)} %get-tuple-element.26), channel_id=1, source_target_pairs={{0,3},{1,0},{2,1},{3,2},{4,7},{5,4},{6,5},{7,6},{8,11},{9,8},{10,9... | collective-permute-start | bytes 3538952 | tf_op jit(solution)/shard_map/ppermute | solution.py:63
  91.1 1.9 collective-permute-start.2
  93.0 4.6 %collective-permute-start.3 = (bf16[4608,128]{1,0:T(8,128)(2,1)}, bf16[4608,128]{1,0:T(8,128)(2,1)}, u32[]{:S(2)}, u32[]{:S(2)}) collective-permute-start(bf16[4608,128]{1,0:T(8,128)(2,1)} %get-tuple-element.28), channel_id=1, source_target_pairs={{0,12},{1,13},{2,14},{3,15},{4,0},{5,1},{6,2},{7,3},{8,4},{9,5},{1... | collective-permute-start | bytes 3538952 | tf_op jit(solution)/shard_map/ppermute | solution.py:63
  97.8 1.1 broadcast_in_dim.7
  98.9 6.8 %all-to-all-start.3 = ((bf16[32,8,2048]{2,1,0:T(8,128)(2,1)}), bf16[32,8,2048]{2,1,0:T(8,128)(2,1)S(1)}, u32[]{:S(2)}, u32[]{:S(2)}) async-start(bf16[32,8,2048]{2,1,0:T(8,128)(2,1)} %bitcast.36), calls=%async_computation.3 | async-start | bytes 2097152 | tf_op jit(solution)/shard_map/all_to_all | solution.py:314
  105.8 8.1 %collective-permute-done.refs_3_ = bf16[4608,128]{1,0:T(8,128)(2,1)} collective-permute-done((bf16[4608,128]{1,0:T(8,128)(2,1)}, bf16[4608,128]{1,0:T(8,128)(2,1)}, u32[]{:S(2)}, u32[]{:S(2)}) %collective-permute-start) | collective-permute-done | bytes 1179680 | tf_op jit(solution)/shard_map/ppermute | solution.py:63
  113.9 0.6 collective-permute-done.1.refs_4_
  114.4 13.5 %collective-permute-done.2.refs_5_ = bf16[4608,128]{1,0:T(8,128)(2,1)} collective-permute-done((bf16[4608,128]{1,0:T(8,128)(2,1)}, bf16[4608,128]{1,0:T(8,128)(2,1)}, u32[]{:S(2)}, u32[]{:S(2)}) %collective-permute-start.2) | collective-permute-done | bytes 1179680 | tf_op jit(solution)/shard_map/ppermute | solution.py:63
  127.9 1.1 collective-permute-done.3.refs_6_
  129.0 4.7 %all-to-all-done.3 = bf16[32,8,2048]{2,1,0:T(8,128)(2,1)S(1)} async-done(((bf16[32,8,2048]{2,1,0:T(8,128)(2,1)}), bf16[32,8,2048]{2,1,0:T(8,128)(2,1)S(1)}, u32[]{:S(2)}, u32[]{:S(2)}) %all-to-all-start.3) | async-done | bytes 1048608 | tf_op jit(solution)/shard_map/all_to_all | solution.py:314
  133.7 8.1 %run_experts.1 = bf16[256,2048]{1,0:T(8,128)(2,1)S(1)} custom-call(bf16[256,2048]{1,0:T(8,128)(2,1)S(1)} %bitcast.159, bf16[2048,384]{1,0:T(8,128)(2,1)} %bitcast.162, bf16[2048,384]{1,0:T(8,128)(2,1)} %bitcast.164, bf16[384,2048]{1,0:T(8,128)(2,1)} %bitcast.166, bf16[4608,128]{1,0:T(8,128)(2,1)} %collective-permute-done.refs_3_, ...), custom_call_target="tpu_custom_call" | custom-call | tf_op jit(solution)/shard_map/run_experts/pallas_call | solution.py:323
  141.7 22.7 %all_to_all.35 = bf16[32,8,2048]{2,1,0:T(8,128)(2,1)S(1)} all-to-all(bf16[32,8,2048]{2,1,0:T(8,128)(2,1)S(1)} %bitcast.160), channel_id=1, replica_groups=mesh['zh'=8,'zl'=2,'c'=2,'tp'=16] {'c','tp'}, dimensions={0} | all-to-all | bytes 2097152 | tf_op jit(solution)/shard_map/all_to_all | solution.py:314
  164.8 0.7 reshape.128
  165.6 11.5 %all-to-all-start.5 = ((bf16[16,16,256]{2,1,0:T(8,128)(2,1)}), bf16[16,16,256]{2,1,0:T(8,128)(2,1)S(1)}, u32[]{:S(2)}, u32[]{:S(2)}) async-start(bf16[16,16,256]{2,1,0:T(8,128)(2,1)} %reshape.128), calls=%async_computation.5 | async-start | bytes 262144 | tf_op jit(solution)/shard_map/all_to_all | solution.py:310
  177.1 11.9 %all-to-all-done.5 = bf16[16,16,256]{2,1,0:T(8,128)(2,1)S(1)} async-done(((bf16[16,16,256]{2,1,0:T(8,128)(2,1)}), bf16[16,16,256]{2,1,0:T(8,128)(2,1)S(1)}, u32[]{:S(2)}, u32[]{:S(2)}) %all-to-all-start.5) | async-done | bytes 131104 | tf_op jit(solution)/shard_map/all_to_all | solution.py:310
  189.8 13.0 %all_to_all.36 = bf16[16,8,2048]{2,1,0:T(8,128)(2,1)S(1)} all-to-all(bf16[16,8,2048]{2,1,0:T(8,128)(2,1)S(1)} %broadcast_in_dim.8), channel_id=1, replica_groups=mesh['zh'=8,'zl'=2,'c'=2,'tp'=16] {'tp'}, dimensions={0} | all-to-all | bytes 1048576 | tf_op jit(solution)/shard_map/all_to_all | solution.py:111
  202.8 0.8 copy.52
  (60 shorter events, 4.8 us)
Async XLA Ops:
  0.0 56.4 %copy-start = (bf16[128,2048]{1,0:T(8,128)(2,1)S(1)}, bf16[128,2048]{1,0:T(8,128)(2,1)}, u32[]{:S(2)}) copy-start(bf16[128,2048]{1,0:T(8,128)(2,1)} %param.26) | copy-start | bytes 1572868
  23.8 23.7 %all-to-all-start = ((bf16[16,64,128]{2,1,0:T(8,128)(2,1)}), bf16[16,64,128]{2,1,0:T(8,128)(2,1)S(1)}, u32[]{:S(2)}, u32[]{:S(2)}) async-start(bf16[16,64,128]{2,1,0:T(8,128)(2,1)} %broadcast_in_dim.6), calls=%async_computation | async-start | bytes 524288 | tf_op jit(solution)/shard_map/all_to_all | solution.py:87
  54.5 1.9 copy-start.1
  54.5 1.9 copy-start.6
  56.0 8.4 %copy-start.4 = (s32[128,2]{0,1:T(2,128)S(1)}, s32[128,2]{0,1:T(2,128)}, u32[]{:S(2)}) copy-start(s32[128,2]{0,1:T(2,128)} %param.29) | copy-start | bytes 3076
  57.5 19.6 %copy-start.2 = (f32[2048]{0:T(1024)S(1)}, f32[2048]{0:T(1024)}, u32[]{:S(2)}) copy-start(f32[2048]{0:T(1024)} %param.27) | copy-start | bytes 24580
  57.5 17.6 %all-to-all-start.1 = ((bf16[16,8,2048]{2,1,0:T(8,128)(2,1)}), bf16[16,8,2048]{2,1,0:T(8,128)(2,1)S(1)}, u32[]{:S(2)}, u32[]{:S(2)}) async-start(bf16[16,8,2048]{2,1,0:T(8,128)(2,1)} %fusion), calls=%async_computation.1 | async-start | bytes 1048576 | tf_op jit(solution)/shard_map/all_to_all | solution.py:105
  78.9 18.7 %all-to-all-start.2 = ((bf16[16,16,256]{2,1,0:T(8,128)(2,1)}), bf16[16,16,256]{2,1,0:T(8,128)(2,1)S(1)}, u32[]{:S(2)}, u32[]{:S(2)}) async-start(bf16[16,16,256]{2,1,0:T(8,128)(2,1)} %reshape.122), calls=%async_computation.2 | async-start | bytes 262144 | tf_op jit(solution)/shard_map/all_to_all | solution.py:310
  84.6 29.3 %collective-permute-start = (bf16[4608,128]{1,0:T(8,128)(2,1)}, bf16[4608,128]{1,0:T(8,128)(2,1)}, u32[]{:S(2)}, u32[]{:S(2)}) collective-permute-start(bf16[4608,128]{1,0:T(8,128)(2,1)} %get-tuple-element.25), channel_id=1, source_target_pairs={{0,1},{1,2},{2,3},{3,0},{4,5},{5,6},{6,7},{7,4},{8,9},{9,10},{10,1... | collective-permute-start | bytes 3538952 | tf_op jit(solution)/shard_map/ppermute | solution.py:63
  86.8 27.6 %collective-permute-start.1 = (bf16[4608,128]{1,0:T(8,128)(2,1)}, bf16[4608,128]{1,0:T(8,128)(2,1)}, u32[]{:S(2)}, u32[]{:S(2)}) collective-permute-start(bf16[4608,128]{1,0:T(8,128)(2,1)} %get-tuple-element.26), channel_id=1, source_target_pairs={{0,3},{1,0},{2,1},{3,2},{4,7},{5,4},{6,5},{7,6},{8,11},{9,8},{10,9... | collective-permute-start | bytes 3538952 | tf_op jit(solution)/shard_map/ppermute | solution.py:63
  91.1 36.8 %collective-permute-start.2 = (bf16[4608,128]{1,0:T(8,128)(2,1)}, bf16[4608,128]{1,0:T(8,128)(2,1)}, u32[]{:S(2)}, u32[]{:S(2)}) collective-permute-start(bf16[4608,128]{1,0:T(8,128)(2,1)} %get-tuple-element.27), channel_id=1, source_target_pairs={{0,4},{1,5},{2,6},{3,7},{4,8},{5,9},{6,10},{7,11},{8,12},{9,13},{1... | collective-permute-start | bytes 3538952 | tf_op jit(solution)/shard_map/ppermute | solution.py:63
  93.0 36.0 %collective-permute-start.3 = (bf16[4608,128]{1,0:T(8,128)(2,1)}, bf16[4608,128]{1,0:T(8,128)(2,1)}, u32[]{:S(2)}, u32[]{:S(2)}) collective-permute-start(bf16[4608,128]{1,0:T(8,128)(2,1)} %get-tuple-element.28), channel_id=1, source_target_pairs={{0,12},{1,13},{2,14},{3,15},{4,0},{5,1},{6,2},{7,3},{8,4},{9,5},{1... | collective-permute-start | bytes 3538952 | tf_op jit(solution)/shard_map/ppermute | solution.py:63
  98.9 34.7 %all-to-all-start.3 = ((bf16[32,8,2048]{2,1,0:T(8,128)(2,1)}), bf16[32,8,2048]{2,1,0:T(8,128)(2,1)S(1)}, u32[]{:S(2)}, u32[]{:S(2)}) async-start(bf16[32,8,2048]{2,1,0:T(8,128)(2,1)} %bitcast.36), calls=%async_computation.3 | async-start | bytes 2097152 | tf_op jit(solution)/shard_map/all_to_all | solution.py:314
  164.6 12.4 %copy-start.5 = (f32[128,2]{0,1:T(2,128)S(1)}, f32[128,2]{0,1:T(2,128)}, u32[]{:S(2)}) copy-start(f32[128,2]{0,1:T(2,128)} %param.30) | copy-start | bytes 3076
  164.6 25.1 %copy-start.3 = (f32[2048]{0:T(1024)S(1)}, f32[2048]{0:T(1024)}, u32[]{:S(2)}) copy-start(f32[2048]{0:T(1024)} %param.28) | copy-start | bytes 24580
  165.6 23.5 %all-to-all-start.5 = ((bf16[16,16,256]{2,1,0:T(8,128)(2,1)}), bf16[16,16,256]{2,1,0:T(8,128)(2,1)S(1)}, u32[]{:S(2)}, u32[]{:S(2)}) async-start(bf16[16,16,256]{2,1,0:T(8,128)(2,1)} %reshape.128), calls=%async_computation.5 | async-start | bytes 262144 | tf_op jit(solution)/shard_map/all_to_all | solution.py:310

commit v6 on v5

--- a/solution.py
+++ b/solution.py
@@ -35,21 +35,34 @@
     return jnp.where(same, 1.0, 0.0).astype(jnp.bfloat16)
 
 
-def pack_parts(gate_ref, up_ref, down_ref, outs):
+def pack_parts(gate_ref, up_ref, down_ref, bufs, outs, sems):
     depth, hidden = gate_ref.shape
-    half, lanes = (depth // 2, LANES // 4)
+    half, lanes, blocks = (depth // 2, LANES // 4, hidden // LANES)
+    copies = []
+
+    def leave(rows):
+        for buf, out in zip(bufs, outs):
+            copies.append(pltpu.make_async_copy(buf.at[rows], out.at[rows], sems.at[len(copies)]))
+            copies[-1].start()
+
+    for part, buf in enumerate(bufs):
+        for block in range(blocks):
+            first = block * LANES + part * lanes
+            for k in range(depth // LANES):
+                row = blocks * (half + k * lanes) + block * lanes
+                buf[row : row + lanes] = down_ref[first : first + lanes, k * LANES : (k + 1) * LANES]
+    leave(pl.ds(blocks * half, blocks * lanes * (depth // LANES)))
     order = regroup(lanes)
-    for block in range(hidden // LANES):
+    for block in range(blocks):
         cut = slice(block * LANES, (block + 1) * LANES)
         kinds = [ref[k : k + half, cut] for ref in (gate_ref, up_ref) for k in (0, half)]
         parts = jnp.dot(jnp.concatenate(kinds, 1), order, preferred_element_type=jnp.float32)
         parts = parts.astype(jnp.bfloat16)
-        for part, out in enumerate(outs):
-            out[block * half : (block + 1) * half] = parts[:, part * LANES : (part + 1) * LANES]
-            first = block * LANES + part * lanes
-            for k in range(depth // LANES):
-                row = hidden // LANES * (half + k * lanes) + block * lanes
-                out[row : row + lanes] = down_ref[first : first + lanes, k * LANES : (k + 1) * LANES]
+        for part, buf in enumerate(bufs):
+            buf[block * half : (block + 1) * half] = parts[:, part * LANES : (part + 1) * LANES]
+        leave(pl.ds(block * half, half))
+    for copy in copies:
+        copy.wait()
 
 
 def spread(parts, side):
@@ -171,14 +184,6 @@
         col < row, dot(k_ref[...], k_ref[...], ((1,), (1,))) * across * (beta * key_scale), 0.0
     )
     scores = dot(q_ref[...], k_ref[...], ((1,), (1,))) * across * query_scale
-    for copy in copies:
-        copy.wait()
-    pack_parts(*bufs, part_bufs)
-    copies = [
-        pltpu.make_async_copy(x, y, sems.at[3 + k]) for k, (x, y) in enumerate(zip(part_bufs, outs))
-    ]
-    for copy in copies:
-        copy.start()
     differ = row ^ col
     inverse = jnp.where(eye, 1.0, 0.0) - jnp.where(differ == 1, lower, 0.0)
     for level in range(1, 7):
@@ -196,6 +201,7 @@
     out_ref[...] = seen[:, size:]
     for copy in copies:
         copy.wait()
+    pack_parts(*bufs, part_bufs, outs, sems.at[3:])
 
 
 def run_experts(rows_ref, *refs):
@@ -281,7 +287,7 @@
         out_specs=(vmem,) * 3 + (anywhere,) * 4,
         scratch_shapes=[pltpu.VMEM(x.shape, x.dtype) for x in tables]
         + [pltpu.VMEM(packed, jnp.bfloat16)] * 4
-        + [pltpu.SemaphoreType.DMA((7,))],
+        + [pltpu.SemaphoreType.DMA((19,))],
         name="local_span",
     )(queries, keys, values, beta_logit, decay_logit, decay_log, *tables)
     state, parts = entering(both, parts, side)
@@ -294,7 +300,7 @@
     projected = sum_at_owner(
         jnp.dot(gated, out_weight, preferred_element_type=jnp.float32).astype(jnp.bfloat16), "tp", 0
     )
-    residual = lax.dynamic_slice_in_dim(residual_in, first, rows, 0)
+    residual = lax.optimization_barrier(lax.dynamic_slice_in_dim(residual_in, first, rows, 0))
     routes = lax.dynamic_slice_in_dim(expert_index, first, rows, 0)
     weights = lax.dynamic_slice_in_dim(route_weights, first, rows, 0)
     hidden_in = layer_norm(
@@ -307,7 +313,7 @@
     ).astype(jnp.bfloat16)
 
     def along_z(x):
-        out = lax.all_to_all(x.reshape(chips, 16, width // 8), Z, 0, 0, tiled=True)
+        out = lax.all_to_all(x.reshape(chips, 2, width), Z, 0, 0, tiled=True)
         return out.reshape(chips, 2, width)
 
     def in_plane(x):

time: 207 us -> 203 us (0.981)
  Pallas kernels: 16.8 us -> 14.4 us
    pallas_call x1, Pallas kernels: 8.73 us -> 6.37 us  [per_device(): pl.pallas_call(local_span, out_shape=(pltpu.VMEM((2 * HEAD_FEATURES, HEAD...]
where the time goes in v6:
time: 203 us; the launch traced here: 199 us
  waiting for transfers between devices  63.3 us (31%)
  blocking collectives  55 us (27%)
  starting transfers between devices  53.5 us (26%)
  Pallas kernels  14.4 us (7%)
  local copies, waits for them, and re-layouts  5.45 us (3%)
  matrix products  4.32 us (2%)
    ppermute x4, waiting for transfers between devices, spread(): out.append(lax.ppermute(part, 'tp', pairs))  22.8 us
    all_to_all x1, blocking collectives, in_plane(): return lax.all_to_all(x, PLANE, 0, 0, tiled=True)  22.7 us
    all_to_all x2, starting transfers between devices, along_z(): out = lax.all_to_all(x.reshape(chips, 2, width), Z, 0, 0, tiled=True)  17.2 us
    all_to_all x1, waiting for transfers between devices, entering(): far = lax.all_to_all(far, Z, 0, 0, tiled=True)  14.1 us
    all_to_all x1, blocking collectives, copy_for_each(): lax.all_to_all(jnp.broadcast_to(x[None], (length, *x.shape)), axis, 0, 0,...  13 us
    ppermute x4, starting transfers between devices, spread(): out.append(lax.ppermute(part, 'tp', pairs))  13 us
    all_gather x1, blocking collectives, entering(): near = lax.all_gather(own, ('zl', 'c')).astype(jnp.float32)  12.5 us
    all_to_all x2, waiting for transfers between devices, along_z(): out = lax.all_to_all(x.reshape(chips, 2, width), Z, 0, 0, tiled=True)  11.9 us
  transfers between devices with their start and end apart: 9, of which 8 were waited for; matrix products, arithmetic and copies ran while one was open for 1% of the time, Pallas kernels for 0%

profile of v6, /device:TPU:1, one launch (start us, length us, event | category | flops | bytes accessed | tf_op | source)
XLA Modules:
  0.0 198.9 jit_solution(16306985448012369638)
XLA Ops:
  0.7 6.4 %local_span.1 = (bf16[256,128]{1,0:T(8,128)(2,1)S(1)}, f32[128,128]{1,0:T(8,128)S(1)}, f32[128,128]{1,0:T(8,128)S(1)}, bf16[4608,128]{1,0:T(8,128)(2,1)}, bf16[4...) custom-call(bf16[128,128]{1,0:T(8,128)(2,1)} %q_ref.1, bf16[128,128]{1,0:T(8,128)(2,1)} %k_ref.1, ...), custom_call_target="tpu_custom_call" | custom-call | tf_op jit(solution)/shard_map/local_span/pallas_call | solution.py:278
  7.1 12.5 %all-gather = bf16[1024,128]{1,0:T(8,128)(2,1)S(1)} all-gather(bf16[256,128]{1,0:T(8,128)(2,1)S(1)} %get-tuple-element.19), channel_id=2, replica_groups=mesh['zh'=8,'zl'=2,'c'=2,'tp'=16] {'zl','c'}, dimensions={0}, use_global_device_ids=true | all-gather | bytes 327680 | tf_op jit(solution)/shard_map/all_gather | solution.py:83
  20.7 0.8 broadcast_in_dim.6
  21.5 9.6 %all-to-all-start = ((bf16[16,64,128]{2,1,0:T(8,128)(2,1)}), bf16[16,64,128]{2,1,0:T(8,128)(2,1)S(1)}, u32[]{:S(2)}, u32[]{:S(2)}) async-start(bf16[16,64,128]{2,1,0:T(8,128)(2,1)} %broadcast_in_dim.6), calls=%async_computation | async-start | bytes 524288 | tf_op jit(solution)/shard_map/all_to_all | solution.py:100
  31.1 14.1 %all-to-all-done = bf16[16,64,128]{2,1,0:T(8,128)(2,1)S(1)} async-done(((bf16[16,64,128]{2,1,0:T(8,128)(2,1)}), bf16[16,64,128]{2,1,0:T(8,128)(2,1)S(1)}, u32[]{:S(2)}, u32[]{:S(2)}) %all-to-all-start) | async-done | bytes 262176 | tf_op jit(solution)/shard_map/all_to_all | solution.py:100
  45.2 6.8 %all-gather.1 = bf16[32,64,128]{2,1,0:T(8,128)(2,1)S(1)} all-gather(bf16[16,64,128]{2,1,0:T(8,128)(2,1)S(1)} %all-to-all-done), channel_id=3, replica_groups=mesh['zh'=8,'zl'=2,'c'=2,'tp'=16] {'c'}, dimensions={0}, use_global_device_ids=true | all-gather | bytes 786432 | tf_op jit(solution)/shard_map/all_gather | solution.py:101
  53.7 0.3 multiply_reduce_fusion.2
  54.0 1.1 fusion
  55.2 6.9 %all-to-all-start.1 = ((bf16[16,8,2048]{2,1,0:T(8,128)(2,1)}), bf16[16,8,2048]{2,1,0:T(8,128)(2,1)S(1)}, u32[]{:S(2)}, u32[]{:S(2)}) async-start(bf16[16,8,2048]{2,1,0:T(8,128)(2,1)} %fusion), calls=%async_computation.1 | async-start | bytes 1048576 | tf_op jit(solution)/shard_map/all_to_all | solution.py:118
  62.1 0.8 constant_dynamic-slice_fusion.2
  63.0 9.8 %all-to-all-done.1 = bf16[16,8,2048]{2,1,0:T(8,128)(2,1)S(1)} async-done(((bf16[16,8,2048]{2,1,0:T(8,128)(2,1)}), bf16[16,8,2048]{2,1,0:T(8,128)(2,1)S(1)}, u32[]{:S(2)}, u32[]{:S(2)}) %all-to-all-start.1) | async-done | bytes 524320 | tf_op jit(solution)/shard_map/all_to_all | solution.py:118
  73.5 0.8 reshape.119
  74.3 5.7 %all-to-all-start.2 = ((bf16[16,2,2048]{2,1,0:T(2,128)(2,1)}), bf16[16,2,2048]{2,1,0:T(2,128)(2,1)S(1)}, u32[]{:S(2)}, u32[]{:S(2)}) async-start(bf16[16,2,2048]{2,1,0:T(2,128)(2,1)} %reshape.119), calls=%async_computation.2 | async-start | bytes 262144 | tf_op jit(solution)/shard_map/all_to_all | solution.py:316
  80.0 2.2 %collective-permute-start = (bf16[4608,128]{1,0:T(8,128)(2,1)}, bf16[4608,128]{1,0:T(8,128)(2,1)}, u32[]{:S(2)}, u32[]{:S(2)}) collective-permute-start(bf16[4608,128]{1,0:T(8,128)(2,1)} %get-tuple-element.25), channel_id=1, source_target_pairs={{0,1},{1,2},{2,3},{3,0},{4,5},{5,6},{6,7},{7,4},{8,9},{9,10},{10,1... | collective-permute-start | bytes 3538952 | tf_op jit(solution)/shard_map/ppermute | solution.py:76
  82.2 4.3 %collective-permute-start.1 = (bf16[4608,128]{1,0:T(8,128)(2,1)}, bf16[4608,128]{1,0:T(8,128)(2,1)}, u32[]{:S(2)}, u32[]{:S(2)}) collective-permute-start(bf16[4608,128]{1,0:T(8,128)(2,1)} %get-tuple-element.26), channel_id=1, source_target_pairs={{0,3},{1,0},{2,1},{3,2},{4,7},{5,4},{6,5},{7,6},{8,11},{9,8},{10,9... | collective-permute-start | bytes 3538952 | tf_op jit(solution)/shard_map/ppermute | solution.py:76
  86.5 1.9 collective-permute-start.2
  88.4 4.6 %collective-permute-start.3 = (bf16[4608,128]{1,0:T(8,128)(2,1)}, bf16[4608,128]{1,0:T(8,128)(2,1)}, u32[]{:S(2)}, u32[]{:S(2)}) collective-permute-start(bf16[4608,128]{1,0:T(8,128)(2,1)} %get-tuple-element.28), channel_id=1, source_target_pairs={{0,12},{1,13},{2,14},{3,15},{4,0},{5,1},{6,2},{7,3},{8,4},{9,5},{1... | collective-permute-start | bytes 3538952 | tf_op jit(solution)/shard_map/ppermute | solution.py:76
  93.1 0.4 pad_maximum_fusion
  93.6 1.1 broadcast_in_dim.7
  94.7 6.8 %all-to-all-start.3 = ((bf16[32,8,2048]{2,1,0:T(8,128)(2,1)}), bf16[32,8,2048]{2,1,0:T(8,128)(2,1)S(1)}, u32[]{:S(2)}, u32[]{:S(2)}) async-start(bf16[32,8,2048]{2,1,0:T(8,128)(2,1)} %bitcast.36), calls=%async_computation.3 | async-start | bytes 2097152 | tf_op jit(solution)/shard_map/all_to_all | solution.py:320
  101.6 7.7 %collective-permute-done.refs_3_ = bf16[4608,128]{1,0:T(8,128)(2,1)} collective-permute-done((bf16[4608,128]{1,0:T(8,128)(2,1)}, bf16[4608,128]{1,0:T(8,128)(2,1)}, u32[]{:S(2)}, u32[]{:S(2)}) %collective-permute-start) | collective-permute-done | bytes 1179680 | tf_op jit(solution)/shard_map/ppermute | solution.py:76
  109.3 0.6 collective-permute-done.1.refs_4_
  109.8 13.5 %collective-permute-done.2.refs_5_ = bf16[4608,128]{1,0:T(8,128)(2,1)} collective-permute-done((bf16[4608,128]{1,0:T(8,128)(2,1)}, bf16[4608,128]{1,0:T(8,128)(2,1)}, u32[]{:S(2)}, u32[]{:S(2)}) %collective-permute-start.2) | collective-permute-done | bytes 1179680 | tf_op jit(solution)/shard_map/ppermute | solution.py:76
  123.3 1.1 collective-permute-done.3.refs_6_
  124.4 4.7 %all-to-all-done.3 = bf16[32,8,2048]{2,1,0:T(8,128)(2,1)S(1)} async-done(((bf16[32,8,2048]{2,1,0:T(8,128)(2,1)}), bf16[32,8,2048]{2,1,0:T(8,128)(2,1)S(1)}, u32[]{:S(2)}, u32[]{:S(2)}) %all-to-all-start.3) | async-done | bytes 1048608 | tf_op jit(solution)/shard_map/all_to_all | solution.py:320
  129.1 8.1 %run_experts.1 = bf16[256,2048]{1,0:T(8,128)(2,1)S(1)} custom-call(bf16[256,2048]{1,0:T(8,128)(2,1)S(1)} %bitcast.159, bf16[2048,384]{1,0:T(8,128)(2,1)} %bitcast.162, bf16[2048,384]{1,0:T(8,128)(2,1)} %bitcast.164, bf16[384,2048]{1,0:T(8,128)(2,1)} %bitcast.166, bf16[4608,128]{1,0:T(8,128)(2,1)} %collective-permute-done.refs_3_, ...), custom_call_target="tpu_custom_call" | custom-call | tf_op jit(solution)/shard_map/run_experts/pallas_call | solution.py:329
  137.1 22.7 %all_to_all.35 = bf16[32,8,2048]{2,1,0:T(8,128)(2,1)S(1)} all-to-all(bf16[32,8,2048]{2,1,0:T(8,128)(2,1)S(1)} %bitcast.160), channel_id=1, replica_groups=mesh['zh'=8,'zl'=2,'c'=2,'tp'=16] {'c','tp'}, dimensions={0} | all-to-all | bytes 2097152 | tf_op jit(solution)/shard_map/all_to_all | solution.py:320
  160.1 0.8 copy.41
  160.8 11.5 %all-to-all-start.5 = ((bf16[16,2,2048]{2,1,0:T(2,128)(2,1)}), bf16[16,2,2048]{2,1,0:T(2,128)(2,1)S(1)}, u32[]{:S(2)}, u32[]{:S(2)}) async-start(bf16[16,2,2048]{2,1,0:T(2,128)(2,1)} %copy.41), calls=%async_computation.5 | async-start | bytes 262144 | tf_op jit(solution)/shard_map/all_to_all | solution.py:316
  172.4 11.9 %all-to-all-done.5 = bf16[16,2,2048]{2,1,0:T(2,128)(2,1)S(1)} async-done(((bf16[16,2,2048]{2,1,0:T(2,128)(2,1)}), bf16[16,2,2048]{2,1,0:T(2,128)(2,1)S(1)}, u32[]{:S(2)}, u32[]{:S(2)}) %all-to-all-start.5) | async-done | bytes 131104 | tf_op jit(solution)/shard_map/all_to_all | solution.py:316
  185.1 13.0 %all_to_all.36 = bf16[16,8,2048]{2,1,0:T(8,128)(2,1)S(1)} all-to-all(bf16[16,8,2048]{2,1,0:T(8,128)(2,1)S(1)} %broadcast_in_dim.8), channel_id=1, replica_groups=mesh['zh'=8,'zl'=2,'c'=2,'tp'=16] {'tp'}, dimensions={0} | all-to-all | bytes 1048576 | tf_op jit(solution)/shard_map/all_to_all | solution.py:124
  198.1 0.8 copy.48
  (58 shorter events, 4.8 us)
Async XLA Ops:
  0.0 54.0 %copy-start = (bf16[128,2048]{1,0:T(8,128)(2,1)S(1)}, bf16[128,2048]{1,0:T(8,128)(2,1)}, u32[]{:S(2)}) copy-start(bf16[128,2048]{1,0:T(8,128)(2,1)} %param.26) | copy-start | bytes 1572868
  21.5 23.7 %all-to-all-start = ((bf16[16,64,128]{2,1,0:T(8,128)(2,1)}), bf16[16,64,128]{2,1,0:T(8,128)(2,1)S(1)}, u32[]{:S(2)}, u32[]{:S(2)}) async-start(bf16[16,64,128]{2,1,0:T(8,128)(2,1)} %broadcast_in_dim.6), calls=%async_computation | async-start | bytes 524288 | tf_op jit(solution)/shard_map/all_to_all | solution.py:100
  52.1 1.9 copy-start.1
  52.1 1.9 copy-start.6
  54.0 8.9 %copy-start.4 = (s32[128,2]{0,1:T(2,128)S(1)}, s32[128,2]{0,1:T(2,128)}, u32[]{:S(2)}) copy-start(s32[128,2]{0,1:T(2,128)} %param.29) | copy-start | bytes 3076
  55.2 18.0 %copy-start.2 = (f32[2048]{0:T(1024)S(1)}, f32[2048]{0:T(1024)}, u32[]{:S(2)}) copy-start(f32[2048]{0:T(1024)} %param.27) | copy-start | bytes 24580
  55.2 17.6 %all-to-all-start.1 = ((bf16[16,8,2048]{2,1,0:T(8,128)(2,1)}), bf16[16,8,2048]{2,1,0:T(8,128)(2,1)S(1)}, u32[]{:S(2)}, u32[]{:S(2)}) async-start(bf16[16,8,2048]{2,1,0:T(8,128)(2,1)} %fusion), calls=%async_computation.1 | async-start | bytes 1048576 | tf_op jit(solution)/shard_map/all_to_all | solution.py:118
  74.3 18.7 %all-to-all-start.2 = ((bf16[16,2,2048]{2,1,0:T(2,128)(2,1)}), bf16[16,2,2048]{2,1,0:T(2,128)(2,1)S(1)}, u32[]{:S(2)}, u32[]{:S(2)}) async-start(bf16[16,2,2048]{2,1,0:T(2,128)(2,1)} %reshape.119), calls=%async_computation.2 | async-start | bytes 262144 | tf_op jit(solution)/shard_map/all_to_all | solution.py:316
  80.0 29.3 %collective-permute-start = (bf16[4608,128]{1,0:T(8,128)(2,1)}, bf16[4608,128]{1,0:T(8,128)(2,1)}, u32[]{:S(2)}, u32[]{:S(2)}) collective-permute-start(bf16[4608,128]{1,0:T(8,128)(2,1)} %get-tuple-element.25), channel_id=1, source_target_pairs={{0,1},{1,2},{2,3},{3,0},{4,5},{5,6},{6,7},{7,4},{8,9},{9,10},{10,1... | collective-permute-start | bytes 3538952 | tf_op jit(solution)/shard_map/ppermute | solution.py:76
  82.2 27.6 %collective-permute-start.1 = (bf16[4608,128]{1,0:T(8,128)(2,1)}, bf16[4608,128]{1,0:T(8,128)(2,1)}, u32[]{:S(2)}, u32[]{:S(2)}) collective-permute-start(bf16[4608,128]{1,0:T(8,128)(2,1)} %get-tuple-element.26), channel_id=1, source_target_pairs={{0,3},{1,0},{2,1},{3,2},{4,7},{5,4},{6,5},{7,6},{8,11},{9,8},{10,9... | collective-permute-start | bytes 3538952 | tf_op jit(solution)/shard_map/ppermute | solution.py:76
  86.5 36.8 %collective-permute-start.2 = (bf16[4608,128]{1,0:T(8,128)(2,1)}, bf16[4608,128]{1,0:T(8,128)(2,1)}, u32[]{:S(2)}, u32[]{:S(2)}) collective-permute-start(bf16[4608,128]{1,0:T(8,128)(2,1)} %get-tuple-element.27), channel_id=1, source_target_pairs={{0,4},{1,5},{2,6},{3,7},{4,8},{5,9},{6,10},{7,11},{8,12},{9,13},{1... | collective-permute-start | bytes 3538952 | tf_op jit(solution)/shard_map/ppermute | solution.py:76
  88.4 36.0 %collective-permute-start.3 = (bf16[4608,128]{1,0:T(8,128)(2,1)}, bf16[4608,128]{1,0:T(8,128)(2,1)}, u32[]{:S(2)}, u32[]{:S(2)}) collective-permute-start(bf16[4608,128]{1,0:T(8,128)(2,1)} %get-tuple-element.28), channel_id=1, source_target_pairs={{0,12},{1,13},{2,14},{3,15},{4,0},{5,1},{6,2},{7,3},{8,4},{9,5},{1... | collective-permute-start | bytes 3538952 | tf_op jit(solution)/shard_map/ppermute | solution.py:76
  94.7 34.4 %all-to-all-start.3 = ((bf16[32,8,2048]{2,1,0:T(8,128)(2,1)}), bf16[32,8,2048]{2,1,0:T(8,128)(2,1)S(1)}, u32[]{:S(2)}, u32[]{:S(2)}) async-start(bf16[32,8,2048]{2,1,0:T(8,128)(2,1)} %bitcast.36), calls=%async_computation.3 | async-start | bytes 2097152 | tf_op jit(solution)/shard_map/all_to_all | solution.py:320
  159.8 12.5 %copy-start.5 = (f32[128,2]{0,1:T(2,128)S(1)}, f32[128,2]{0,1:T(2,128)}, u32[]{:S(2)}) copy-start(f32[128,2]{0,1:T(2,128)} %param.30) | copy-start | bytes 3076
  160.0 24.9 %copy-start.3 = (f32[2048]{0:T(1024)S(1)}, f32[2048]{0:T(1024)}, u32[]{:S(2)}) copy-start(f32[2048]{0:T(1024)} %param.28) | copy-start | bytes 24580
  160.8 23.5 %all-to-all-start.5 = ((bf16[16,2,2048]{2,1,0:T(2,128)(2,1)}), bf16[16,2,2048]{2,1,0:T(2,128)(2,1)S(1)}, u32[]{:S(2)}, u32[]{:S(2)}) async-start(bf16[16,2,2048]{2,1,0:T(2,128)(2,1)} %copy.41), calls=%async_computation.5 | async-start | bytes 262144 | tf_op jit(solution)/shard_map/all_to_all | solution.py:316

commit v7 on v6

--- a/solution.py
+++ b/solution.py
@@ -38,20 +38,15 @@
 def pack_parts(gate_ref, up_ref, down_ref, bufs, outs, sems):
     depth, hidden = gate_ref.shape
     half, lanes, blocks = (depth // 2, LANES // 4, hidden // LANES)
+    size = bufs[0].shape[0] // blocks
+    early = size * (blocks - 1)
     copies = []
-
-    def leave(rows):
-        for buf, out in zip(bufs, outs):
-            copies.append(pltpu.make_async_copy(buf.at[rows], out.at[rows], sems.at[len(copies)]))
-            copies[-1].start()
-
     for part, buf in enumerate(bufs):
         for block in range(blocks):
             first = block * LANES + part * lanes
             for k in range(depth // LANES):
-                row = blocks * (half + k * lanes) + block * lanes
+                row = block * size + half + k * lanes
                 buf[row : row + lanes] = down_ref[first : first + lanes, k * LANES : (k + 1) * LANES]
-    leave(pl.ds(blocks * half, blocks * lanes * (depth // LANES)))
     order = regroup(lanes)
     for block in range(blocks):
         cut = slice(block * LANES, (block + 1) * LANES)
@@ -59,8 +54,12 @@
         parts = jnp.dot(jnp.concatenate(kinds, 1), order, preferred_element_type=jnp.float32)
         parts = parts.astype(jnp.bfloat16)
         for part, buf in enumerate(bufs):
-            buf[block * half : (block + 1) * half] = parts[:, part * LANES : (part + 1) * LANES]
-        leave(pl.ds(block * half, half))
+            row = block * size
+            buf[row : row + half] = parts[:, part * LANES : (part + 1) * LANES]
+            last = row == early
+            out = outs[part + 4] if last else outs[part].at[pl.ds(row, size)]
+            copies.append(pltpu.make_async_copy(buf.at[pl.ds(row, size)], out, sems.at[len(copies)]))
+            copies[-1].start()
     for copy in copies:
         copy.wait()
 
@@ -141,8 +140,8 @@
 
 
 def local_span(q_ref, k_ref, v_ref, beta_ref, decay_ref, rate_ref, *refs):
-    tables, (both_ref, mix_ref, out_ref), outs = refs[:3], refs[3:6], refs[6:10]
-    bufs, part_bufs, sems = refs[10:13], refs[13:17], refs[17]
+    tables, (both_ref, mix_ref, out_ref), outs = refs[:3], refs[3:6], refs[6:14]
+    bufs, part_bufs, sems = refs[14:17], refs[17:21], refs[21]
     copies = [pltpu.make_async_copy(x, y, sems.at[k]) for k, (x, y) in enumerate(zip(tables, bufs))]
     for copy in copies:
         copy.start()
@@ -205,27 +204,38 @@
 
 
 def run_experts(rows_ref, *refs):
-    out_ref, bufs, sems = refs[7], refs[8:15], refs[15]
-    copies = [pltpu.make_async_copy(refs[k], bufs[k], sems.at[k]) for k in range(7)]
-    for copy in (*copies[:2], *copies[3:], copies[2]):
-        copy.start()
+    out_ref, bufs, sems = refs[11], refs[12:23], refs[23]
+    copies = [pltpu.make_async_copy(refs[k], bufs[k], sems.at[k]) for k in range(11)]
     gate_ref, up_ref, down_ref = bufs[:3]
     rows = rows_ref[...]
     width = rows.shape[1]
     half, lanes, blocks = (width // 2, LANES // 4, down_ref.shape[0] // LANES)
+    size = bufs[7].shape[0]
 
     def dot(a, b):
         return jnp.dot(a, b, preferred_element_type=jnp.float32)
 
+    copies[0].start()
+    copies[1].start()
     copies[0].wait()
+    for k in range(3, 11):
+        copies[k].start()
     gate = dot(rows, gate_ref[...])
     copies[1].wait()
+    copies[2].start()
     inner = (jax.nn.silu(gate) * dot(rows, up_ref[...])).astype(jnp.bfloat16)
     place = lax.broadcasted_iota(jnp.int32, (rows.shape[0], LANES), 1) // lanes
     arrived = [jnp.zeros((rows.shape[0], LANES), jnp.float32)] * blocks
-    for part, (copy, ref) in enumerate(zip(copies[3:], bufs[3:])):
-        copy.wait()
-        table = jnp.concatenate([ref[k * half : (k + 1) * half] for k in range(blocks)], 1)
+
+    def run(part, block, first, count):
+        last = block == blocks - 1
+        ref, row = (bufs[7 + part], first) if last else (bufs[3 + part], block * size + first)
+        return ref[row : row + count]
+
+    for part in range(4):
+        copies[3 + part].wait()
+        copies[7 + part].wait()
+        table = jnp.concatenate([run(part, k, 0, half) for k in range(blocks)], 1)
         low, high = (dot(rows[:, :half], table), dot(rows[:, half:], table))
         for k in range(blocks):
             cut = slice(k * LANES, (k + 1) * LANES)
@@ -238,8 +248,8 @@
     copies[2].wait()
 
     def down_block(k):
-        row = blocks * (half + k * lanes)
-        runs = [ref[row + b * lanes : row + (b + 1) * lanes] for b in range(blocks) for ref in bufs[3:]]
+        first = half + k * lanes
+        runs = [run(part, block, first, lanes) for block in range(blocks) for part in range(4)]
         return jnp.concatenate(runs, 0)
 
     for k in range(0, width // LANES, 2):
@@ -282,15 +292,16 @@
             pltpu.VMEM((length, HEAD_FEATURES), jnp.float32),
             pltpu.VMEM((length, HEAD_FEATURES), jnp.float32),
         )
-        + (jax.ShapeDtypeStruct(packed, jnp.bfloat16),) * 4,
+        + (jax.ShapeDtypeStruct((packed[0] - packed[0] // 3, LANES), jnp.bfloat16),) * 4
+        + (jax.ShapeDtypeStruct((packed[0] // 3, LANES), jnp.bfloat16),) * 4,
         in_specs=[vmem] * 5 + [pl.BlockSpec(memory_space=pltpu.SMEM)] + [anywhere] * 3,
-        out_specs=(vmem,) * 3 + (anywhere,) * 4,
+        out_specs=(vmem,) * 3 + (anywhere,) * 8,
         scratch_shapes=[pltpu.VMEM(x.shape, x.dtype) for x in tables]
         + [pltpu.VMEM(packed, jnp.bfloat16)] * 4
-        + [pltpu.SemaphoreType.DMA((19,))],
+        + [pltpu.SemaphoreType.DMA((15,))],
         name="local_span",
     )(queries, keys, values, beta_logit, decay_logit, decay_log, *tables)
-    state, parts = entering(both, parts, side)
+    state, early = entering(both, parts[:4], side)
     mixed = local + mm(mix, state)
     normalized = mixed * lax.rsqrt(jnp.mean(mixed * mixed, -1, keepdims=True) + 1e-06) * head_gain
     gated = (normalized * jax.nn.silu(out_gate.astype(jnp.float32))).astype(jnp.bfloat16)
@@ -320,19 +331,22 @@
         return lax.all_to_all(x, PLANE, 0, 0, tiled=True)
 
     half = chips // 2
-    arrived = along_z(send).transpose(1, 0, 2).reshape(2, 2, half, width)
+    send, late = lax.optimization_barrier((send, parts[4:]))
+    late = spread(late, side)
+    arrived = along_z(send)
+    arrived = arrived.transpose(1, 0, 2).reshape(2, 2, half, width)
     swapped = arrived[:, ::-1]
     turns = jnp.stack([arrived, swapped], 1)[:, None, :, None]
     turns = jnp.broadcast_to(turns, (2, side // 2, 2, side // 2, 2, half, width))
     piece = in_plane(turns.reshape(2 * split_count, half, width)).reshape(-1, width)
-    tables += tuple(parts)
+    tables += tuple(early + late)
     partial_value = pl.pallas_call(
         run_experts,
         out_shape=pltpu.VMEM(piece.shape, jnp.bfloat16),
-        in_specs=[vmem] + [anywhere] * 7,
+        in_specs=[vmem] + [anywhere] * 11,
         out_specs=vmem,
         scratch_shapes=[pltpu.VMEM(x.shape, x.dtype) for x in tables]
-        + [pltpu.SemaphoreType.DMA((7,))],
+        + [pltpu.SemaphoreType.DMA((11,))],
         name="run_experts",
     )(held(piece), *tables)
     shares = in_plane(partial_value.reshape(2 * split_count, half, width))

time: 203 us -> 212 us (1.044)
  starting transfers between devices: 53.5 us -> 63.6 us
  waiting for transfers between devices: 63.3 us -> 58.5 us
    ppermute x4 -> x8, starting transfers between devices: 13 us -> 26.1 us  [spread(): out.append(lax.ppermute(part, 'tp', pairs))]
    all_to_all x1, waiting for transfers between devices: 4.65 us -> 0.01 us  [in_plane(): return lax.all_to_all(x, PLANE, 0, 0, tiled=True)]
    all_to_all x2, starting transfers between devices: 17.2 us -> 13.4 us  [along_z(): out = lax.all_to_all(x.reshape(chips, 2, width), Z, 0, 0, tiled=True)]
    ppermute x4 -> x8, waiting for transfers between devices: 22.8 us -> 19.2 us  [spread(): out.append(lax.ppermute(part, 'tp', pairs))]
    all_to_all x2, waiting for transfers between devices: 11.9 us -> 15.4 us  [along_z(): out = lax.all_to_all(x.reshape(chips, 2, width), Z, 0, 0, tiled=True)]
  transfers between devices with their start and end apart: 9 -> 13, of which waited for: 8 -> 6; matrix products, arithmetic and copies ran while one was open for 1% -> 1% of each run, Pallas kernels for 0% -> 0%
where the time goes in v7:
time: 212 us; the launch traced here: 208 us
  starting transfers between devices  63.6 us (30%)
  waiting for transfers between devices  58.5 us (28%)
  blocking collectives  56 us (26%)
  Pallas kernels  15.3 us (7%)
  local copies, waits for them, and re-layouts  7.35 us (3%)
  matrix products  4.32 us (2%)
    ppermute x8, starting transfers between devices, spread(): out.append(lax.ppermute(part, 'tp', pairs))  26.1 us
    all_to_all x1, blocking collectives, in_plane(): return lax.all_to_all(x, PLANE, 0, 0, tiled=True)  23.8 us
    ppermute x8, waiting for transfers between devices, spread(): out.append(lax.ppermute(part, 'tp', pairs))  19.2 us
    all_to_all x2, waiting for transfers between devices, along_z(): out = lax.all_to_all(x.reshape(chips, 2, width), Z, 0, 0, tiled=True)  15.4 us
    all_to_all x1, waiting for transfers between devices, entering(): far = lax.all_to_all(far, Z, 0, 0, tiled=True)  14.1 us
    all_to_all x2, starting transfers between devices, along_z(): out = lax.all_to_all(x.reshape(chips, 2, width), Z, 0, 0, tiled=True)  13.4 us
    all_to_all x1, blocking collectives, copy_for_each(): lax.all_to_all(jnp.broadcast_to(x[None], (length, *x.shape)), axis, 0, 0,...  13 us
    all_gather x1, blocking collectives, entering(): near = lax.all_gather(own, ('zl', 'c')).astype(jnp.float32)  12.5 us
  transfers between devices with their start and end apart: 13, of which 6 were waited for; matrix products, arithmetic and copies ran while one was open for 1% of the time, Pallas kernels for 0%

profile of v7, /device:TPU:1, one launch (start us, length us, event | category | flops | bytes accessed | tf_op | source)
XLA Modules:
  0.0 208.2 jit_solution(1950108502774158149)
XLA Ops:
  0.7 6.5 %local_span.1 = (bf16[256,128]{1,0:T(8,128)(2,1)S(1)}, f32[128,128]{1,0:T(8,128)S(1)}, f32[128,128]{1,0:T(8,128)S(1)}, bf16[3072,128]{1,0:T(8,128)(2,1)}, bf16[3...) custom-call(bf16[128,128]{1,0:T(8,128)(2,1)} %q_ref.1, ...), custom_call_target="tpu_custom_call" | custom-call | tf_op jit(solution)/shard_map/local_span/pallas_call | solution.py:288
  7.3 12.5 %all-gather = bf16[1024,128]{1,0:T(8,128)(2,1)S(1)} all-gather(bf16[256,128]{1,0:T(8,128)(2,1)S(1)} %get-tuple-element.28), channel_id=2, replica_groups=mesh['zh'=8,'zl'=2,'c'=2,'tp'=16] {'zl','c'}, dimensions={0}, use_global_device_ids=true | all-gather | bytes 327680 | tf_op jit(solution)/shard_map/all_gather | solution.py:82
  21.6 9.6 %all-to-all-start = ((bf16[16,64,128]{2,1,0:T(8,128)(2,1)}), bf16[16,64,128]{2,1,0:T(8,128)(2,1)S(1)}, u32[]{:S(2)}, u32[]{:S(2)}) async-start(bf16[16,64,128]{2,1,0:T(8,128)(2,1)} %broadcast_in_dim.6), calls=%async_computation | async-start | bytes 524288 | tf_op jit(solution)/shard_map/all_to_all | solution.py:99
  31.2 14.1 %all-to-all-done = bf16[16,64,128]{2,1,0:T(8,128)(2,1)S(1)} async-done(((bf16[16,64,128]{2,1,0:T(8,128)(2,1)}), bf16[16,64,128]{2,1,0:T(8,128)(2,1)S(1)}, u32[]{:S(2)}, u32[]{:S(2)}) %all-to-all-start) | async-done | bytes 262176 | tf_op jit(solution)/shard_map/all_to_all | solution.py:99
  45.3 6.8 %all-gather.1 = bf16[32,64,128]{2,1,0:T(8,128)(2,1)S(1)} all-gather(bf16[16,64,128]{2,1,0:T(8,128)(2,1)S(1)} %all-to-all-done), channel_id=3, replica_groups=mesh['zh'=8,'zl'=2,'c'=2,'tp'=16] {'c'}, dimensions={0}, use_global_device_ids=true | all-gather | bytes 786432 | tf_op jit(solution)/shard_map/all_gather | solution.py:100
  54.2 1.1 fusion
  55.3 6.8 %all-to-all-start.1 = ((bf16[16,8,2048]{2,1,0:T(8,128)(2,1)}), bf16[16,8,2048]{2,1,0:T(8,128)(2,1)S(1)}, u32[]{:S(2)}, u32[]{:S(2)}) async-start(bf16[16,8,2048]{2,1,0:T(8,128)(2,1)} %fusion), calls=%async_computation.1 | async-start | bytes 1048576 | tf_op jit(solution)/shard_map/all_to_all | solution.py:117
  62.1 0.8 constant_dynamic-slice_fusion.2
  63.0 9.8 %all-to-all-done.1 = bf16[16,8,2048]{2,1,0:T(8,128)(2,1)S(1)} async-done(((bf16[16,8,2048]{2,1,0:T(8,128)(2,1)}), bf16[16,8,2048]{2,1,0:T(8,128)(2,1)S(1)}, u32[]{:S(2)}, u32[]{:S(2)}) %all-to-all-start.1) | async-done | bytes 524320 | tf_op jit(solution)/shard_map/all_to_all | solution.py:117
  73.6 0.8 reshape.119
  74.3 5.7 %all-to-all-start.2 = ((bf16[16,2,2048]{2,1,0:T(2,128)(2,1)}), bf16[16,2,2048]{2,1,0:T(2,128)(2,1)S(1)}, u32[]{:S(2)}, u32[]{:S(2)}) async-start(bf16[16,2,2048]{2,1,0:T(2,128)(2,1)} %reshape.119), calls=%async_computation.2 | async-start | bytes 262144 | tf_op jit(solution)/shard_map/all_to_all | solution.py:327
  80.0 2.2 %collective-permute-start = (bf16[3072,128]{1,0:T(8,128)(2,1)}, bf16[3072,128]{1,0:T(8,128)(2,1)S(1)}, u32[]{:S(2)}, u32[]{:S(2)}) collective-permute-start(bf16[3072,128]{1,0:T(8,128)(2,1)} %get-tuple-element.39), channel_id=1, source_target_pairs={{0,1},{1,2},{2,3},{3,0},{4,5},{5,6},{6,7},{7,4},{8,9},{9,10},{10,1... | collective-permute-start | bytes 2359304 | tf_op jit(solution)/shard_map/ppermute | solution.py:75
  82.2 4.3 %collective-permute-start.1 = (bf16[3072,128]{1,0:T(8,128)(2,1)}, bf16[3072,128]{1,0:T(8,128)(2,1)S(1)}, u32[]{:S(2)}, u32[]{:S(2)}) collective-permute-start(bf16[3072,128]{1,0:T(8,128)(2,1)} %get-tuple-element.40), channel_id=1, source_target_pairs={{0,3},{1,0},{2,1},{3,2},{4,7},{5,4},{6,5},{7,6},{8,11},{9,8},{10,9... | collective-permute-start | bytes 2359304 | tf_op jit(solution)/shard_map/ppermute | solution.py:75
  86.5 1.9 collective-permute-start.2
  88.5 3.5 %all-to-all-done.2 = bf16[16,2,2048]{2,1,0:T(2,128)(2,1)S(1)} async-done(((bf16[16,2,2048]{2,1,0:T(2,128)(2,1)}), bf16[16,2,2048]{2,1,0:T(2,128)(2,1)S(1)}, u32[]{:S(2)}, u32[]{:S(2)}) %all-to-all-start.2) | async-done | bytes 131104 | tf_op jit(solution)/shard_map/all_to_all | solution.py:327
  92.6 1.1 broadcast_in_dim.7
  93.7 7.7 %all-to-all-start.3 = ((bf16[32,8,2048]{2,1,0:T(8,128)(2,1)}), bf16[32,8,2048]{2,1,0:T(8,128)(2,1)S(1)}, u32[]{:S(2)}, u32[]{:S(2)}) async-start(bf16[32,8,2048]{2,1,0:T(8,128)(2,1)} %bitcast.36), calls=%async_computation.3 | async-start | bytes 2097152 | tf_op jit(solution)/shard_map/all_to_all | solution.py:331
  101.4 4.6 %collective-permute-start.3 = (bf16[3072,128]{1,0:T(8,128)(2,1)}, bf16[3072,128]{1,0:T(8,128)(2,1)S(1)}, u32[]{:S(2)}, u32[]{:S(2)}) collective-permute-start(bf16[3072,128]{1,0:T(8,128)(2,1)} %get-tuple-element.42), channel_id=1, source_target_pairs={{0,12},{1,13},{2,14},{3,15},{4,0},{5,1},{6,2},{7,3},{8,4},{9,5},{1... | collective-permute-start | bytes 2359304 | tf_op jit(solution)/shard_map/ppermute | solution.py:75
  105.9 3.1 %collective-permute-start.4 = (bf16[1536,128]{1,0:T(8,128)(2,1)}, bf16[1536,128]{1,0:T(8,128)(2,1)S(1)}, u32[]{:S(2)}, u32[]{:S(2)}) collective-permute-start(bf16[1536,128]{1,0:T(8,128)(2,1)} %get-tuple-element.43), channel_id=1, source_target_pairs={{0,1},{1,2},{2,3},{3,0},{4,5},{5,6},{6,7},{7,4},{8,9},{9,10},{10,1... | collective-permute-start | bytes 1179656 | tf_op jit(solution)/shard_map/ppermute | solution.py:75
  109.1 3.4 %collective-permute-start.5 = (bf16[1536,128]{1,0:T(8,128)(2,1)}, bf16[1536,128]{1,0:T(8,128)(2,1)S(1)}, u32[]{:S(2)}, u32[]{:S(2)}) collective-permute-start(bf16[1536,128]{1,0:T(8,128)(2,1)} %get-tuple-element.44), channel_id=1, source_target_pairs={{0,3},{1,0},{2,1},{3,2},{4,7},{5,4},{6,5},{7,6},{8,11},{9,8},{10,9... | collective-permute-start | bytes 1179656 | tf_op jit(solution)/shard_map/ppermute | solution.py:75
  112.5 1.9 collective-permute-start.6
  114.4 4.8 %collective-permute-start.7 = (bf16[1536,128]{1,0:T(8,128)(2,1)}, bf16[1536,128]{1,0:T(8,128)(2,1)}, u32[]{:S(2)}, u32[]{:S(2)}) collective-permute-start(bf16[1536,128]{1,0:T(8,128)(2,1)} %get-tuple-element.46), channel_id=1, source_target_pairs={{0,12},{1,13},{2,14},{3,15},{4,0},{5,1},{6,2},{7,3},{8,4},{9,5},{1... | collective-permute-start | bytes 1179656 | tf_op jit(solution)/shard_map/ppermute | solution.py:75
  119.2 12.5 %collective-permute-done.3.refs_6_ = bf16[3072,128]{1,0:T(8,128)(2,1)S(1)} collective-permute-done((bf16[3072,128]{1,0:T(8,128)(2,1)}, bf16[3072,128]{1,0:T(8,128)(2,1)S(1)}, u32[]{:S(2)}, u32[]{:S(2)}) %collective-permute-start.3) | collective-permute-done | bytes 786464 | tf_op jit(solution)/shard_map/ppermute | solution.py:75
  131.8 0.9 copy-done.3
  133.7 6.6 %collective-permute-done.7.refs_10_ = bf16[1536,128]{1,0:T(8,128)(2,1)} collective-permute-done((bf16[1536,128]{1,0:T(8,128)(2,1)}, bf16[1536,128]{1,0:T(8,128)(2,1)}, u32[]{:S(2)}, u32[]{:S(2)}) %collective-permute-start.7) | collective-permute-done | bytes 393248 | tf_op jit(solution)/shard_map/ppermute | solution.py:75
  140.3 8.7 %run_experts.1 = bf16[256,2048]{1,0:T(8,128)(2,1)S(1)} custom-call(bf16[256,2048]{1,0:T(8,128)(2,1)S(1)} %bitcast.159, bf16[2048,384]{1,0:T(8,128)(2,1)} %bitcast.162, bf16[2048,384]{1,0:T(8,128)(2,1)} %bitcast.164, bf16[384,2048]{1,0:T(8,128)(2,1)} %bitcast.166, bf16[3072,128]{1,0:T(8,128)(2,1)} %copy-done.1, bf16[3072,128]{1,0:T(8,128)(2,1)} %copy-done.2, ...), custom_call_target="tpu_custom_call" | custom-call | tf_op jit(solution)/shard_map/run_experts/pallas_call | solution.py:343
  149.0 23.8 %all_to_all.35 = bf16[32,8,2048]{2,1,0:T(8,128)(2,1)S(1)} all-to-all(bf16[32,8,2048]{2,1,0:T(8,128)(2,1)S(1)} %bitcast.160), channel_id=1, replica_groups=mesh['zh'=8,'zl'=2,'c'=2,'tp'=16] {'c','tp'}, dimensions={0} | all-to-all | bytes 2097152 | tf_op jit(solution)/shard_map/all_to_all | solution.py:331
  173.0 0.8 copy.41
  173.8 7.7 %all-to-all-start.5 = ((bf16[16,2,2048]{2,1,0:T(2,128)(2,1)}), bf16[16,2,2048]{2,1,0:T(2,128)(2,1)S(1)}, u32[]{:S(2)}, u32[]{:S(2)}) async-start(bf16[16,2,2048]{2,1,0:T(2,128)(2,1)} %copy.41), calls=%async_computation.5 | async-start | bytes 262144 | tf_op jit(solution)/shard_map/all_to_all | solution.py:327
  181.7 11.9 %all-to-all-done.5 = bf16[16,2,2048]{2,1,0:T(2,128)(2,1)S(1)} async-done(((bf16[16,2,2048]{2,1,0:T(2,128)(2,1)}), bf16[16,2,2048]{2,1,0:T(2,128)(2,1)S(1)}, u32[]{:S(2)}, u32[]{:S(2)}) %all-to-all-start.5) | async-done | bytes 131104 | tf_op jit(solution)/shard_map/all_to_all | solution.py:327
  194.3 13.0 %all_to_all.36 = bf16[16,8,2048]{2,1,0:T(8,128)(2,1)S(1)} all-to-all(bf16[16,8,2048]{2,1,0:T(8,128)(2,1)S(1)} %broadcast_in_dim.8), channel_id=1, replica_groups=mesh['zh'=8,'zl'=2,'c'=2,'tp'=16] {'tp'}, dimensions={0} | all-to-all | bytes 1048576 | tf_op jit(solution)/shard_map/all_to_all | solution.py:123
  207.4 0.8 copy.48
  (78 shorter events, 7.3 us)
Async XLA Ops:
  0.0 54.2 %copy-start = (bf16[128,2048]{1,0:T(8,128)(2,1)S(1)}, bf16[128,2048]{1,0:T(8,128)(2,1)}, u32[]{:S(2)}) copy-start(bf16[128,2048]{1,0:T(8,128)(2,1)} %param.26) | copy-start | bytes 1572868
  21.6 23.7 %all-to-all-start = ((bf16[16,64,128]{2,1,0:T(8,128)(2,1)}), bf16[16,64,128]{2,1,0:T(8,128)(2,1)S(1)}, u32[]{:S(2)}, u32[]{:S(2)}) async-start(bf16[16,64,128]{2,1,0:T(8,128)(2,1)} %broadcast_in_dim.6), calls=%async_computation | async-start | bytes 524288 | tf_op jit(solution)/shard_map/all_to_all | solution.py:99
  52.2 2.0 copy-start.7
  52.2 2.0 copy-start.12
  53.4 9.4 %copy-start.10 = (s32[128,2]{0,1:T(2,128)S(1)}, s32[128,2]{0,1:T(2,128)}, u32[]{:S(2)}) copy-start(s32[128,2]{0,1:T(2,128)} %param.29) | copy-start | bytes 3076
  54.1 19.1 %copy-start.8 = (f32[2048]{0:T(1024)S(1)}, f32[2048]{0:T(1024)}, u32[]{:S(2)}) copy-start(f32[2048]{0:T(1024)} %param.27) | copy-start | bytes 24580
  55.3 17.5 %all-to-all-start.1 = ((bf16[16,8,2048]{2,1,0:T(8,128)(2,1)}), bf16[16,8,2048]{2,1,0:T(8,128)(2,1)S(1)}, u32[]{:S(2)}, u32[]{:S(2)}) async-start(bf16[16,8,2048]{2,1,0:T(8,128)(2,1)} %fusion), calls=%async_computation.1 | async-start | bytes 1048576 | tf_op jit(solution)/shard_map/all_to_all | solution.py:117
  74.3 17.7 %all-to-all-start.2 = ((bf16[16,2,2048]{2,1,0:T(2,128)(2,1)}), bf16[16,2,2048]{2,1,0:T(2,128)(2,1)S(1)}, u32[]{:S(2)}, u32[]{:S(2)}) async-start(bf16[16,2,2048]{2,1,0:T(2,128)(2,1)} %reshape.119), calls=%async_computation.2 | async-start | bytes 262144 | tf_op jit(solution)/shard_map/all_to_all | solution.py:327
  80.0 29.0 %collective-permute-start = (bf16[3072,128]{1,0:T(8,128)(2,1)}, bf16[3072,128]{1,0:T(8,128)(2,1)S(1)}, u32[]{:S(2)}, u32[]{:S(2)}) collective-permute-start(bf16[3072,128]{1,0:T(8,128)(2,1)} %get-tuple-element.39), channel_id=1, source_target_pairs={{0,1},{1,2},{2,3},{3,0},{4,5},{5,6},{6,7},{7,4},{8,9},{9,10},{10,1... | collective-permute-start | bytes 2359304 | tf_op jit(solution)/shard_map/ppermute | solution.py:75
  82.2 30.2 %collective-permute-start.1 = (bf16[3072,128]{1,0:T(8,128)(2,1)}, bf16[3072,128]{1,0:T(8,128)(2,1)S(1)}, u32[]{:S(2)}, u32[]{:S(2)}) collective-permute-start(bf16[3072,128]{1,0:T(8,128)(2,1)} %get-tuple-element.40), channel_id=1, source_target_pairs={{0,3},{1,0},{2,1},{3,2},{4,7},{5,4},{6,5},{7,6},{8,11},{9,8},{10,9... | collective-permute-start | bytes 2359304 | tf_op jit(solution)/shard_map/ppermute | solution.py:75
  86.5 27.9 %collective-permute-start.2 = (bf16[3072,128]{1,0:T(8,128)(2,1)}, bf16[3072,128]{1,0:T(8,128)(2,1)}, u32[]{:S(2)}, u32[]{:S(2)}) collective-permute-start(bf16[3072,128]{1,0:T(8,128)(2,1)} %get-tuple-element.41), channel_id=1, source_target_pairs={{0,4},{1,5},{2,6},{3,7},{4,8},{5,9},{6,10},{7,11},{8,12},{9,13},{1... | collective-permute-start | bytes 2359304 | tf_op jit(solution)/shard_map/ppermute | solution.py:75
  93.7 46.6 %all-to-all-start.3 = ((bf16[32,8,2048]{2,1,0:T(8,128)(2,1)}), bf16[32,8,2048]{2,1,0:T(8,128)(2,1)S(1)}, u32[]{:S(2)}, u32[]{:S(2)}) async-start(bf16[32,8,2048]{2,1,0:T(8,128)(2,1)} %bitcast.36), calls=%async_computation.3 | async-start | bytes 2097152 | tf_op jit(solution)/shard_map/all_to_all | solution.py:331
  101.4 30.3 %collective-permute-start.3 = (bf16[3072,128]{1,0:T(8,128)(2,1)}, bf16[3072,128]{1,0:T(8,128)(2,1)S(1)}, u32[]{:S(2)}, u32[]{:S(2)}) collective-permute-start(bf16[3072,128]{1,0:T(8,128)(2,1)} %get-tuple-element.42), channel_id=1, source_target_pairs={{0,12},{1,13},{2,14},{3,15},{4,0},{5,1},{6,2},{7,3},{8,4},{9,5},{1... | collective-permute-start | bytes 2359304 | tf_op jit(solution)/shard_map/ppermute | solution.py:75
  105.9 25.8 %collective-permute-start.4 = (bf16[1536,128]{1,0:T(8,128)(2,1)}, bf16[1536,128]{1,0:T(8,128)(2,1)S(1)}, u32[]{:S(2)}, u32[]{:S(2)}) collective-permute-start(bf16[1536,128]{1,0:T(8,128)(2,1)} %get-tuple-element.43), channel_id=1, source_target_pairs={{0,1},{1,2},{2,3},{3,0},{4,5},{5,6},{6,7},{7,4},{8,9},{9,10},{10,1... | collective-permute-start | bytes 1179656 | tf_op jit(solution)/shard_map/ppermute | solution.py:75
  109.1 31.2 %copy-start.1 = (bf16[3072,128]{1,0:T(8,128)(2,1)}, bf16[3072,128]{1,0:T(8,128)(2,1)S(1)}, u32[]{:S(2)}) copy-start(bf16[3072,128]{1,0:T(8,128)(2,1)S(1)} %collective-permute-done.refs_3_) | copy-start | bytes 2359300
  109.1 22.7 %collective-permute-start.5 = (bf16[1536,128]{1,0:T(8,128)(2,1)}, bf16[1536,128]{1,0:T(8,128)(2,1)S(1)}, u32[]{:S(2)}, u32[]{:S(2)}) collective-permute-start(bf16[1536,128]{1,0:T(8,128)(2,1)} %get-tuple-element.44), channel_id=1, source_target_pairs={{0,3},{1,0},{2,1},{3,2},{4,7},{5,4},{6,5},{7,6},{8,11},{9,8},{10,9... | collective-permute-start | bytes 1179656 | tf_op jit(solution)/shard_map/ppermute | solution.py:75
  112.5 27.8 %copy-start.2 = (bf16[3072,128]{1,0:T(8,128)(2,1)}, bf16[3072,128]{1,0:T(8,128)(2,1)S(1)}, u32[]{:S(2)}) copy-start(bf16[3072,128]{1,0:T(8,128)(2,1)S(1)} %collective-permute-done.1.refs_4_) | copy-start | bytes 2359300
  112.5 19.3 %collective-permute-start.6 = (bf16[1536,128]{1,0:T(8,128)(2,1)}, bf16[1536,128]{1,0:T(8,128)(2,1)S(1)}, u32[]{:S(2)}, u32[]{:S(2)}) collective-permute-start(bf16[1536,128]{1,0:T(8,128)(2,1)} %get-tuple-element.45), channel_id=1, source_target_pairs={{0,4},{1,5},{2,6},{3,7},{4,8},{5,9},{6,10},{7,11},{8,12},{9,13},{1... | collective-permute-start | bytes 1179656 | tf_op jit(solution)/shard_map/ppermute | solution.py:75
  114.4 25.8 %collective-permute-start.7 = (bf16[1536,128]{1,0:T(8,128)(2,1)}, bf16[1536,128]{1,0:T(8,128)(2,1)}, u32[]{:S(2)}, u32[]{:S(2)}) collective-permute-start(bf16[1536,128]{1,0:T(8,128)(2,1)} %get-tuple-element.46), channel_id=1, source_target_pairs={{0,12},{1,13},{2,14},{3,15},{4,0},{5,1},{6,2},{7,3},{8,4},{9,5},{1... | collective-permute-start | bytes 1179656 | tf_op jit(solution)/shard_map/ppermute | solution.py:75
  131.7 0.9 copy-start.3
  131.7 1.0 copy-start.4
  131.7 1.1 copy-start.5
  132.9 0.8 copy-start.6
  172.8 8.8 %copy-start.11 = (f32[128,2]{0,1:T(2,128)S(1)}, f32[128,2]{0,1:T(2,128)}, u32[]{:S(2)}) copy-start(f32[128,2]{0,1:T(2,128)} %param.30) | copy-start | bytes 3076
  172.8 21.4 %copy-start.9 = (f32[2048]{0:T(1024)S(1)}, f32[2048]{0:T(1024)}, u32[]{:S(2)}) copy-start(f32[2048]{0:T(1024)} %param.28) | copy-start | bytes 24580
  173.8 19.7 %all-to-all-start.5 = ((bf16[16,2,2048]{2,1,0:T(2,128)(2,1)}), bf16[16,2,2048]{2,1,0:T(2,128)(2,1)S(1)}, u32[]{:S(2)}, u32[]{:S(2)}) async-start(bf16[16,2,2048]{2,1,0:T(2,128)(2,1)} %copy.41), calls=%async_computation.5 | async-start | bytes 262144 | tf_op jit(solution)/shard_map/all_to_all | solution.py:327

commit v8 on v7

--- a/solution.py
+++ b/solution.py
@@ -56,17 +56,18 @@
         for part, buf in enumerate(bufs):
             row = block * size
             buf[row : row + half] = parts[:, part * LANES : (part + 1) * LANES]
-            last = row == early
-            out = outs[part + 4] if last else outs[part].at[pl.ds(row, size)]
+            late = row == early and part > 1
+            out = outs[part + 2] if late else outs[part].at[pl.ds(row, size)]
             copies.append(pltpu.make_async_copy(buf.at[pl.ds(row, size)], out, sems.at[len(copies)]))
             copies[-1].start()
     for copy in copies:
         copy.wait()
 
 
-def spread(parts, side):
+def spread(parts, side, start=0):
     out = []
-    for part, (dy, dx) in zip(parts, ((0, 1), (0, side - 1), (1, 0), (side - 1, 0))):
+    ways = ((0, 1), (0, side - 1), (1, 0), (side - 1, 0))
+    for part, (dy, dx) in zip(parts, ways[start:]):
         pairs = [
             (y * side + x, (y + dy) % side * side + (x + dx) % side)
             for y in range(side)
@@ -140,8 +141,8 @@
 
 
 def local_span(q_ref, k_ref, v_ref, beta_ref, decay_ref, rate_ref, *refs):
-    tables, (both_ref, mix_ref, out_ref), outs = refs[:3], refs[3:6], refs[6:14]
-    bufs, part_bufs, sems = refs[14:17], refs[17:21], refs[21]
+    tables, (both_ref, mix_ref, out_ref), outs = refs[:3], refs[3:6], refs[6:12]
+    bufs, part_bufs, sems = refs[12:15], refs[15:19], refs[19]
     copies = [pltpu.make_async_copy(x, y, sems.at[k]) for k, (x, y) in enumerate(zip(tables, bufs))]
     for copy in copies:
         copy.start()
@@ -204,8 +205,10 @@
 
 
 def run_experts(rows_ref, *refs):
-    out_ref, bufs, sems = refs[11], refs[12:23], refs[23]
-    copies = [pltpu.make_async_copy(refs[k], bufs[k], sems.at[k]) for k in range(11)]
+    out_ref, bufs, sems = refs[9], refs[10:19], refs[19]
+    copies = [pltpu.make_async_copy(refs[k], bufs[k], sems.at[k]) for k in range(9)]
+    for copy in (*copies[:2], *copies[3:], copies[2]):
+        copy.start()
     gate_ref, up_ref, down_ref = bufs[:3]
     rows = rows_ref[...]
     width = rows.shape[1]
@@ -215,26 +218,22 @@
     def dot(a, b):
         return jnp.dot(a, b, preferred_element_type=jnp.float32)
 
-    copies[0].start()
-    copies[1].start()
     copies[0].wait()
-    for k in range(3, 11):
-        copies[k].start()
     gate = dot(rows, gate_ref[...])
     copies[1].wait()
-    copies[2].start()
     inner = (jax.nn.silu(gate) * dot(rows, up_ref[...])).astype(jnp.bfloat16)
     place = lax.broadcasted_iota(jnp.int32, (rows.shape[0], LANES), 1) // lanes
     arrived = [jnp.zeros((rows.shape[0], LANES), jnp.float32)] * blocks
 
     def run(part, block, first, count):
-        last = block == blocks - 1
-        ref, row = (bufs[7 + part], first) if last else (bufs[3 + part], block * size + first)
+        late = block == blocks - 1 and part > 1
+        ref, row = (bufs[5 + part], first) if late else (bufs[3 + part], block * size + first)
         return ref[row : row + count]
 
     for part in range(4):
         copies[3 + part].wait()
-        copies[7 + part].wait()
+        if part > 1:
+            copies[5 + part].wait()
         table = jnp.concatenate([run(part, k, 0, half) for k in range(blocks)], 1)
         low, high = (dot(rows[:, :half], table), dot(rows[:, half:], table))
         for k in range(blocks):
@@ -292,10 +291,11 @@
             pltpu.VMEM((length, HEAD_FEATURES), jnp.float32),
             pltpu.VMEM((length, HEAD_FEATURES), jnp.float32),
         )
-        + (jax.ShapeDtypeStruct((packed[0] - packed[0] // 3, LANES), jnp.bfloat16),) * 4
-        + (jax.ShapeDtypeStruct((packed[0] // 3, LANES), jnp.bfloat16),) * 4,
+        + (jax.ShapeDtypeStruct(packed, jnp.bfloat16),) * 2
+        + (jax.ShapeDtypeStruct((packed[0] - packed[0] // 3, LANES), jnp.bfloat16),) * 2
+        + (jax.ShapeDtypeStruct((packed[0] // 3, LANES), jnp.bfloat16),) * 2,
         in_specs=[vmem] * 5 + [pl.BlockSpec(memory_space=pltpu.SMEM)] + [anywhere] * 3,
-        out_specs=(vmem,) * 3 + (anywhere,) * 8,
+        out_specs=(vmem,) * 3 + (anywhere,) * 6,
         scratch_shapes=[pltpu.VMEM(x.shape, x.dtype) for x in tables]
         + [pltpu.VMEM(packed, jnp.bfloat16)] * 4
         + [pltpu.SemaphoreType.DMA((15,))],
@@ -332,7 +332,7 @@
 
     half = chips // 2
     send, late = lax.optimization_barrier((send, parts[4:]))
-    late = spread(late, side)
+    late = spread(late, side, 2)
     arrived = along_z(send)
     arrived = arrived.transpose(1, 0, 2).reshape(2, 2, half, width)
     swapped = arrived[:, ::-1]
@@ -343,10 +343,10 @@
     partial_value = pl.pallas_call(
         run_experts,
         out_shape=pltpu.VMEM(piece.shape, jnp.bfloat16),
-        in_specs=[vmem] + [anywhere] * 11,
+        in_specs=[vmem] + [anywhere] * 9,
         out_specs=vmem,
         scratch_shapes=[pltpu.VMEM(x.shape, x.dtype) for x in tables]
-        + [pltpu.SemaphoreType.DMA((11,))],
+        + [pltpu.SemaphoreType.DMA((9,))],
         name="run_experts",
     )(held(piece), *tables)
     shares = in_plane(partial_value.reshape(2 * split_count, half, width))

time: 212 us -> 212 us (level)
  waiting for transfers between devices: 58.5 us -> 66.1 us
  starting transfers between devices: 63.6 us -> 57.2 us
    ppermute x8 -> x6, waiting for transfers between devices: 19.2 us -> 26.8 us  [spread(): out.append(lax.ppermute(part, 'tp', pairs))]
    ppermute x8 -> x6, starting transfers between devices: 26.1 us -> 19.6 us  [spread(): out.append(lax.ppermute(part, 'tp', pairs))]
  transfers between devices with their start and end apart: 13 -> 11, of which waited for: 6 -> 6; matrix products, arithmetic and copies ran while one was open for 1% -> 1% of each run, Pallas kernels for 0% -> 0%
where the time goes in v8:
time: 212 us; the launch traced here: 208 us
  waiting for transfers between devices  66.1 us (31%)
  starting transfers between devices  57.2 us (27%)
  blocking collectives  56.6 us (27%)
  Pallas kernels  14.6 us (7%)
  local copies, waits for them, and re-layouts  6.32 us (3%)
  matrix products  4.32 us (2%)
    ppermute x6, waiting for transfers between devices, spread(): out.append(lax.ppermute(part, 'tp', pairs))  26.8 us
    all_to_all x1, blocking collectives, in_plane(): return lax.all_to_all(x, PLANE, 0, 0, tiled=True)  24.4 us
    ppermute x6, starting transfers between devices, spread(): out.append(lax.ppermute(part, 'tp', pairs))  19.6 us
    all_to_all x2, waiting for transfers between devices, along_z(): out = lax.all_to_all(x.reshape(chips, 2, width), Z, 0, 0, tiled=True)  15.4 us
    all_to_all x1, waiting for transfers between devices, entering(): far = lax.all_to_all(far, Z, 0, 0, tiled=True)  14.1 us
    all_to_all x2, starting transfers between devices, along_z(): out = lax.all_to_all(x.reshape(chips, 2, width), Z, 0, 0, tiled=True)  13.5 us
    all_to_all x1, blocking collectives, copy_for_each(): lax.all_to_all(jnp.broadcast_to(x[None], (length, *x.shape)), axis, 0, 0,...  13 us
    all_gather x1, blocking collectives, entering(): near = lax.all_gather(own, ('zl', 'c')).astype(jnp.float32)  12.5 us
  transfers between devices with their start and end apart: 11, of which 6 were waited for; matrix products, arithmetic and copies ran while one was open for 1% of the time, Pallas kernels for 0%

profile of v8, /device:TPU:1, one launch (start us, length us, event | category | flops | bytes accessed | tf_op | source)
XLA Modules:
  0.0 208.2 jit_solution(15556829238315215160)
XLA Ops:
  0.7 6.5 %local_span.1 = (bf16[256,128]{1,0:T(8,128)(2,1)S(1)}, f32[128,128]{1,0:T(8,128)S(1)}, f32[128,128]{1,0:T(8,128)S(1)}, bf16[4608,128]{1,0:T(8,128)(2,1)}, bf16[4...) custom-call(bf16[128,128]{1,0:T(8,128)(2,1)} %q_ref.1, ...), custom_call_target="tpu_custom_call" | custom-call | tf_op jit(solution)/shard_map/local_span/pallas_call | solution.py:287
  7.2 12.5 %all-gather = bf16[1024,128]{1,0:T(8,128)(2,1)S(1)} all-gather(bf16[256,128]{1,0:T(8,128)(2,1)S(1)} %get-tuple-element.24), channel_id=2, replica_groups=mesh['zh'=8,'zl'=2,'c'=2,'tp'=16] {'zl','c'}, dimensions={0}, use_global_device_ids=true | all-gather | bytes 327680 | tf_op jit(solution)/shard_map/all_gather | solution.py:83
  20.8 0.8 broadcast_in_dim.6
  21.6 9.6 %all-to-all-start = ((bf16[16,64,128]{2,1,0:T(8,128)(2,1)}), bf16[16,64,128]{2,1,0:T(8,128)(2,1)S(1)}, u32[]{:S(2)}, u32[]{:S(2)}) async-start(bf16[16,64,128]{2,1,0:T(8,128)(2,1)} %broadcast_in_dim.6), calls=%async_computation | async-start | bytes 524288 | tf_op jit(solution)/shard_map/all_to_all | solution.py:100
  31.2 14.1 %all-to-all-done = bf16[16,64,128]{2,1,0:T(8,128)(2,1)S(1)} async-done(((bf16[16,64,128]{2,1,0:T(8,128)(2,1)}), bf16[16,64,128]{2,1,0:T(8,128)(2,1)S(1)}, u32[]{:S(2)}, u32[]{:S(2)}) %all-to-all-start) | async-done | bytes 262176 | tf_op jit(solution)/shard_map/all_to_all | solution.py:100
  45.3 6.8 %all-gather.1 = bf16[32,64,128]{2,1,0:T(8,128)(2,1)S(1)} all-gather(bf16[16,64,128]{2,1,0:T(8,128)(2,1)S(1)} %all-to-all-done), channel_id=3, replica_groups=mesh['zh'=8,'zl'=2,'c'=2,'tp'=16] {'c'}, dimensions={0}, use_global_device_ids=true | all-gather | bytes 786432 | tf_op jit(solution)/shard_map/all_gather | solution.py:101
  54.1 1.1 fusion
  55.3 6.8 %all-to-all-start.1 = ((bf16[16,8,2048]{2,1,0:T(8,128)(2,1)}), bf16[16,8,2048]{2,1,0:T(8,128)(2,1)S(1)}, u32[]{:S(2)}, u32[]{:S(2)}) async-start(bf16[16,8,2048]{2,1,0:T(8,128)(2,1)} %fusion), calls=%async_computation.1 | async-start | bytes 1048576 | tf_op jit(solution)/shard_map/all_to_all | solution.py:118
  62.0 0.8 constant_dynamic-slice_fusion.2
  63.0 9.8 %all-to-all-done.1 = bf16[16,8,2048]{2,1,0:T(8,128)(2,1)S(1)} async-done(((bf16[16,8,2048]{2,1,0:T(8,128)(2,1)}), bf16[16,8,2048]{2,1,0:T(8,128)(2,1)S(1)}, u32[]{:S(2)}, u32[]{:S(2)}) %all-to-all-start.1) | async-done | bytes 524320 | tf_op jit(solution)/shard_map/all_to_all | solution.py:118
  73.5 0.8 reshape.119
  74.3 5.7 %all-to-all-start.2 = ((bf16[16,2,2048]{2,1,0:T(2,128)(2,1)}), bf16[16,2,2048]{2,1,0:T(2,128)(2,1)S(1)}, u32[]{:S(2)}, u32[]{:S(2)}) async-start(bf16[16,2,2048]{2,1,0:T(2,128)(2,1)} %reshape.119), calls=%async_computation.2 | async-start | bytes 262144 | tf_op jit(solution)/shard_map/all_to_all | solution.py:327
  80.0 2.2 %collective-permute-start = (bf16[4608,128]{1,0:T(8,128)(2,1)}, bf16[4608,128]{1,0:T(8,128)(2,1)}, u32[]{:S(2)}, u32[]{:S(2)}) collective-permute-start(bf16[4608,128]{1,0:T(8,128)(2,1)} %get-tuple-element.33), channel_id=1, source_target_pairs={{0,1},{1,2},{2,3},{3,0},{4,5},{5,6},{6,7},{7,4},{8,9},{9,10},{10,1... | collective-permute-start | bytes 3538952 | tf_op jit(solution)/shard_map/ppermute | solution.py:76
  82.2 4.3 %collective-permute-start.1 = (bf16[4608,128]{1,0:T(8,128)(2,1)}, bf16[4608,128]{1,0:T(8,128)(2,1)}, u32[]{:S(2)}, u32[]{:S(2)}) collective-permute-start(bf16[4608,128]{1,0:T(8,128)(2,1)} %get-tuple-element.34), channel_id=1, source_target_pairs={{0,3},{1,0},{2,1},{3,2},{4,7},{5,4},{6,5},{7,6},{8,11},{9,8},{10,9... | collective-permute-start | bytes 3538952 | tf_op jit(solution)/shard_map/ppermute | solution.py:76
  86.5 1.9 collective-permute-start.2
  88.4 3.5 %all-to-all-done.2 = bf16[16,2,2048]{2,1,0:T(2,128)(2,1)S(1)} async-done(((bf16[16,2,2048]{2,1,0:T(2,128)(2,1)}), bf16[16,2,2048]{2,1,0:T(2,128)(2,1)S(1)}, u32[]{:S(2)}, u32[]{:S(2)}) %all-to-all-start.2) | async-done | bytes 131104 | tf_op jit(solution)/shard_map/all_to_all | solution.py:327
  92.1 0.4 pad_maximum_fusion
  92.5 1.1 broadcast_in_dim.7
  93.7 7.7 %all-to-all-start.3 = ((bf16[32,8,2048]{2,1,0:T(8,128)(2,1)}), bf16[32,8,2048]{2,1,0:T(8,128)(2,1)S(1)}, u32[]{:S(2)}, u32[]{:S(2)}) async-start(bf16[32,8,2048]{2,1,0:T(8,128)(2,1)} %bitcast.36), calls=%async_computation.3 | async-start | bytes 2097152 | tf_op jit(solution)/shard_map/all_to_all | solution.py:331
  101.4 4.6 %collective-permute-start.3 = (bf16[3072,128]{1,0:T(8,128)(2,1)}, bf16[3072,128]{1,0:T(8,128)(2,1)S(1)}, u32[]{:S(2)}, u32[]{:S(2)}) collective-permute-start(bf16[3072,128]{1,0:T(8,128)(2,1)} %get-tuple-element.36), channel_id=1, source_target_pairs={{0,12},{1,13},{2,14},{3,15},{4,0},{5,1},{6,2},{7,3},{8,4},{9,5},{1... | collective-permute-start | bytes 2359304 | tf_op jit(solution)/shard_map/ppermute | solution.py:76
  105.9 1.9 collective-permute-start.4
  107.9 4.8 %collective-permute-start.5 = (bf16[1536,128]{1,0:T(8,128)(2,1)}, bf16[1536,128]{1,0:T(8,128)(2,1)}, u32[]{:S(2)}, u32[]{:S(2)}) collective-permute-start(bf16[1536,128]{1,0:T(8,128)(2,1)} %get-tuple-element.38), channel_id=1, source_target_pairs={{0,12},{1,13},{2,14},{3,15},{4,0},{5,1},{6,2},{7,3},{8,4},{9,5},{1... | collective-permute-start | bytes 1179656 | tf_op jit(solution)/shard_map/ppermute | solution.py:76
  112.7 19.1 %collective-permute-done.3.refs_6_ = bf16[3072,128]{1,0:T(8,128)(2,1)S(1)} collective-permute-done((bf16[3072,128]{1,0:T(8,128)(2,1)}, bf16[3072,128]{1,0:T(8,128)(2,1)S(1)}, u32[]{:S(2)}, u32[]{:S(2)}) %collective-permute-start.3) | collective-permute-done | bytes 786464 | tf_op jit(solution)/shard_map/ppermute | solution.py:76
  131.8 0.8 copy-done.3
  132.6 7.7 %collective-permute-done.5.refs_8_ = bf16[1536,128]{1,0:T(8,128)(2,1)} collective-permute-done((bf16[1536,128]{1,0:T(8,128)(2,1)}, bf16[1536,128]{1,0:T(8,128)(2,1)}, u32[]{:S(2)}, u32[]{:S(2)}) %collective-permute-start.5) | collective-permute-done | bytes 393248 | tf_op jit(solution)/shard_map/ppermute | solution.py:76
  140.3 8.1 %run_experts.1 = bf16[256,2048]{1,0:T(8,128)(2,1)S(1)} custom-call(bf16[256,2048]{1,0:T(8,128)(2,1)S(1)} %bitcast.159, bf16[2048,384]{1,0:T(8,128)(2,1)} %bitcast.162, bf16[2048,384]{1,0:T(8,128)(2,1)} %bitcast.164, bf16[384,2048]{1,0:T(8,128)(2,1)} %bitcast.166, bf16[4608,128]{1,0:T(8,128)(2,1)} %collective-permute-done.refs_3_, ...), custom_call_target="tpu_custom_call" | custom-call | tf_op jit(solution)/shard_map/run_experts/pallas_call | solution.py:343
  148.4 24.4 %all_to_all.35 = bf16[32,8,2048]{2,1,0:T(8,128)(2,1)S(1)} all-to-all(bf16[32,8,2048]{2,1,0:T(8,128)(2,1)S(1)} %bitcast.160), channel_id=1, replica_groups=mesh['zh'=8,'zl'=2,'c'=2,'tp'=16] {'c','tp'}, dimensions={0} | all-to-all | bytes 2097152 | tf_op jit(solution)/shard_map/all_to_all | solution.py:331
  173.0 0.8 copy.41
  173.8 7.9 %all-to-all-start.5 = ((bf16[16,2,2048]{2,1,0:T(2,128)(2,1)}), bf16[16,2,2048]{2,1,0:T(2,128)(2,1)S(1)}, u32[]{:S(2)}, u32[]{:S(2)}) async-start(bf16[16,2,2048]{2,1,0:T(2,128)(2,1)} %copy.41), calls=%async_computation.5 | async-start | bytes 262144 | tf_op jit(solution)/shard_map/all_to_all | solution.py:327
  181.7 11.9 %all-to-all-done.5 = bf16[16,2,2048]{2,1,0:T(2,128)(2,1)S(1)} async-done(((bf16[16,2,2048]{2,1,0:T(2,128)(2,1)}), bf16[16,2,2048]{2,1,0:T(2,128)(2,1)S(1)}, u32[]{:S(2)}, u32[]{:S(2)}) %all-to-all-start.5) | async-done | bytes 131104 | tf_op jit(solution)/shard_map/all_to_all | solution.py:327
  194.4 13.0 %all_to_all.36 = bf16[16,8,2048]{2,1,0:T(8,128)(2,1)S(1)} all-to-all(bf16[16,8,2048]{2,1,0:T(8,128)(2,1)S(1)} %broadcast_in_dim.8), channel_id=1, replica_groups=mesh['zh'=8,'zl'=2,'c'=2,'tp'=16] {'tp'}, dimensions={0} | all-to-all | bytes 1048576 | tf_op jit(solution)/shard_map/all_to_all | solution.py:124
  207.4 0.8 copy.48
  (68 shorter events, 5.1 us)
Async XLA Ops:
  0.0 54.1 %copy-start = (bf16[128,2048]{1,0:T(8,128)(2,1)S(1)}, bf16[128,2048]{1,0:T(8,128)(2,1)}, u32[]{:S(2)}) copy-start(bf16[128,2048]{1,0:T(8,128)(2,1)} %param.26) | copy-start | bytes 1572868
  21.6 23.7 %all-to-all-start = ((bf16[16,64,128]{2,1,0:T(8,128)(2,1)}), bf16[16,64,128]{2,1,0:T(8,128)(2,1)S(1)}, u32[]{:S(2)}, u32[]{:S(2)}) async-start(bf16[16,64,128]{2,1,0:T(8,128)(2,1)} %broadcast_in_dim.6), calls=%async_computation | async-start | bytes 524288 | tf_op jit(solution)/shard_map/all_to_all | solution.py:100
  52.1 2.0 copy-start.4
  52.1 2.0 copy-start.9
  53.4 9.4 %copy-start.7 = (s32[128,2]{0,1:T(2,128)S(1)}, s32[128,2]{0,1:T(2,128)}, u32[]{:S(2)}) copy-start(s32[128,2]{0,1:T(2,128)} %param.29) | copy-start | bytes 3076
  54.1 19.1 %copy-start.5 = (f32[2048]{0:T(1024)S(1)}, f32[2048]{0:T(1024)}, u32[]{:S(2)}) copy-start(f32[2048]{0:T(1024)} %param.27) | copy-start | bytes 24580
  55.3 17.5 %all-to-all-start.1 = ((bf16[16,8,2048]{2,1,0:T(8,128)(2,1)}), bf16[16,8,2048]{2,1,0:T(8,128)(2,1)S(1)}, u32[]{:S(2)}, u32[]{:S(2)}) async-start(bf16[16,8,2048]{2,1,0:T(8,128)(2,1)} %fusion), calls=%async_computation.1 | async-start | bytes 1048576 | tf_op jit(solution)/shard_map/all_to_all | solution.py:118
  74.3 17.7 %all-to-all-start.2 = ((bf16[16,2,2048]{2,1,0:T(2,128)(2,1)}), bf16[16,2,2048]{2,1,0:T(2,128)(2,1)S(1)}, u32[]{:S(2)}, u32[]{:S(2)}) async-start(bf16[16,2,2048]{2,1,0:T(2,128)(2,1)} %reshape.119), calls=%async_computation.2 | async-start | bytes 262144 | tf_op jit(solution)/shard_map/all_to_all | solution.py:327
  80.0 51.7 %collective-permute-start = (bf16[4608,128]{1,0:T(8,128)(2,1)}, bf16[4608,128]{1,0:T(8,128)(2,1)}, u32[]{:S(2)}, u32[]{:S(2)}) collective-permute-start(bf16[4608,128]{1,0:T(8,128)(2,1)} %get-tuple-element.33), channel_id=1, source_target_pairs={{0,1},{1,2},{2,3},{3,0},{4,5},{5,6},{6,7},{7,4},{8,9},{9,10},{10,1... | collective-permute-start | bytes 3538952 | tf_op jit(solution)/shard_map/ppermute | solution.py:76
  82.2 49.5 %collective-permute-start.1 = (bf16[4608,128]{1,0:T(8,128)(2,1)}, bf16[4608,128]{1,0:T(8,128)(2,1)}, u32[]{:S(2)}, u32[]{:S(2)}) collective-permute-start(bf16[4608,128]{1,0:T(8,128)(2,1)} %get-tuple-element.34), channel_id=1, source_target_pairs={{0,3},{1,0},{2,1},{3,2},{4,7},{5,4},{6,5},{7,6},{8,11},{9,8},{10,9... | collective-permute-start | bytes 3538952 | tf_op jit(solution)/shard_map/ppermute | solution.py:76
  86.5 21.4 %collective-permute-start.2 = (bf16[3072,128]{1,0:T(8,128)(2,1)}, bf16[3072,128]{1,0:T(8,128)(2,1)S(1)}, u32[]{:S(2)}, u32[]{:S(2)}) collective-permute-start(bf16[3072,128]{1,0:T(8,128)(2,1)} %get-tuple-element.35), channel_id=1, source_target_pairs={{0,4},{1,5},{2,6},{3,7},{4,8},{5,9},{6,10},{7,11},{8,12},{9,13},{1... | collective-permute-start | bytes 2359304 | tf_op jit(solution)/shard_map/ppermute | solution.py:76
  93.7 46.6 %all-to-all-start.3 = ((bf16[32,8,2048]{2,1,0:T(8,128)(2,1)}), bf16[32,8,2048]{2,1,0:T(8,128)(2,1)S(1)}, u32[]{:S(2)}, u32[]{:S(2)}) async-start(bf16[32,8,2048]{2,1,0:T(8,128)(2,1)} %bitcast.36), calls=%async_computation.3 | async-start | bytes 2097152 | tf_op jit(solution)/shard_map/all_to_all | solution.py:331
  101.4 30.3 %collective-permute-start.3 = (bf16[3072,128]{1,0:T(8,128)(2,1)}, bf16[3072,128]{1,0:T(8,128)(2,1)S(1)}, u32[]{:S(2)}, u32[]{:S(2)}) collective-permute-start(bf16[3072,128]{1,0:T(8,128)(2,1)} %get-tuple-element.36), channel_id=1, source_target_pairs={{0,12},{1,13},{2,14},{3,15},{4,0},{5,1},{6,2},{7,3},{8,4},{9,5},{1... | collective-permute-start | bytes 2359304 | tf_op jit(solution)/shard_map/ppermute | solution.py:76
  105.9 25.8 %collective-permute-start.4 = (bf16[1536,128]{1,0:T(8,128)(2,1)}, bf16[1536,128]{1,0:T(8,128)(2,1)S(1)}, u32[]{:S(2)}, u32[]{:S(2)}) collective-permute-start(bf16[1536,128]{1,0:T(8,128)(2,1)} %get-tuple-element.37), channel_id=1, source_target_pairs={{0,4},{1,5},{2,6},{3,7},{4,8},{5,9},{6,10},{7,11},{8,12},{9,13},{1... | collective-permute-start | bytes 1179656 | tf_op jit(solution)/shard_map/ppermute | solution.py:76
  107.9 32.4 %copy-start.1 = (bf16[3072,128]{1,0:T(8,128)(2,1)}, bf16[3072,128]{1,0:T(8,128)(2,1)S(1)}, u32[]{:S(2)}) copy-start(bf16[3072,128]{1,0:T(8,128)(2,1)S(1)} %collective-permute-done.2.refs_5_) | copy-start | bytes 2359300
  107.9 32.4 %collective-permute-start.5 = (bf16[1536,128]{1,0:T(8,128)(2,1)}, bf16[1536,128]{1,0:T(8,128)(2,1)}, u32[]{:S(2)}, u32[]{:S(2)}) collective-permute-start(bf16[1536,128]{1,0:T(8,128)(2,1)} %get-tuple-element.38), channel_id=1, source_target_pairs={{0,12},{1,13},{2,14},{3,15},{4,0},{5,1},{6,2},{7,3},{8,4},{9,5},{1... | collective-permute-start | bytes 1179656 | tf_op jit(solution)/shard_map/ppermute | solution.py:76
  131.7 8.5 %copy-start.2 = (bf16[3072,128]{1,0:T(8,128)(2,1)}, bf16[3072,128]{1,0:T(8,128)(2,1)S(1)}, u32[]{:S(2)}) copy-start(bf16[3072,128]{1,0:T(8,128)(2,1)S(1)} %collective-permute-done.3.refs_6_) | copy-start | bytes 2359300
  131.7 0.8 copy-start.3
  172.7 8.9 %copy-start.8 = (f32[128,2]{0,1:T(2,128)S(1)}, f32[128,2]{0,1:T(2,128)}, u32[]{:S(2)}) copy-start(f32[128,2]{0,1:T(2,128)} %param.30) | copy-start | bytes 3076
  172.7 21.5 %copy-start.6 = (f32[2048]{0:T(1024)S(1)}, f32[2048]{0:T(1024)}, u32[]{:S(2)}) copy-start(f32[2048]{0:T(1024)} %param.28) | copy-start | bytes 24580
  173.8 19.9 %all-to-all-start.5 = ((bf16[16,2,2048]{2,1,0:T(2,128)(2,1)}), bf16[16,2,2048]{2,1,0:T(2,128)(2,1)S(1)}, u32[]{:S(2)}, u32[]{:S(2)}) async-start(bf16[16,2,2048]{2,1,0:T(2,128)(2,1)} %copy.41), calls=%async_computation.5 | async-start | bytes 262144 | tf_op jit(solution)/shard_map/all_to_all | solution.py:327

commit v9 on v8

--- a/solution.py
+++ b/solution.py
@@ -111,12 +111,6 @@
     shape = x.shape
     blocks = x.reshape(*shape[:dim], length, shape[dim] // length, *shape[dim + 1 :])
     return jnp.moveaxis(blocks, dim, 0)
-
-
-def sum_at_owner(x, axis, dim):
-    length = lax.axis_size(axis)
-    blocks = lax.all_to_all(in_blocks(x, dim, length), axis, 0, 0, tiled=True)
-    return jnp.sum(blocks.astype(jnp.float32), axis=0)
 
 
 def copy_for_each(x, axis):
@@ -308,9 +302,11 @@
     expert_count = lax.axis_size(SP) * expert_gate.shape[0]
     rows = length // split_count
     first = lax.axis_index("tp") * rows
-    projected = sum_at_owner(
-        jnp.dot(gated, out_weight, preferred_element_type=jnp.float32).astype(jnp.bfloat16), "tp", 0
-    )
+    product = jnp.dot(gated, out_weight, preferred_element_type=jnp.float32).astype(jnp.bfloat16)
+    product, late = lax.optimization_barrier((product, parts[4:]))
+    late = spread(late, side, 2)
+    product = lax.all_to_all(in_blocks(product, 0, split_count), "tp", 0, 0, tiled=True)
+    projected = jnp.sum(product.astype(jnp.float32), axis=0)
     residual = lax.optimization_barrier(lax.dynamic_slice_in_dim(residual_in, first, rows, 0))
     routes = lax.dynamic_slice_in_dim(expert_index, first, rows, 0)
     weights = lax.dynamic_slice_in_dim(route_weights, first, rows, 0)
@@ -331,10 +327,8 @@
         return lax.all_to_all(x, PLANE, 0, 0, tiled=True)
 
     half = chips // 2
-    send, late = lax.optimization_barrier((send, parts[4:]))
-    late = spread(late, side, 2)
-    arrived = along_z(send)
-    arrived = arrived.transpose(1, 0, 2).reshape(2, 2, half, width)
+    arrived = lax.all_to_all(send.reshape(chips, 16, width // 8), Z, 0, 0, tiled=True)
+    arrived = arrived.reshape(chips, 2, width).transpose(1, 0, 2).reshape(2, 2, half, width)
     swapped = arrived[:, ::-1]
     turns = jnp.stack([arrived, swapped], 1)[:, None, :, None]
     turns = jnp.broadcast_to(turns, (2, side // 2, 2, side // 2, 2, half, width))

time: 212 us -> 211 us (level)
    all_to_all x2 -> x1, starting transfers between devices: 13.5 us -> 7.74 us  [along_z(): out = lax.all_to_all(x.reshape(chips, 2, width), Z, 0, 0, tiled=True)]
    all_to_all x1 -> x2, starting transfers between devices: 6.75 us -> 12.4 us  [the longest x1 6.75 us: per_device(): lax.all_to_all(in_blocks(product, 0, split_count), 'tp', 0, 0, tiled=True)]
    all_to_all x1 -> x2, waiting for transfers between devices: 9.81 us -> 13.3 us  [the longest x1 9.81 us: per_device(): lax.all_to_all(in_blocks(product, 0, split_count), 'tp', 0, 0, tiled=True)]
    all_to_all x2 -> x1, waiting for transfers between devices: 15.4 us -> 11.9 us  [along_z(): out = lax.all_to_all(x.reshape(chips, 2, width), Z, 0, 0, tiled=True)]
where the time goes in v9:
time: 211 us; the launch traced here: 208 us
  waiting for transfers between devices  66.1 us (31%)
  starting transfers between devices  57.1 us (27%)
  blocking collectives  56.8 us (27%)
  Pallas kernels  14.6 us (7%)
  local copies, waits for them, and re-layouts  6.23 us (3%)
  matrix products  4.32 us (2%)
    ppermute x6, waiting for transfers between devices, spread(): out.append(lax.ppermute(part, 'tp', pairs))  26.8 us
    all_to_all x1, blocking collectives, in_plane(): return lax.all_to_all(x, PLANE, 0, 0, tiled=True)  24.5 us
    ppermute x6, starting transfers between devices, spread(): out.append(lax.ppermute(part, 'tp', pairs))  19.6 us
    all_to_all x1, waiting for transfers between devices, entering(): far = lax.all_to_all(far, Z, 0, 0, tiled=True)  14.1 us
    all_to_all x1, blocking collectives, copy_for_each(): lax.all_to_all(jnp.broadcast_to(x[None], (length, *x.shape)), axis, 0, 0,...  13 us
    all_gather x1, blocking collectives, entering(): near = lax.all_gather(own, ('zl', 'c')).astype(jnp.float32)  12.5 us
    all_to_all x1, waiting for transfers between devices, along_z(): out = lax.all_to_all(x.reshape(chips, 2, width), Z, 0, 0, tiled=True)  11.9 us
    all_to_all x1, waiting for transfers between devices, per_device(): lax.all_to_all(in_blocks(product, 0, split_count), 'tp', 0, 0, tiled=True)  9.81 us
  transfers between devices with their start and end apart: 11, of which 6 were waited for; matrix products, arithmetic and copies ran while one was open for 1% of the time, Pallas kernels for 0%

profile of v9, /device:TPU:1, one launch (start us, length us, event | category | flops | bytes accessed | tf_op | source)
XLA Modules:
  0.0 207.8 jit_solution(12854302773952521357)
XLA Ops:
  0.7 6.5 %local_span.1 = (bf16[256,128]{1,0:T(8,128)(2,1)S(1)}, f32[128,128]{1,0:T(8,128)S(1)}, f32[128,128]{1,0:T(8,128)S(1)}, bf16[4608,128]{1,0:T(8,128)(2,1)}, bf16[4...) custom-call(bf16[128,128]{1,0:T(8,128)(2,1)} %q_ref.1, ...), custom_call_target="tpu_custom_call" | custom-call | tf_op jit(solution)/shard_map/local_span/pallas_call | solution.py:281
  7.2 12.5 %all-gather = bf16[1024,128]{1,0:T(8,128)(2,1)S(1)} all-gather(bf16[256,128]{1,0:T(8,128)(2,1)S(1)} %get-tuple-element.24), channel_id=2, replica_groups=mesh['zh'=8,'zl'=2,'c'=2,'tp'=16] {'zl','c'}, dimensions={0}, use_global_device_ids=true | all-gather | bytes 327680 | tf_op jit(solution)/shard_map/all_gather | solution.py:83
  20.8 0.8 broadcast_in_dim.6
  21.6 9.6 %all-to-all-start = ((bf16[16,64,128]{2,1,0:T(8,128)(2,1)}), bf16[16,64,128]{2,1,0:T(8,128)(2,1)S(1)}, u32[]{:S(2)}, u32[]{:S(2)}) async-start(bf16[16,64,128]{2,1,0:T(8,128)(2,1)} %broadcast_in_dim.6), calls=%async_computation | async-start | bytes 524288 | tf_op jit(solution)/shard_map/all_to_all | solution.py:100
  31.2 14.1 %all-to-all-done = bf16[16,64,128]{2,1,0:T(8,128)(2,1)S(1)} async-done(((bf16[16,64,128]{2,1,0:T(8,128)(2,1)}), bf16[16,64,128]{2,1,0:T(8,128)(2,1)S(1)}, u32[]{:S(2)}, u32[]{:S(2)}) %all-to-all-start) | async-done | bytes 262176 | tf_op jit(solution)/shard_map/all_to_all | solution.py:100
  45.3 6.8 %all-gather.1 = bf16[32,64,128]{2,1,0:T(8,128)(2,1)S(1)} all-gather(bf16[16,64,128]{2,1,0:T(8,128)(2,1)S(1)} %all-to-all-done), channel_id=3, replica_groups=mesh['zh'=8,'zl'=2,'c'=2,'tp'=16] {'c'}, dimensions={0}, use_global_device_ids=true | all-gather | bytes 786432 | tf_op jit(solution)/shard_map/all_gather | solution.py:101
  53.8 0.3 multiply_reduce_fusion.2
  54.1 1.1 convolution_convert_fusion
  55.3 6.8 %all-to-all-start.1 = ((bf16[16,8,2048]{2,1,0:T(8,128)(2,1)}), bf16[16,8,2048]{2,1,0:T(8,128)(2,1)S(1)}, u32[]{:S(2)}, u32[]{:S(2)}) async-start(bf16[16,8,2048]{2,1,0:T(8,128)(2,1)} %bitcast.31), calls=%async_computation.1 | async-start | bytes 1048576 | tf_op jit(solution)/shard_map/all_to_all | solution.py:308
  62.0 0.8 constant_dynamic-slice_fusion.2
  63.0 9.8 %all-to-all-done.1 = bf16[16,8,2048]{2,1,0:T(8,128)(2,1)S(1)} async-done(((bf16[16,8,2048]{2,1,0:T(8,128)(2,1)}), bf16[16,8,2048]{2,1,0:T(8,128)(2,1)S(1)}, u32[]{:S(2)}, u32[]{:S(2)}) %all-to-all-start.1) | async-done | bytes 524320 | tf_op jit(solution)/shard_map/all_to_all | solution.py:308
  73.5 0.7 reshape.122
  74.2 5.7 %all-to-all-start.2 = ((bf16[16,16,256]{2,1,0:T(8,128)(2,1)}), bf16[16,16,256]{2,1,0:T(8,128)(2,1)S(1)}, u32[]{:S(2)}, u32[]{:S(2)}) async-start(bf16[16,16,256]{2,1,0:T(8,128)(2,1)} %reshape.122), calls=%async_computation.2 | async-start | bytes 262144 | tf_op jit(solution)/shard_map/all_to_all | solution.py:330
  79.9 2.2 %collective-permute-start = (bf16[4608,128]{1,0:T(8,128)(2,1)}, bf16[4608,128]{1,0:T(8,128)(2,1)}, u32[]{:S(2)}, u32[]{:S(2)}) collective-permute-start(bf16[4608,128]{1,0:T(8,128)(2,1)} %get-tuple-element.33), channel_id=1, source_target_pairs={{0,1},{1,2},{2,3},{3,0},{4,5},{5,6},{6,7},{7,4},{8,9},{9,10},{10,1... | collective-permute-start | bytes 3538952 | tf_op jit(solution)/shard_map/ppermute | solution.py:76
  82.1 4.3 %collective-permute-start.1 = (bf16[4608,128]{1,0:T(8,128)(2,1)}, bf16[4608,128]{1,0:T(8,128)(2,1)}, u32[]{:S(2)}, u32[]{:S(2)}) collective-permute-start(bf16[4608,128]{1,0:T(8,128)(2,1)} %get-tuple-element.34), channel_id=1, source_target_pairs={{0,3},{1,0},{2,1},{3,2},{4,7},{5,4},{6,5},{7,6},{8,11},{9,8},{10,9... | collective-permute-start | bytes 3538952 | tf_op jit(solution)/shard_map/ppermute | solution.py:76
  86.5 1.9 collective-permute-start.2
  88.4 3.5 %all-to-all-done.2 = bf16[16,16,256]{2,1,0:T(8,128)(2,1)S(1)} async-done(((bf16[16,16,256]{2,1,0:T(8,128)(2,1)}), bf16[16,16,256]{2,1,0:T(8,128)(2,1)S(1)}, u32[]{:S(2)}, u32[]{:S(2)}) %all-to-all-start.2) | async-done | bytes 131104 | tf_op jit(solution)/shard_map/all_to_all | solution.py:330
  92.1 1.1 broadcast_in_dim.7
  93.3 7.7 %all-to-all-start.3 = ((bf16[32,8,2048]{2,1,0:T(8,128)(2,1)}), bf16[32,8,2048]{2,1,0:T(8,128)(2,1)S(1)}, u32[]{:S(2)}, u32[]{:S(2)}) async-start(bf16[32,8,2048]{2,1,0:T(8,128)(2,1)} %bitcast.36), calls=%async_computation.3 | async-start | bytes 2097152 | tf_op jit(solution)/shard_map/all_to_all | solution.py:327
  101.0 4.6 %collective-permute-start.3 = (bf16[3072,128]{1,0:T(8,128)(2,1)}, bf16[3072,128]{1,0:T(8,128)(2,1)S(1)}, u32[]{:S(2)}, u32[]{:S(2)}) collective-permute-start(bf16[3072,128]{1,0:T(8,128)(2,1)} %get-tuple-element.36), channel_id=1, source_target_pairs={{0,12},{1,13},{2,14},{3,15},{4,0},{5,1},{6,2},{7,3},{8,4},{9,5},{1... | collective-permute-start | bytes 2359304 | tf_op jit(solution)/shard_map/ppermute | solution.py:76
  105.5 1.9 collective-permute-start.4
  107.5 4.8 %collective-permute-start.5 = (bf16[1536,128]{1,0:T(8,128)(2,1)}, bf16[1536,128]{1,0:T(8,128)(2,1)}, u32[]{:S(2)}, u32[]{:S(2)}) collective-permute-start(bf16[1536,128]{1,0:T(8,128)(2,1)} %get-tuple-element.38), channel_id=1, source_target_pairs={{0,12},{1,13},{2,14},{3,15},{4,0},{5,1},{6,2},{7,3},{8,4},{9,5},{1... | collective-permute-start | bytes 1179656 | tf_op jit(solution)/shard_map/ppermute | solution.py:76
  112.2 19.1 %collective-permute-done.3.refs_6_ = bf16[3072,128]{1,0:T(8,128)(2,1)S(1)} collective-permute-done((bf16[3072,128]{1,0:T(8,128)(2,1)}, bf16[3072,128]{1,0:T(8,128)(2,1)S(1)}, u32[]{:S(2)}, u32[]{:S(2)}) %collective-permute-start.3) | collective-permute-done | bytes 786464 | tf_op jit(solution)/shard_map/ppermute | solution.py:76
  131.3 0.8 copy-done.3
  132.2 7.7 %collective-permute-done.5.refs_8_ = bf16[1536,128]{1,0:T(8,128)(2,1)} collective-permute-done((bf16[1536,128]{1,0:T(8,128)(2,1)}, bf16[1536,128]{1,0:T(8,128)(2,1)}, u32[]{:S(2)}, u32[]{:S(2)}) %collective-permute-start.5) | collective-permute-done | bytes 393248 | tf_op jit(solution)/shard_map/ppermute | solution.py:76
  139.9 8.1 %run_experts.1 = bf16[256,2048]{1,0:T(8,128)(2,1)S(1)} custom-call(bf16[256,2048]{1,0:T(8,128)(2,1)S(1)} %bitcast.158, bf16[2048,384]{1,0:T(8,128)(2,1)} %bitcast.161, bf16[2048,384]{1,0:T(8,128)(2,1)} %bitcast.163, bf16[384,2048]{1,0:T(8,128)(2,1)} %bitcast.165, bf16[4608,128]{1,0:T(8,128)(2,1)} %collective-permute-done.refs_3_, ...), custom_call_target="tpu_custom_call" | custom-call | tf_op jit(solution)/shard_map/run_experts/pallas_call | solution.py:337
  147.9 24.5 %all_to_all.35 = bf16[32,8,2048]{2,1,0:T(8,128)(2,1)S(1)} all-to-all(bf16[32,8,2048]{2,1,0:T(8,128)(2,1)S(1)} %bitcast.159), channel_id=1, replica_groups=mesh['zh'=8,'zl'=2,'c'=2,'tp'=16] {'c','tp'}, dimensions={0} | all-to-all | bytes 2097152 | tf_op jit(solution)/shard_map/all_to_all | solution.py:327
  172.7 0.8 copy.46
  173.5 7.7 %all-to-all-start.5 = ((bf16[16,2,2048]{2,1,0:T(2,128)(2,1)}), bf16[16,2,2048]{2,1,0:T(2,128)(2,1)S(1)}, u32[]{:S(2)}, u32[]{:S(2)}) async-start(bf16[16,2,2048]{2,1,0:T(2,128)(2,1)} %copy.46), calls=%async_computation.5 | async-start | bytes 262144 | tf_op jit(solution)/shard_map/all_to_all | solution.py:323
  181.3 11.9 %all-to-all-done.5 = bf16[16,2,2048]{2,1,0:T(2,128)(2,1)S(1)} async-done(((bf16[16,2,2048]{2,1,0:T(2,128)(2,1)}), bf16[16,2,2048]{2,1,0:T(2,128)(2,1)S(1)}, u32[]{:S(2)}, u32[]{:S(2)}) %all-to-all-start.5) | async-done | bytes 131104 | tf_op jit(solution)/shard_map/all_to_all | solution.py:323
  194.0 13.0 %all_to_all.36 = bf16[16,8,2048]{2,1,0:T(8,128)(2,1)S(1)} all-to-all(bf16[16,8,2048]{2,1,0:T(8,128)(2,1)S(1)} %broadcast_in_dim.8), channel_id=1, replica_groups=mesh['zh'=8,'zl'=2,'c'=2,'tp'=16] {'tp'}, dimensions={0} | all-to-all | bytes 1048576 | tf_op jit(solution)/shard_map/all_to_all | solution.py:118
  207.0 0.8 copy.53
  (70 shorter events, 4.8 us)
Async XLA Ops:
  0.0 54.1 %copy-start = (bf16[128,2048]{1,0:T(8,128)(2,1)S(1)}, bf16[128,2048]{1,0:T(8,128)(2,1)}, u32[]{:S(2)}) copy-start(bf16[128,2048]{1,0:T(8,128)(2,1)} %param.26) | copy-start | bytes 1572868
  21.6 23.7 %all-to-all-start = ((bf16[16,64,128]{2,1,0:T(8,128)(2,1)}), bf16[16,64,128]{2,1,0:T(8,128)(2,1)S(1)}, u32[]{:S(2)}, u32[]{:S(2)}) async-start(bf16[16,64,128]{2,1,0:T(8,128)(2,1)} %broadcast_in_dim.6), calls=%async_computation | async-start | bytes 524288 | tf_op jit(solution)/shard_map/all_to_all | solution.py:100
  52.1 2.0 copy-start.4
  52.1 2.0 copy-start.9
  53.4 9.4 %copy-start.7 = (s32[128,2]{0,1:T(2,128)S(1)}, s32[128,2]{0,1:T(2,128)}, u32[]{:S(2)}) copy-start(s32[128,2]{0,1:T(2,128)} %param.29) | copy-start | bytes 3076
  54.1 19.1 %copy-start.5 = (f32[2048]{0:T(1024)S(1)}, f32[2048]{0:T(1024)}, u32[]{:S(2)}) copy-start(f32[2048]{0:T(1024)} %param.27) | copy-start | bytes 24580
  55.3 17.5 %all-to-all-start.1 = ((bf16[16,8,2048]{2,1,0:T(8,128)(2,1)}), bf16[16,8,2048]{2,1,0:T(8,128)(2,1)S(1)}, u32[]{:S(2)}, u32[]{:S(2)}) async-start(bf16[16,8,2048]{2,1,0:T(8,128)(2,1)} %bitcast.31), calls=%async_computation.1 | async-start | bytes 1048576 | tf_op jit(solution)/shard_map/all_to_all | solution.py:308
  74.2 17.7 %all-to-all-start.2 = ((bf16[16,16,256]{2,1,0:T(8,128)(2,1)}), bf16[16,16,256]{2,1,0:T(8,128)(2,1)S(1)}, u32[]{:S(2)}, u32[]{:S(2)}) async-start(bf16[16,16,256]{2,1,0:T(8,128)(2,1)} %reshape.122), calls=%async_computation.2 | async-start | bytes 262144 | tf_op jit(solution)/shard_map/all_to_all | solution.py:330
  79.9 51.4 %collective-permute-start = (bf16[4608,128]{1,0:T(8,128)(2,1)}, bf16[4608,128]{1,0:T(8,128)(2,1)}, u32[]{:S(2)}, u32[]{:S(2)}) collective-permute-start(bf16[4608,128]{1,0:T(8,128)(2,1)} %get-tuple-element.33), channel_id=1, source_target_pairs={{0,1},{1,2},{2,3},{3,0},{4,5},{5,6},{6,7},{7,4},{8,9},{9,10},{10,1... | collective-permute-start | bytes 3538952 | tf_op jit(solution)/shard_map/ppermute | solution.py:76
  82.1 49.2 %collective-permute-start.1 = (bf16[4608,128]{1,0:T(8,128)(2,1)}, bf16[4608,128]{1,0:T(8,128)(2,1)}, u32[]{:S(2)}, u32[]{:S(2)}) collective-permute-start(bf16[4608,128]{1,0:T(8,128)(2,1)} %get-tuple-element.34), channel_id=1, source_target_pairs={{0,3},{1,0},{2,1},{3,2},{4,7},{5,4},{6,5},{7,6},{8,11},{9,8},{10,9... | collective-permute-start | bytes 3538952 | tf_op jit(solution)/shard_map/ppermute | solution.py:76
  86.5 21.0 %collective-permute-start.2 = (bf16[3072,128]{1,0:T(8,128)(2,1)}, bf16[3072,128]{1,0:T(8,128)(2,1)S(1)}, u32[]{:S(2)}, u32[]{:S(2)}) collective-permute-start(bf16[3072,128]{1,0:T(8,128)(2,1)} %get-tuple-element.35), channel_id=1, source_target_pairs={{0,4},{1,5},{2,6},{3,7},{4,8},{5,9},{6,10},{7,11},{8,12},{9,13},{1... | collective-permute-start | bytes 2359304 | tf_op jit(solution)/shard_map/ppermute | solution.py:76
  93.3 46.6 %all-to-all-start.3 = ((bf16[32,8,2048]{2,1,0:T(8,128)(2,1)}), bf16[32,8,2048]{2,1,0:T(8,128)(2,1)S(1)}, u32[]{:S(2)}, u32[]{:S(2)}) async-start(bf16[32,8,2048]{2,1,0:T(8,128)(2,1)} %bitcast.36), calls=%async_computation.3 | async-start | bytes 2097152 | tf_op jit(solution)/shard_map/all_to_all | solution.py:327
  101.0 30.3 %collective-permute-start.3 = (bf16[3072,128]{1,0:T(8,128)(2,1)}, bf16[3072,128]{1,0:T(8,128)(2,1)S(1)}, u32[]{:S(2)}, u32[]{:S(2)}) collective-permute-start(bf16[3072,128]{1,0:T(8,128)(2,1)} %get-tuple-element.36), channel_id=1, source_target_pairs={{0,12},{1,13},{2,14},{3,15},{4,0},{5,1},{6,2},{7,3},{8,4},{9,5},{1... | collective-permute-start | bytes 2359304 | tf_op jit(solution)/shard_map/ppermute | solution.py:76
  105.5 25.8 %collective-permute-start.4 = (bf16[1536,128]{1,0:T(8,128)(2,1)}, bf16[1536,128]{1,0:T(8,128)(2,1)S(1)}, u32[]{:S(2)}, u32[]{:S(2)}) collective-permute-start(bf16[1536,128]{1,0:T(8,128)(2,1)} %get-tuple-element.37), channel_id=1, source_target_pairs={{0,4},{1,5},{2,6},{3,7},{4,8},{5,9},{6,10},{7,11},{8,12},{9,13},{1... | collective-permute-start | bytes 1179656 | tf_op jit(solution)/shard_map/ppermute | solution.py:76
  107.5 32.4 %copy-start.1 = (bf16[3072,128]{1,0:T(8,128)(2,1)}, bf16[3072,128]{1,0:T(8,128)(2,1)S(1)}, u32[]{:S(2)}) copy-start(bf16[3072,128]{1,0:T(8,128)(2,1)S(1)} %collective-permute-done.2.refs_5_) | copy-start | bytes 2359300
  107.5 32.4 %collective-permute-start.5 = (bf16[1536,128]{1,0:T(8,128)(2,1)}, bf16[1536,128]{1,0:T(8,128)(2,1)}, u32[]{:S(2)}, u32[]{:S(2)}) collective-permute-start(bf16[1536,128]{1,0:T(8,128)(2,1)} %get-tuple-element.38), channel_id=1, source_target_pairs={{0,12},{1,13},{2,14},{3,15},{4,0},{5,1},{6,2},{7,3},{8,4},{9,5},{1... | collective-permute-start | bytes 1179656 | tf_op jit(solution)/shard_map/ppermute | solution.py:76
  131.3 8.5 %copy-start.2 = (bf16[3072,128]{1,0:T(8,128)(2,1)}, bf16[3072,128]{1,0:T(8,128)(2,1)S(1)}, u32[]{:S(2)}) copy-start(bf16[3072,128]{1,0:T(8,128)(2,1)S(1)} %collective-permute-done.3.refs_6_) | copy-start | bytes 2359300
  131.3 0.8 copy-start.3
  172.4 8.8 %copy-start.8 = (f32[128,2]{0,1:T(2,128)S(1)}, f32[128,2]{0,1:T(2,128)}, u32[]{:S(2)}) copy-start(f32[128,2]{0,1:T(2,128)} %param.30) | copy-start | bytes 3076
  172.4 21.4 %copy-start.6 = (f32[2048]{0:T(1024)S(1)}, f32[2048]{0:T(1024)}, u32[]{:S(2)}) copy-start(f32[2048]{0:T(1024)} %param.28) | copy-start | bytes 24580
  173.5 19.8 %all-to-all-start.5 = ((bf16[16,2,2048]{2,1,0:T(2,128)(2,1)}), bf16[16,2,2048]{2,1,0:T(2,128)(2,1)S(1)}, u32[]{:S(2)}, u32[]{:S(2)}) async-start(bf16[16,2,2048]{2,1,0:T(2,128)(2,1)} %copy.46), calls=%async_computation.5 | async-start | bytes 262144 | tf_op jit(solution)/shard_map/all_to_all | solution.py:323

commit v10 on v9

--- a/solution.py
+++ b/solution.py
@@ -39,7 +39,6 @@
     depth, hidden = gate_ref.shape
     half, lanes, blocks = (depth // 2, LANES // 4, hidden // LANES)
     size = bufs[0].shape[0] // blocks
-    early = size * (blocks - 1)
     copies = []
     for part, buf in enumerate(bufs):
         for block in range(blocks):
@@ -56,9 +55,8 @@
         for part, buf in enumerate(bufs):
             row = block * size
             buf[row : row + half] = parts[:, part * LANES : (part + 1) * LANES]
-            late = row == early and part > 1
-            out = outs[part + 2] if late else outs[part].at[pl.ds(row, size)]
-            copies.append(pltpu.make_async_copy(buf.at[pl.ds(row, size)], out, sems.at[len(copies)]))
+            run = pl.ds(row, size)
+            copies.append(pltpu.make_async_copy(buf.at[run], outs[part].at[run], sems.at[len(copies)]))
             copies[-1].start()
     for copy in copies:
         copy.wait()
@@ -135,8 +133,8 @@
 
 
 def local_span(q_ref, k_ref, v_ref, beta_ref, decay_ref, rate_ref, *refs):
-    tables, (both_ref, mix_ref, out_ref), outs = refs[:3], refs[3:6], refs[6:12]
-    bufs, part_bufs, sems = refs[12:15], refs[15:19], refs[19]
+    tables, (both_ref, mix_ref, out_ref), outs = refs[:3], refs[3:6], refs[6:10]
+    bufs, part_bufs, sems = refs[10:13], refs[13:17], refs[17]
     copies = [pltpu.make_async_copy(x, y, sems.at[k]) for k, (x, y) in enumerate(zip(tables, bufs))]
     for copy in copies:
         copy.start()
@@ -199,15 +197,15 @@
 
 
 def run_experts(rows_ref, *refs):
-    out_ref, bufs, sems = refs[9], refs[10:19], refs[19]
-    copies = [pltpu.make_async_copy(refs[k], bufs[k], sems.at[k]) for k in range(9)]
+    out_ref, bufs, sems = refs[7], refs[8:15], refs[15]
+    copies = [pltpu.make_async_copy(refs[k], bufs[k], sems.at[k]) for k in range(7)]
     for copy in (*copies[:2], *copies[3:], copies[2]):
         copy.start()
     gate_ref, up_ref, down_ref = bufs[:3]
     rows = rows_ref[...]
     width = rows.shape[1]
     half, lanes, blocks = (width // 2, LANES // 4, down_ref.shape[0] // LANES)
-    size = bufs[7].shape[0]
+    size = bufs[3].shape[0] // blocks
 
     def dot(a, b):
         return jnp.dot(a, b, preferred_element_type=jnp.float32)
@@ -220,14 +218,11 @@
     arrived = [jnp.zeros((rows.shape[0], LANES), jnp.float32)] * blocks
 
     def run(part, block, first, count):
-        late = block == blocks - 1 and part > 1
-        ref, row = (bufs[5 + part], first) if late else (bufs[3 + part], block * size + first)
-        return ref[row : row + count]
+        row = block * size + first
+        return bufs[3 + part][row : row + count]
 
     for part in range(4):
         copies[3 + part].wait()
-        if part > 1:
-            copies[5 + part].wait()
         table = jnp.concatenate([run(part, k, 0, half) for k in range(blocks)], 1)
         low, high = (dot(rows[:, :half], table), dot(rows[:, half:], table))
         for k in range(blocks):
@@ -285,17 +280,15 @@
             pltpu.VMEM((length, HEAD_FEATURES), jnp.float32),
             pltpu.VMEM((length, HEAD_FEATURES), jnp.float32),
         )
-        + (jax.ShapeDtypeStruct(packed, jnp.bfloat16),) * 2
-        + (jax.ShapeDtypeStruct((packed[0] - packed[0] // 3, LANES), jnp.bfloat16),) * 2
-        + (jax.ShapeDtypeStruct((packed[0] // 3, LANES), jnp.bfloat16),) * 2,
+        + (jax.ShapeDtypeStruct(packed, jnp.bfloat16),) * 4,
         in_specs=[vmem] * 5 + [pl.BlockSpec(memory_space=pltpu.SMEM)] + [anywhere] * 3,
-        out_specs=(vmem,) * 3 + (anywhere,) * 6,
+        out_specs=(vmem,) * 3 + (anywhere,) * 4,
         scratch_shapes=[pltpu.VMEM(x.shape, x.dtype) for x in tables]
         + [pltpu.VMEM(packed, jnp.bfloat16)] * 4
         + [pltpu.SemaphoreType.DMA((15,))],
         name="local_span",
     )(queries, keys, values, beta_logit, decay_logit, decay_log, *tables)
-    state, early = entering(both, parts[:4], side)
+    state, early = entering(both, parts[:2], side)
     mixed = local + mm(mix, state)
     normalized = mixed * lax.rsqrt(jnp.mean(mixed * mixed, -1, keepdims=True) + 1e-06) * head_gain
     gated = (normalized * jax.nn.silu(out_gate.astype(jnp.float32))).astype(jnp.bfloat16)
@@ -303,7 +296,7 @@
     rows = length // split_count
     first = lax.axis_index("tp") * rows
     product = jnp.dot(gated, out_weight, preferred_element_type=jnp.float32).astype(jnp.bfloat16)
-    product, late = lax.optimization_barrier((product, parts[4:]))
+    product, late = lax.optimization_barrier((product, parts[2:]))
     late = spread(late, side, 2)
     product = lax.all_to_all(in_blocks(product, 0, split_count), "tp", 0, 0, tiled=True)
     projected = jnp.sum(product.astype(jnp.float32), axis=0)
@@ -337,10 +330,10 @@
     partial_value = pl.pallas_call(
         run_experts,
         out_shape=pltpu.VMEM(piece.shape, jnp.bfloat16),
-        in_specs=[vmem] + [anywhere] * 9,
+        in_specs=[vmem] + [anywhere] * 7,
         out_specs=vmem,
         scratch_shapes=[pltpu.VMEM(x.shape, x.dtype) for x in tables]
-        + [pltpu.SemaphoreType.DMA((9,))],
+        + [pltpu.SemaphoreType.DMA((7,))],
         name="run_experts",
     )(held(piece), *tables)
     shares = in_plane(partial_value.reshape(2 * split_count, half, width))

time: 211 us -> 203 us (0.962)
  starting transfers between devices: 57.1 us -> 53.5 us
  waiting for transfers between devices: 66.1 us -> 63.7 us
    ppermute x6 -> x4, starting transfers between devices: 19.6 us -> 13 us  [spread(): out.append(lax.ppermute(part, 'tp', pairs))]
    all_to_all x1, waiting for transfers between devices: 0.01 us -> 4.64 us  [in_plane(): return lax.all_to_all(x, PLANE, 0, 0, tiled=True)]
    all_to_all x1, starting transfers between devices: 7.74 us -> 11.5 us  [along_z(): out = lax.all_to_all(x.reshape(chips, 2, width), Z, 0, 0, tiled=True)]
    ppermute x6 -> x4, waiting for transfers between devices: 26.8 us -> 23.2 us  [spread(): out.append(lax.ppermute(part, 'tp', pairs))]
    all_to_all x1, waiting for transfers between devices: 3.53 us -> 0.01 us  [per_device(): lax.all_to_all(send.reshape(chips, 16, width // 8), Z, 0, 0, tiled=True)]
  transfers between devices with their start and end apart: 11 -> 9, of which waited for: 6 -> 8; matrix products, arithmetic and copies ran while one was open for 1% -> 1% of each run, Pallas kernels for 0% -> 0%
where the time goes in v10:
time: 203 us; the launch traced here: 199 us
  waiting for transfers between devices  63.7 us (31%)
  blocking collectives  55 us (27%)
  starting transfers between devices  53.5 us (26%)
  Pallas kernels  14.6 us (7%)
  local copies, waits for them, and re-layouts  5.37 us (3%)
  matrix products  4.32 us (2%)
    ppermute x4, waiting for transfers between devices, spread(): out.append(lax.ppermute(part, 'tp', pairs))  23.2 us
    all_to_all x1, blocking collectives, in_plane(): return lax.all_to_all(x, PLANE, 0, 0, tiled=True)  22.7 us
    all_to_all x1, waiting for transfers between devices, entering(): far = lax.all_to_all(far, Z, 0, 0, tiled=True)  14.1 us
    all_to_all x1, blocking collectives, copy_for_each(): lax.all_to_all(jnp.broadcast_to(x[None], (length, *x.shape)), axis, 0, 0,...  13 us
    ppermute x4, starting transfers between devices, spread(): out.append(lax.ppermute(part, 'tp', pairs))  13 us
    all_gather x1, blocking collectives, entering(): near = lax.all_gather(own, ('zl', 'c')).astype(jnp.float32)  12.4 us
    all_to_all x1, waiting for transfers between devices, along_z(): out = lax.all_to_all(x.reshape(chips, 2, width), Z, 0, 0, tiled=True)  11.9 us
    all_to_all x1, starting transfers between devices, along_z(): out = lax.all_to_all(x.reshape(chips, 2, width), Z, 0, 0, tiled=True)  11.5 us
  transfers between devices with their start and end apart: 9, of which 8 were waited for; matrix products, arithmetic and copies ran while one was open for 1% of the time, Pallas kernels for 0%

profile of v10, /device:TPU:1, one launch (start us, length us, event | category | flops | bytes accessed | tf_op | source)
XLA Modules:
  0.0 199.0 jit_solution(6772602954932719261)
XLA Ops:
  0.7 6.5 %local_span.1 = (bf16[256,128]{1,0:T(8,128)(2,1)S(1)}, f32[128,128]{1,0:T(8,128)S(1)}, f32[128,128]{1,0:T(8,128)S(1)}, bf16[4608,128]{1,0:T(8,128)(2,1)}, bf16[4...) custom-call(bf16[128,128]{1,0:T(8,128)(2,1)} %q_ref.1, bf16[128,128]{1,0:T(8,128)(2,1)} %k_ref.1, ...), custom_call_target="tpu_custom_call" | custom-call | tf_op jit(solution)/shard_map/local_span/pallas_call | solution.py:276
  7.2 12.4 %all-gather = bf16[1024,128]{1,0:T(8,128)(2,1)S(1)} all-gather(bf16[256,128]{1,0:T(8,128)(2,1)S(1)} %get-tuple-element.20), channel_id=2, replica_groups=mesh['zh'=8,'zl'=2,'c'=2,'tp'=16] {'zl','c'}, dimensions={0}, use_global_device_ids=true | all-gather | bytes 327680 | tf_op jit(solution)/shard_map/all_gather | solution.py:81
  20.9 0.8 broadcast_in_dim.6
  21.6 9.6 %all-to-all-start = ((bf16[16,64,128]{2,1,0:T(8,128)(2,1)}), bf16[16,64,128]{2,1,0:T(8,128)(2,1)S(1)}, u32[]{:S(2)}, u32[]{:S(2)}) async-start(bf16[16,64,128]{2,1,0:T(8,128)(2,1)} %broadcast_in_dim.6), calls=%async_computation | async-start | bytes 524288 | tf_op jit(solution)/shard_map/all_to_all | solution.py:98
  31.2 14.1 %all-to-all-done = bf16[16,64,128]{2,1,0:T(8,128)(2,1)S(1)} async-done(((bf16[16,64,128]{2,1,0:T(8,128)(2,1)}), bf16[16,64,128]{2,1,0:T(8,128)(2,1)S(1)}, u32[]{:S(2)}, u32[]{:S(2)}) %all-to-all-start) | async-done | bytes 262176 | tf_op jit(solution)/shard_map/all_to_all | solution.py:98
  45.3 6.8 %all-gather.1 = bf16[32,64,128]{2,1,0:T(8,128)(2,1)S(1)} all-gather(bf16[16,64,128]{2,1,0:T(8,128)(2,1)S(1)} %all-to-all-done), channel_id=3, replica_groups=mesh['zh'=8,'zl'=2,'c'=2,'tp'=16] {'c'}, dimensions={0}, use_global_device_ids=true | all-gather | bytes 786432 | tf_op jit(solution)/shard_map/all_gather | solution.py:99
  53.8 0.3 multiply_reduce_fusion.2
  54.2 1.1 convolution_convert_fusion
  55.3 6.9 %all-to-all-start.1 = ((bf16[16,8,2048]{2,1,0:T(8,128)(2,1)}), bf16[16,8,2048]{2,1,0:T(8,128)(2,1)S(1)}, u32[]{:S(2)}, u32[]{:S(2)}) async-start(bf16[16,8,2048]{2,1,0:T(8,128)(2,1)} %bitcast.31), calls=%async_computation.1 | async-start | bytes 1048576 | tf_op jit(solution)/shard_map/all_to_all | solution.py:301
  62.2 0.8 constant_dynamic-slice_fusion.2
  63.1 9.8 %all-to-all-done.1 = bf16[16,8,2048]{2,1,0:T(8,128)(2,1)S(1)} async-done(((bf16[16,8,2048]{2,1,0:T(8,128)(2,1)}), bf16[16,8,2048]{2,1,0:T(8,128)(2,1)S(1)}, u32[]{:S(2)}, u32[]{:S(2)}) %all-to-all-start.1) | async-done | bytes 524320 | tf_op jit(solution)/shard_map/all_to_all | solution.py:301
  73.5 0.2 convolution_convert_fusion.1
  73.7 0.7 reshape.122
  74.4 5.7 %all-to-all-start.2 = ((bf16[16,16,256]{2,1,0:T(8,128)(2,1)}), bf16[16,16,256]{2,1,0:T(8,128)(2,1)S(1)}, u32[]{:S(2)}, u32[]{:S(2)}) async-start(bf16[16,16,256]{2,1,0:T(8,128)(2,1)} %reshape.122), calls=%async_computation.2 | async-start | bytes 262144 | tf_op jit(solution)/shard_map/all_to_all | solution.py:323
  80.1 2.2 %collective-permute-start = (bf16[4608,128]{1,0:T(8,128)(2,1)}, bf16[4608,128]{1,0:T(8,128)(2,1)}, u32[]{:S(2)}, u32[]{:S(2)}) collective-permute-start(bf16[4608,128]{1,0:T(8,128)(2,1)} %get-tuple-element.27), channel_id=1, source_target_pairs={{0,1},{1,2},{2,3},{3,0},{4,5},{5,6},{6,7},{7,4},{8,9},{9,10},{10,1... | collective-permute-start | bytes 3538952 | tf_op jit(solution)/shard_map/ppermute | solution.py:74
  82.3 4.3 %collective-permute-start.1 = (bf16[4608,128]{1,0:T(8,128)(2,1)}, bf16[4608,128]{1,0:T(8,128)(2,1)}, u32[]{:S(2)}, u32[]{:S(2)}) collective-permute-start(bf16[4608,128]{1,0:T(8,128)(2,1)} %get-tuple-element.28), channel_id=1, source_target_pairs={{0,3},{1,0},{2,1},{3,2},{4,7},{5,4},{6,5},{7,6},{8,11},{9,8},{10,9... | collective-permute-start | bytes 3538952 | tf_op jit(solution)/shard_map/ppermute | solution.py:74
  86.6 1.9 collective-permute-start.2
  88.6 4.6 %collective-permute-start.3 = (bf16[4608,128]{1,0:T(8,128)(2,1)}, bf16[4608,128]{1,0:T(8,128)(2,1)}, u32[]{:S(2)}, u32[]{:S(2)}) collective-permute-start(bf16[4608,128]{1,0:T(8,128)(2,1)} %get-tuple-element.30), channel_id=1, source_target_pairs={{0,12},{1,13},{2,14},{3,15},{4,0},{5,1},{6,2},{7,3},{8,4},{9,5},{1... | collective-permute-start | bytes 3538952 | tf_op jit(solution)/shard_map/ppermute | solution.py:74
  93.4 1.1 broadcast_in_dim.7
  94.5 6.8 %all-to-all-start.3 = ((bf16[32,8,2048]{2,1,0:T(8,128)(2,1)}), bf16[32,8,2048]{2,1,0:T(8,128)(2,1)S(1)}, u32[]{:S(2)}, u32[]{:S(2)}) async-start(bf16[32,8,2048]{2,1,0:T(8,128)(2,1)} %bitcast.36), calls=%async_computation.3 | async-start | bytes 2097152 | tf_op jit(solution)/shard_map/all_to_all | solution.py:320
  101.3 8.1 %collective-permute-done.refs_3_ = bf16[4608,128]{1,0:T(8,128)(2,1)} collective-permute-done((bf16[4608,128]{1,0:T(8,128)(2,1)}, bf16[4608,128]{1,0:T(8,128)(2,1)}, u32[]{:S(2)}, u32[]{:S(2)}) %collective-permute-start) | collective-permute-done | bytes 1179680 | tf_op jit(solution)/shard_map/ppermute | solution.py:74
  109.4 0.6 collective-permute-done.1.refs_4_
  110.0 13.5 %collective-permute-done.2.refs_5_ = bf16[4608,128]{1,0:T(8,128)(2,1)} collective-permute-done((bf16[4608,128]{1,0:T(8,128)(2,1)}, bf16[4608,128]{1,0:T(8,128)(2,1)}, u32[]{:S(2)}, u32[]{:S(2)}) %collective-permute-start.2) | collective-permute-done | bytes 1179680 | tf_op jit(solution)/shard_map/ppermute | solution.py:74
  123.4 1.1 collective-permute-done.3.refs_6_
  124.5 4.6 %all-to-all-done.3 = bf16[32,8,2048]{2,1,0:T(8,128)(2,1)S(1)} async-done(((bf16[32,8,2048]{2,1,0:T(8,128)(2,1)}), bf16[32,8,2048]{2,1,0:T(8,128)(2,1)S(1)}, u32[]{:S(2)}, u32[]{:S(2)}) %all-to-all-start.3) | async-done | bytes 1048608 | tf_op jit(solution)/shard_map/all_to_all | solution.py:320
  129.2 8.1 %run_experts.1 = bf16[256,2048]{1,0:T(8,128)(2,1)S(1)} custom-call(bf16[256,2048]{1,0:T(8,128)(2,1)S(1)} %bitcast.158, bf16[2048,384]{1,0:T(8,128)(2,1)} %bitcast.161, bf16[2048,384]{1,0:T(8,128)(2,1)} %bitcast.163, bf16[384,2048]{1,0:T(8,128)(2,1)} %bitcast.165, bf16[4608,128]{1,0:T(8,128)(2,1)} %collective-permute-done.refs_3_, ...), custom_call_target="tpu_custom_call" | custom-call | tf_op jit(solution)/shard_map/run_experts/pallas_call | solution.py:330
  137.2 22.7 %all_to_all.35 = bf16[32,8,2048]{2,1,0:T(8,128)(2,1)S(1)} all-to-all(bf16[32,8,2048]{2,1,0:T(8,128)(2,1)S(1)} %bitcast.159), channel_id=1, replica_groups=mesh['zh'=8,'zl'=2,'c'=2,'tp'=16] {'c','tp'}, dimensions={0} | all-to-all | bytes 2097152 | tf_op jit(solution)/shard_map/all_to_all | solution.py:320
  160.2 0.8 copy.46
  161.0 11.5 %all-to-all-start.5 = ((bf16[16,2,2048]{2,1,0:T(2,128)(2,1)}), bf16[16,2,2048]{2,1,0:T(2,128)(2,1)S(1)}, u32[]{:S(2)}, u32[]{:S(2)}) async-start(bf16[16,2,2048]{2,1,0:T(2,128)(2,1)} %copy.46), calls=%async_computation.5 | async-start | bytes 262144 | tf_op jit(solution)/shard_map/all_to_all | solution.py:316
  172.5 11.9 %all-to-all-done.5 = bf16[16,2,2048]{2,1,0:T(2,128)(2,1)S(1)} async-done(((bf16[16,2,2048]{2,1,0:T(2,128)(2,1)}), bf16[16,2,2048]{2,1,0:T(2,128)(2,1)S(1)}, u32[]{:S(2)}, u32[]{:S(2)}) %all-to-all-start.5) | async-done | bytes 131104 | tf_op jit(solution)/shard_map/all_to_all | solution.py:316
  185.2 13.0 %all_to_all.36 = bf16[16,8,2048]{2,1,0:T(8,128)(2,1)S(1)} all-to-all(bf16[16,8,2048]{2,1,0:T(8,128)(2,1)S(1)} %broadcast_in_dim.8), channel_id=1, replica_groups=mesh['zh'=8,'zl'=2,'c'=2,'tp'=16] {'tp'}, dimensions={0} | all-to-all | bytes 1048576 | tf_op jit(solution)/shard_map/all_to_all | solution.py:116
  198.2 0.8 copy.53
  (60 shorter events, 4.6 us)
Async XLA Ops:
  0.0 54.1 %copy-start = (bf16[128,2048]{1,0:T(8,128)(2,1)S(1)}, bf16[128,2048]{1,0:T(8,128)(2,1)}, u32[]{:S(2)}) copy-start(bf16[128,2048]{1,0:T(8,128)(2,1)} %param.26) | copy-start | bytes 1572868
  21.6 23.7 %all-to-all-start = ((bf16[16,64,128]{2,1,0:T(8,128)(2,1)}), bf16[16,64,128]{2,1,0:T(8,128)(2,1)S(1)}, u32[]{:S(2)}, u32[]{:S(2)}) async-start(bf16[16,64,128]{2,1,0:T(8,128)(2,1)} %broadcast_in_dim.6), calls=%async_computation | async-start | bytes 524288 | tf_op jit(solution)/shard_map/all_to_all | solution.py:98
  52.3 1.9 copy-start.1
  52.3 1.9 copy-start.6
  54.1 8.9 %copy-start.4 = (s32[128,2]{0,1:T(2,128)S(1)}, s32[128,2]{0,1:T(2,128)}, u32[]{:S(2)}) copy-start(s32[128,2]{0,1:T(2,128)} %param.29) | copy-start | bytes 3076
  55.3 18.1 %copy-start.2 = (f32[2048]{0:T(1024)S(1)}, f32[2048]{0:T(1024)}, u32[]{:S(2)}) copy-start(f32[2048]{0:T(1024)} %param.27) | copy-start | bytes 24580
  55.3 17.6 %all-to-all-start.1 = ((bf16[16,8,2048]{2,1,0:T(8,128)(2,1)}), bf16[16,8,2048]{2,1,0:T(8,128)(2,1)S(1)}, u32[]{:S(2)}, u32[]{:S(2)}) async-start(bf16[16,8,2048]{2,1,0:T(8,128)(2,1)} %bitcast.31), calls=%async_computation.1 | async-start | bytes 1048576 | tf_op jit(solution)/shard_map/all_to_all | solution.py:301
  74.4 18.8 %all-to-all-start.2 = ((bf16[16,16,256]{2,1,0:T(8,128)(2,1)}), bf16[16,16,256]{2,1,0:T(8,128)(2,1)S(1)}, u32[]{:S(2)}, u32[]{:S(2)}) async-start(bf16[16,16,256]{2,1,0:T(8,128)(2,1)} %reshape.122), calls=%async_computation.2 | async-start | bytes 262144 | tf_op jit(solution)/shard_map/all_to_all | solution.py:323
  80.1 29.3 %collective-permute-start = (bf16[4608,128]{1,0:T(8,128)(2,1)}, bf16[4608,128]{1,0:T(8,128)(2,1)}, u32[]{:S(2)}, u32[]{:S(2)}) collective-permute-start(bf16[4608,128]{1,0:T(8,128)(2,1)} %get-tuple-element.27), channel_id=1, source_target_pairs={{0,1},{1,2},{2,3},{3,0},{4,5},{5,6},{6,7},{7,4},{8,9},{9,10},{10,1... | collective-permute-start | bytes 3538952 | tf_op jit(solution)/shard_map/ppermute | solution.py:74
  82.3 27.6 %collective-permute-start.1 = (bf16[4608,128]{1,0:T(8,128)(2,1)}, bf16[4608,128]{1,0:T(8,128)(2,1)}, u32[]{:S(2)}, u32[]{:S(2)}) collective-permute-start(bf16[4608,128]{1,0:T(8,128)(2,1)} %get-tuple-element.28), channel_id=1, source_target_pairs={{0,3},{1,0},{2,1},{3,2},{4,7},{5,4},{6,5},{7,6},{8,11},{9,8},{10,9... | collective-permute-start | bytes 3538952 | tf_op jit(solution)/shard_map/ppermute | solution.py:74
  86.6 36.8 %collective-permute-start.2 = (bf16[4608,128]{1,0:T(8,128)(2,1)}, bf16[4608,128]{1,0:T(8,128)(2,1)}, u32[]{:S(2)}, u32[]{:S(2)}) collective-permute-start(bf16[4608,128]{1,0:T(8,128)(2,1)} %get-tuple-element.29), channel_id=1, source_target_pairs={{0,4},{1,5},{2,6},{3,7},{4,8},{5,9},{6,10},{7,11},{8,12},{9,13},{1... | collective-permute-start | bytes 3538952 | tf_op jit(solution)/shard_map/ppermute | solution.py:74
  88.6 36.0 %collective-permute-start.3 = (bf16[4608,128]{1,0:T(8,128)(2,1)}, bf16[4608,128]{1,0:T(8,128)(2,1)}, u32[]{:S(2)}, u32[]{:S(2)}) collective-permute-start(bf16[4608,128]{1,0:T(8,128)(2,1)} %get-tuple-element.30), channel_id=1, source_target_pairs={{0,12},{1,13},{2,14},{3,15},{4,0},{5,1},{6,2},{7,3},{8,4},{9,5},{1... | collective-permute-start | bytes 3538952 | tf_op jit(solution)/shard_map/ppermute | solution.py:74
  94.5 34.7 %all-to-all-start.3 = ((bf16[32,8,2048]{2,1,0:T(8,128)(2,1)}), bf16[32,8,2048]{2,1,0:T(8,128)(2,1)S(1)}, u32[]{:S(2)}, u32[]{:S(2)}) async-start(bf16[32,8,2048]{2,1,0:T(8,128)(2,1)} %bitcast.36), calls=%async_computation.3 | async-start | bytes 2097152 | tf_op jit(solution)/shard_map/all_to_all | solution.py:320
  159.9 12.5 %copy-start.5 = (f32[128,2]{0,1:T(2,128)S(1)}, f32[128,2]{0,1:T(2,128)}, u32[]{:S(2)}) copy-start(f32[128,2]{0,1:T(2,128)} %param.30) | copy-start | bytes 3076
  160.1 24.9 %copy-start.3 = (f32[2048]{0:T(1024)S(1)}, f32[2048]{0:T(1024)}, u32[]{:S(2)}) copy-start(f32[2048]{0:T(1024)} %param.28) | copy-start | bytes 24580
  161.0 23.5 %all-to-all-start.5 = ((bf16[16,2,2048]{2,1,0:T(2,128)(2,1)}), bf16[16,2,2048]{2,1,0:T(2,128)(2,1)S(1)}, u32[]{:S(2)}, u32[]{:S(2)}) async-start(bf16[16,2,2048]{2,1,0:T(2,128)(2,1)} %copy.46), calls=%async_computation.5 | async-start | bytes 262144 | tf_op jit(solution)/shard_map/all_to_all | solution.py:316

commit v11 on v10

--- a/solution.py
+++ b/solution.py
@@ -62,6 +62,31 @@
         copy.wait()
 
 
+def pack_experts(*refs):
+    tables, outs, bufs, part_bufs, sems = refs[:3], refs[3:7], refs[7:10], refs[10:14], refs[14]
+    copies = [pltpu.make_async_copy(x, y, sems.at[k]) for k, (x, y) in enumerate(zip(tables, bufs))]
+    for copy in copies:
+        copy.start()
+    for copy in copies:
+        copy.wait()
+    pack_parts(*bufs, part_bufs, outs, sems.at[3:])
+
+
+def packed_parts(tables):
+    packed = (3 * tables[0].size // 4 // LANES, LANES)
+    anywhere = pl.BlockSpec(memory_space=pl.ANY)
+    return pl.pallas_call(
+        pack_experts,
+        out_shape=(jax.ShapeDtypeStruct(packed, jnp.bfloat16),) * 4,
+        in_specs=[anywhere] * 3,
+        out_specs=(anywhere,) * 4,
+        scratch_shapes=[pltpu.VMEM(x.shape, x.dtype) for x in tables]
+        + [pltpu.VMEM(packed, jnp.bfloat16)] * 4
+        + [pltpu.SemaphoreType.DMA((15,))],
+        name="pack_experts",
+    )(*tables)
+
+
 def spread(parts, side, start=0):
     out = []
     ways = ((0, 1), (0, side - 1), (1, 0), (side - 1, 0))
@@ -75,7 +100,7 @@
     return out
 
 
-def entering(own, parts, side):
+def entering(own, tables, side):
     kind = jnp.bfloat16
     zh, zl, c = (lax.axis_index(axis) for axis in SP)
     near = lax.all_gather(own, ("zl", "c")).astype(jnp.float32)
@@ -92,8 +117,9 @@
     group = jnp.concatenate([map_all, state_all], 0).astype(kind)
     quarter = lax.dynamic_slice_in_dim(group, (2 * zl + c) * (width // 2), width // 2, 0)
     count = lax.axis_size(Z)
-    quarter, parts = lax.optimization_barrier((quarter, parts))
-    parts = spread(parts, side)
+    quarter, tables = lax.optimization_barrier((quarter, tables))
+    parts = packed_parts(tables)
+    early = spread(parts[:1], side)
     far = jnp.broadcast_to(quarter[None], (count, *quarter.shape))
     far = lax.all_to_all(far, Z, 0, 0, tiled=True)
     far = lax.all_gather(far, "c")
@@ -102,7 +128,7 @@
     state = jnp.zeros((width, width), jnp.float32)
     for k in range(count // 2 - 1):
         state = jnp.where(k < zh, mm(far[k, :width], state) + far[k, width:], state)
-    return mm(map_in, state) + state_in, parts
+    return mm(map_in, state) + state_in, early, parts[1:]
 
 
 def in_blocks(x, dim, length):
@@ -132,12 +158,7 @@
     return center * lax.rsqrt(jnp.mean(center * center, -1, keepdims=True) + 1e-05) * gain
 
 
-def local_span(q_ref, k_ref, v_ref, beta_ref, decay_ref, rate_ref, *refs):
-    tables, (both_ref, mix_ref, out_ref), outs = refs[:3], refs[3:6], refs[6:10]
-    bufs, part_bufs, sems = refs[10:13], refs[13:17], refs[17]
-    copies = [pltpu.make_async_copy(x, y, sems.at[k]) for k, (x, y) in enumerate(zip(tables, bufs))]
-    for copy in copies:
-        copy.start()
+def local_span(q_ref, k_ref, v_ref, beta_ref, decay_ref, rate_ref, both_ref, mix_ref, out_ref):
     size = HEAD_FEATURES
     row = lax.broadcasted_iota(jnp.int32, (size, size), 0)
     col = lax.broadcasted_iota(jnp.int32, (size, size), 1)
@@ -191,9 +212,6 @@
     seen = dot(scores, solved)
     mix_ref[...] = query * (query_scale * grown) - seen[:, :size]
     out_ref[...] = seen[:, size:]
-    for copy in copies:
-        copy.wait()
-    pack_parts(*bufs, part_bufs, outs, sems.at[3:])
 
 
 def run_experts(rows_ref, *refs):
@@ -272,23 +290,18 @@
     split_count = lax.axis_size("tp")
     side = round(split_count**0.5)
     tables = (expert_gate[0], expert_up[0], expert_down[0])
-    packed = (3 * tables[0].size // 4 // LANES, LANES)
-    both, mix, local, *parts = pl.pallas_call(
+    both, mix, local = pl.pallas_call(
         local_span,
         out_shape=(
             pltpu.VMEM((2 * HEAD_FEATURES, HEAD_FEATURES), jnp.bfloat16),
             pltpu.VMEM((length, HEAD_FEATURES), jnp.float32),
             pltpu.VMEM((length, HEAD_FEATURES), jnp.float32),
-        )
-        + (jax.ShapeDtypeStruct(packed, jnp.bfloat16),) * 4,
-        in_specs=[vmem] * 5 + [pl.BlockSpec(memory_space=pltpu.SMEM)] + [anywhere] * 3,
-        out_specs=(vmem,) * 3 + (anywhere,) * 4,
-        scratch_shapes=[pltpu.VMEM(x.shape, x.dtype) for x in tables]
-        + [pltpu.VMEM(packed, jnp.bfloat16)] * 4
-        + [pltpu.SemaphoreType.DMA((15,))],
+        ),
+        in_specs=[vmem] * 5 + [pl.BlockSpec(memory_space=pltpu.SMEM)],
+        out_specs=(vmem,) * 3,
         name="local_span",
-    )(queries, keys, values, beta_logit, decay_logit, decay_log, *tables)
-    state, early = entering(both, parts[:2], side)
+    )(queries, keys, values, beta_logit, decay_logit, decay_log)
+    state, early, late = entering(both, tables, side)
     mixed = local + mm(mix, state)
     normalized = mixed * lax.rsqrt(jnp.mean(mixed * mixed, -1, keepdims=True) + 1e-06) * head_gain
     gated = (normalized * jax.nn.silu(out_gate.astype(jnp.float32))).astype(jnp.bfloat16)
@@ -296,8 +309,8 @@
     rows = length // split_count
     first = lax.axis_index("tp") * rows
     product = jnp.dot(gated, out_weight, preferred_element_type=jnp.float32).astype(jnp.bfloat16)
-    product, late = lax.optimization_barrier((product, parts[2:]))
-    late = spread(late, side, 2)
+    product, late = lax.optimization_barrier((product, late))
+    late = spread(late, side, 1)
     product = lax.all_to_all(in_blocks(product, 0, split_count), "tp", 0, 0, tiled=True)
     projected = jnp.sum(product.astype(jnp.float32), axis=0)
     residual = lax.optimization_barrier(lax.dynamic_slice_in_dim(residual_in, first, rows, 0))

time: 203 us -> 199 us (0.980)
  waiting for transfers between devices: 63.7 us -> 58 us
    pallas_call x0 -> x1, Pallas kernels: none -> 5.7 us  [packed_parts(): pl.pallas_call(pack_experts, out_shape=(jax.ShapeDtypeStruct(packed, jnp....]
    all_to_all x1, waiting for transfers between devices: 14.1 us -> 8.42 us  [entering(): far = lax.all_to_all(far, Z, 0, 0, tiled=True)]
    pallas_call x1, Pallas kernels: 6.53 us -> 2.73 us  [per_device(): pl.pallas_call(local_span, out_shape=(pltpu.VMEM((2 * HEAD_FEATURES, HEAD...]
  transfers between devices with their start and end apart: 9 -> 9, of which waited for: 8 -> 8; matrix products, arithmetic and copies ran while one was open for 1% -> 1% of each run, Pallas kernels for 0% -> 3%
where the time goes in v11:
time: 199 us; the launch traced here: 195 us
  waiting for transfers between devices  58 us (29%)
  blocking collectives  55 us (28%)
  starting transfers between devices  53.5 us (27%)
  Pallas kernels  16.5 us (8%)
  local copies, waits for them, and re-layouts  5.37 us (3%)
  matrix products  4.31 us (2%)
    ppermute x4, waiting for transfers between devices, spread(): out.append(lax.ppermute(part, 'tp', pairs))  23.2 us
    all_to_all x1, blocking collectives, in_plane(): return lax.all_to_all(x, PLANE, 0, 0, tiled=True)  22.7 us
    all_to_all x1, blocking collectives, copy_for_each(): lax.all_to_all(jnp.broadcast_to(x[None], (length, *x.shape)), axis, 0, 0,...  13 us
    ppermute x4, starting transfers between devices, spread(): out.append(lax.ppermute(part, 'tp', pairs))  13 us
    all_gather x1, blocking collectives, entering(): near = lax.all_gather(own, ('zl', 'c')).astype(jnp.float32)  12.5 us
    all_to_all x1, waiting for transfers between devices, along_z(): out = lax.all_to_all(x.reshape(chips, 2, width), Z, 0, 0, tiled=True)  11.9 us
    all_to_all x1, starting transfers between devices, along_z(): out = lax.all_to_all(x.reshape(chips, 2, width), Z, 0, 0, tiled=True)  11.5 us
    all_to_all x1, waiting for transfers between devices, per_device(): lax.all_to_all(in_blocks(product, 0, split_count), 'tp', 0, 0, tiled=True)  9.8 us
  transfers between devices with their start and end apart: 9, of which 8 were waited for; matrix products, arithmetic and copies ran while one was open for 1% of the time, Pallas kernels for 3%

profile of v11, /device:TPU:1, one launch (start us, length us, event | category | flops | bytes accessed | tf_op | source)
XLA Modules:
  0.0 195.2 jit_solution(9557602808422355801)
XLA Ops:
  0.7 2.7 %local_span.1 = (bf16[256,128]{1,0:T(8,128)(2,1)S(1)}, f32[128,128]{1,0:T(8,128)S(1)}, f32[128,128]{1,0:T(8,128)S(1)}) custom-call(bf16[128,128]{1,0:T(8,128)(2,1)} %q_ref.1, bf16[128,128]{1,0:T(8,128)(2,1)} %k_ref.1, bf16[128,128]{1,0:T(8,128)(2,1)} %v_ref.1, bf16[1,128]{1,0:T(2,128)(2,1)} %beta_ref.1, bf16[1,128]{1,0:T(2,128)(2,1)} %decay_ref.1, ...), custom_call_target="tpu_custom_call" | custom-call | tf_op jit(solution)/shard_map/local_span/pallas_call | solution.py:293
  3.4 12.5 %all-gather = bf16[1024,128]{1,0:T(8,128)(2,1)S(1)} all-gather(bf16[256,128]{1,0:T(8,128)(2,1)S(1)} %get-tuple-element.22), channel_id=2, replica_groups=mesh['zh'=8,'zl'=2,'c'=2,'tp'=16] {'zl','c'}, dimensions={0}, use_global_device_ids=true | all-gather | bytes 327680 | tf_op jit(solution)/shard_map/all_gather | solution.py:106
  17.1 0.8 broadcast_in_dim.6
  17.8 9.6 %all-to-all-start = ((bf16[16,64,128]{2,1,0:T(8,128)(2,1)}), bf16[16,64,128]{2,1,0:T(8,128)(2,1)S(1)}, u32[]{:S(2)}, u32[]{:S(2)}) async-start(bf16[16,64,128]{2,1,0:T(8,128)(2,1)} %broadcast_in_dim.6), calls=%async_computation | async-start | bytes 524288 | tf_op jit(solution)/shard_map/all_to_all | solution.py:124
  27.4 5.7 %pack_experts.1 = (bf16[4608,128]{1,0:T(8,128)(2,1)}, bf16[4608,128]{1,0:T(8,128)(2,1)}, bf16[4608,128]{1,0:T(8,128)(2,1)}, bf16[4608,128]{1,0:T(8,128)(2,1)}) custom-call(bf16[2048,384]{1,0:T(8,128)(2,1)} %bitcast.160, bf16[2048,384]{1,0:T(8,128)(2,1)} %bitcast.162, bf16[384,2048]{1,0:T(8,128)(2,1)} %bitcast.164), custom_call_target="tpu_custom_call" | custom-call | tf_op jit(solution)/shard_map/pack_experts/pallas_call | solution.py:78
  33.1 8.4 %all-to-all-done = bf16[16,64,128]{2,1,0:T(8,128)(2,1)S(1)} async-done(((bf16[16,64,128]{2,1,0:T(8,128)(2,1)}), bf16[16,64,128]{2,1,0:T(8,128)(2,1)S(1)}, u32[]{:S(2)}, u32[]{:S(2)}) %all-to-all-start) | async-done | bytes 262176 | tf_op jit(solution)/shard_map/all_to_all | solution.py:124
  41.6 6.8 %all-gather.1 = bf16[32,64,128]{2,1,0:T(8,128)(2,1)S(1)} all-gather(bf16[16,64,128]{2,1,0:T(8,128)(2,1)S(1)} %all-to-all-done), channel_id=3, replica_groups=mesh['zh'=8,'zl'=2,'c'=2,'tp'=16] {'c'}, dimensions={0}, use_global_device_ids=true | all-gather | bytes 786432 | tf_op jit(solution)/shard_map/all_gather | solution.py:125
  50.0 0.3 multiply_reduce_fusion.2
  50.4 1.1 convolution_convert_fusion
  51.5 6.9 %all-to-all-start.1 = ((bf16[16,8,2048]{2,1,0:T(8,128)(2,1)}), bf16[16,8,2048]{2,1,0:T(8,128)(2,1)S(1)}, u32[]{:S(2)}, u32[]{:S(2)}) async-start(bf16[16,8,2048]{2,1,0:T(8,128)(2,1)} %bitcast.31), calls=%async_computation.1 | async-start | bytes 1048576 | tf_op jit(solution)/shard_map/all_to_all | solution.py:314
  58.4 0.8 constant_dynamic-slice_fusion.2
  59.3 9.8 %all-to-all-done.1 = bf16[16,8,2048]{2,1,0:T(8,128)(2,1)S(1)} async-done(((bf16[16,8,2048]{2,1,0:T(8,128)(2,1)}), bf16[16,8,2048]{2,1,0:T(8,128)(2,1)S(1)}, u32[]{:S(2)}, u32[]{:S(2)}) %all-to-all-start.1) | async-done | bytes 524320 | tf_op jit(solution)/shard_map/all_to_all | solution.py:314
  69.9 0.7 reshape.122
  70.6 5.7 %all-to-all-start.2 = ((bf16[16,16,256]{2,1,0:T(8,128)(2,1)}), bf16[16,16,256]{2,1,0:T(8,128)(2,1)S(1)}, u32[]{:S(2)}, u32[]{:S(2)}) async-start(bf16[16,16,256]{2,1,0:T(8,128)(2,1)} %reshape.122), calls=%async_computation.2 | async-start | bytes 262144 | tf_op jit(solution)/shard_map/all_to_all | solution.py:336
  76.3 2.2 %collective-permute-start = (bf16[4608,128]{1,0:T(8,128)(2,1)}, bf16[4608,128]{1,0:T(8,128)(2,1)}, u32[]{:S(2)}, u32[]{:S(2)}) collective-permute-start(bf16[4608,128]{1,0:T(8,128)(2,1)} %get-tuple-element.31), channel_id=1, source_target_pairs={{0,1},{1,2},{2,3},{3,0},{4,5},{5,6},{6,7},{7,4},{8,9},{9,10},{10,1... | collective-permute-start | bytes 3538952 | tf_op jit(solution)/shard_map/ppermute | solution.py:99
  78.5 4.3 %collective-permute-start.1 = (bf16[4608,128]{1,0:T(8,128)(2,1)}, bf16[4608,128]{1,0:T(8,128)(2,1)}, u32[]{:S(2)}, u32[]{:S(2)}) collective-permute-start(bf16[4608,128]{1,0:T(8,128)(2,1)} %get-tuple-element.32), channel_id=1, source_target_pairs={{0,3},{1,0},{2,1},{3,2},{4,7},{5,4},{6,5},{7,6},{8,11},{9,8},{10,9... | collective-permute-start | bytes 3538952 | tf_op jit(solution)/shard_map/ppermute | solution.py:99
  82.8 1.9 collective-permute-start.2
  84.8 4.6 %collective-permute-start.3 = (bf16[4608,128]{1,0:T(8,128)(2,1)}, bf16[4608,128]{1,0:T(8,128)(2,1)}, u32[]{:S(2)}, u32[]{:S(2)}) collective-permute-start(bf16[4608,128]{1,0:T(8,128)(2,1)} %get-tuple-element.34), channel_id=1, source_target_pairs={{0,12},{1,13},{2,14},{3,15},{4,0},{5,1},{6,2},{7,3},{8,4},{9,5},{1... | collective-permute-start | bytes 3538952 | tf_op jit(solution)/shard_map/ppermute | solution.py:99
  89.6 1.1 broadcast_in_dim.7
  90.7 6.8 %all-to-all-start.3 = ((bf16[32,8,2048]{2,1,0:T(8,128)(2,1)}), bf16[32,8,2048]{2,1,0:T(8,128)(2,1)S(1)}, u32[]{:S(2)}, u32[]{:S(2)}) async-start(bf16[32,8,2048]{2,1,0:T(8,128)(2,1)} %bitcast.36), calls=%async_computation.3 | async-start | bytes 2097152 | tf_op jit(solution)/shard_map/all_to_all | solution.py:333
  97.5 8.1 %collective-permute-done.refs_3_ = bf16[4608,128]{1,0:T(8,128)(2,1)} collective-permute-done((bf16[4608,128]{1,0:T(8,128)(2,1)}, bf16[4608,128]{1,0:T(8,128)(2,1)}, u32[]{:S(2)}, u32[]{:S(2)}) %collective-permute-start) | collective-permute-done | bytes 1179680 | tf_op jit(solution)/shard_map/ppermute | solution.py:99
  105.6 0.6 collective-permute-done.1.refs_4_
  106.2 13.5 %collective-permute-done.2.refs_5_ = bf16[4608,128]{1,0:T(8,128)(2,1)} collective-permute-done((bf16[4608,128]{1,0:T(8,128)(2,1)}, bf16[4608,128]{1,0:T(8,128)(2,1)}, u32[]{:S(2)}, u32[]{:S(2)}) %collective-permute-start.2) | collective-permute-done | bytes 1179680 | tf_op jit(solution)/shard_map/ppermute | solution.py:99
  119.6 1.1 collective-permute-done.3.refs_6_
  120.7 4.6 %all-to-all-done.3 = bf16[32,8,2048]{2,1,0:T(8,128)(2,1)S(1)} async-done(((bf16[32,8,2048]{2,1,0:T(8,128)(2,1)}), bf16[32,8,2048]{2,1,0:T(8,128)(2,1)S(1)}, u32[]{:S(2)}, u32[]{:S(2)}) %all-to-all-start.3) | async-done | bytes 1048608 | tf_op jit(solution)/shard_map/all_to_all | solution.py:333
  125.4 8.1 %run_experts.1 = bf16[256,2048]{1,0:T(8,128)(2,1)S(1)} custom-call(bf16[256,2048]{1,0:T(8,128)(2,1)S(1)} %bitcast.158, bf16[2048,384]{1,0:T(8,128)(2,1)} %bitcast.161, bf16[2048,384]{1,0:T(8,128)(2,1)} %bitcast.163, bf16[384,2048]{1,0:T(8,128)(2,1)} %bitcast.165, bf16[4608,128]{1,0:T(8,128)(2,1)} %collective-permute-done.refs_3_, ...), custom_call_target="tpu_custom_call" | custom-call | tf_op jit(solution)/shard_map/run_experts/pallas_call | solution.py:343
  133.5 22.7 %all_to_all.35 = bf16[32,8,2048]{2,1,0:T(8,128)(2,1)S(1)} all-to-all(bf16[32,8,2048]{2,1,0:T(8,128)(2,1)S(1)} %bitcast.159), channel_id=1, replica_groups=mesh['zh'=8,'zl'=2,'c'=2,'tp'=16] {'c','tp'}, dimensions={0} | all-to-all | bytes 2097152 | tf_op jit(solution)/shard_map/all_to_all | solution.py:333
  156.4 0.8 copy.46
  157.2 11.5 %all-to-all-start.5 = ((bf16[16,2,2048]{2,1,0:T(2,128)(2,1)}), bf16[16,2,2048]{2,1,0:T(2,128)(2,1)S(1)}, u32[]{:S(2)}, u32[]{:S(2)}) async-start(bf16[16,2,2048]{2,1,0:T(2,128)(2,1)} %copy.46), calls=%async_computation.5 | async-start | bytes 262144 | tf_op jit(solution)/shard_map/all_to_all | solution.py:329
  168.7 11.9 %all-to-all-done.5 = bf16[16,2,2048]{2,1,0:T(2,128)(2,1)S(1)} async-done(((bf16[16,2,2048]{2,1,0:T(2,128)(2,1)}), bf16[16,2,2048]{2,1,0:T(2,128)(2,1)S(1)}, u32[]{:S(2)}, u32[]{:S(2)}) %all-to-all-start.5) | async-done | bytes 131104 | tf_op jit(solution)/shard_map/all_to_all | solution.py:329
  181.4 13.0 %all_to_all.36 = bf16[16,8,2048]{2,1,0:T(8,128)(2,1)S(1)} all-to-all(bf16[16,8,2048]{2,1,0:T(8,128)(2,1)S(1)} %broadcast_in_dim.8), channel_id=1, replica_groups=mesh['zh'=8,'zl'=2,'c'=2,'tp'=16] {'tp'}, dimensions={0} | all-to-all | bytes 1048576 | tf_op jit(solution)/shard_map/all_to_all | solution.py:142
  194.4 0.8 copy.53
  (61 shorter events, 4.8 us)
Async XLA Ops:
  0.0 50.4 %copy-start = (bf16[128,2048]{1,0:T(8,128)(2,1)S(1)}, bf16[128,2048]{1,0:T(8,128)(2,1)}, u32[]{:S(2)}) copy-start(bf16[128,2048]{1,0:T(8,128)(2,1)} %param.26) | copy-start | bytes 1572868
  17.8 23.7 %all-to-all-start = ((bf16[16,64,128]{2,1,0:T(8,128)(2,1)}), bf16[16,64,128]{2,1,0:T(8,128)(2,1)S(1)}, u32[]{:S(2)}, u32[]{:S(2)}) async-start(bf16[16,64,128]{2,1,0:T(8,128)(2,1)} %broadcast_in_dim.6), calls=%async_computation | async-start | bytes 524288 | tf_op jit(solution)/shard_map/all_to_all | solution.py:124
  48.5 1.9 copy-start.1
  48.5 1.9 copy-start.6
  50.3 8.9 %copy-start.4 = (s32[128,2]{0,1:T(2,128)S(1)}, s32[128,2]{0,1:T(2,128)}, u32[]{:S(2)}) copy-start(s32[128,2]{0,1:T(2,128)} %param.29) | copy-start | bytes 3076
  51.5 18.0 %copy-start.2 = (f32[2048]{0:T(1024)S(1)}, f32[2048]{0:T(1024)}, u32[]{:S(2)}) copy-start(f32[2048]{0:T(1024)} %param.27) | copy-start | bytes 24580
  51.5 17.6 %all-to-all-start.1 = ((bf16[16,8,2048]{2,1,0:T(8,128)(2,1)}), bf16[16,8,2048]{2,1,0:T(8,128)(2,1)S(1)}, u32[]{:S(2)}, u32[]{:S(2)}) async-start(bf16[16,8,2048]{2,1,0:T(8,128)(2,1)} %bitcast.31), calls=%async_computation.1 | async-start | bytes 1048576 | tf_op jit(solution)/shard_map/all_to_all | solution.py:314
  70.6 18.8 %all-to-all-start.2 = ((bf16[16,16,256]{2,1,0:T(8,128)(2,1)}), bf16[16,16,256]{2,1,0:T(8,128)(2,1)S(1)}, u32[]{:S(2)}, u32[]{:S(2)}) async-start(bf16[16,16,256]{2,1,0:T(8,128)(2,1)} %reshape.122), calls=%async_computation.2 | async-start | bytes 262144 | tf_op jit(solution)/shard_map/all_to_all | solution.py:336
  76.3 29.3 %collective-permute-start = (bf16[4608,128]{1,0:T(8,128)(2,1)}, bf16[4608,128]{1,0:T(8,128)(2,1)}, u32[]{:S(2)}, u32[]{:S(2)}) collective-permute-start(bf16[4608,128]{1,0:T(8,128)(2,1)} %get-tuple-element.31), channel_id=1, source_target_pairs={{0,1},{1,2},{2,3},{3,0},{4,5},{5,6},{6,7},{7,4},{8,9},{9,10},{10,1... | collective-permute-start | bytes 3538952 | tf_op jit(solution)/shard_map/ppermute | solution.py:99
  78.5 27.6 %collective-permute-start.1 = (bf16[4608,128]{1,0:T(8,128)(2,1)}, bf16[4608,128]{1,0:T(8,128)(2,1)}, u32[]{:S(2)}, u32[]{:S(2)}) collective-permute-start(bf16[4608,128]{1,0:T(8,128)(2,1)} %get-tuple-element.32), channel_id=1, source_target_pairs={{0,3},{1,0},{2,1},{3,2},{4,7},{5,4},{6,5},{7,6},{8,11},{9,8},{10,9... | collective-permute-start | bytes 3538952 | tf_op jit(solution)/shard_map/ppermute | solution.py:99
  82.8 36.8 %collective-permute-start.2 = (bf16[4608,128]{1,0:T(8,128)(2,1)}, bf16[4608,128]{1,0:T(8,128)(2,1)}, u32[]{:S(2)}, u32[]{:S(2)}) collective-permute-start(bf16[4608,128]{1,0:T(8,128)(2,1)} %get-tuple-element.33), channel_id=1, source_target_pairs={{0,4},{1,5},{2,6},{3,7},{4,8},{5,9},{6,10},{7,11},{8,12},{9,13},{1... | collective-permute-start | bytes 3538952 | tf_op jit(solution)/shard_map/ppermute | solution.py:99
  84.8 36.0 %collective-permute-start.3 = (bf16[4608,128]{1,0:T(8,128)(2,1)}, bf16[4608,128]{1,0:T(8,128)(2,1)}, u32[]{:S(2)}, u32[]{:S(2)}) collective-permute-start(bf16[4608,128]{1,0:T(8,128)(2,1)} %get-tuple-element.34), channel_id=1, source_target_pairs={{0,12},{1,13},{2,14},{3,15},{4,0},{5,1},{6,2},{7,3},{8,4},{9,5},{1... | collective-permute-start | bytes 3538952 | tf_op jit(solution)/shard_map/ppermute | solution.py:99
  90.7 34.7 %all-to-all-start.3 = ((bf16[32,8,2048]{2,1,0:T(8,128)(2,1)}), bf16[32,8,2048]{2,1,0:T(8,128)(2,1)S(1)}, u32[]{:S(2)}, u32[]{:S(2)}) async-start(bf16[32,8,2048]{2,1,0:T(8,128)(2,1)} %bitcast.36), calls=%async_computation.3 | async-start | bytes 2097152 | tf_op jit(solution)/shard_map/all_to_all | solution.py:333
  156.1 12.5 %copy-start.5 = (f32[128,2]{0,1:T(2,128)S(1)}, f32[128,2]{0,1:T(2,128)}, u32[]{:S(2)}) copy-start(f32[128,2]{0,1:T(2,128)} %param.30) | copy-start | bytes 3076
  156.3 24.9 %copy-start.3 = (f32[2048]{0:T(1024)S(1)}, f32[2048]{0:T(1024)}, u32[]{:S(2)}) copy-start(f32[2048]{0:T(1024)} %param.28) | copy-start | bytes 24580
  157.2 23.5 %all-to-all-start.5 = ((bf16[16,2,2048]{2,1,0:T(2,128)(2,1)}), bf16[16,2,2048]{2,1,0:T(2,128)(2,1)S(1)}, u32[]{:S(2)}, u32[]{:S(2)}) async-start(bf16[16,2,2048]{2,1,0:T(2,128)(2,1)} %copy.46), calls=%async_computation.5 | async-start | bytes 262144 | tf_op jit(solution)/shard_map/all_to_all | solution.py:329

commit v12 on v11

--- a/solution.py
+++ b/solution.py
@@ -119,7 +119,7 @@
     count = lax.axis_size(Z)
     quarter, tables = lax.optimization_barrier((quarter, tables))
     parts = packed_parts(tables)
-    early = spread(parts[:1], side)
+    early = spread(parts[:2], side)
     far = jnp.broadcast_to(quarter[None], (count, *quarter.shape))
     far = lax.all_to_all(far, Z, 0, 0, tiled=True)
     far = lax.all_gather(far, "c")
@@ -128,7 +128,7 @@
     state = jnp.zeros((width, width), jnp.float32)
     for k in range(count // 2 - 1):
         state = jnp.where(k < zh, mm(far[k, :width], state) + far[k, width:], state)
-    return mm(map_in, state) + state_in, early, parts[1:]
+    return mm(map_in, state) + state_in, early, parts[2:]
 
 
 def in_blocks(x, dim, length):
@@ -310,7 +310,7 @@
     first = lax.axis_index("tp") * rows
     product = jnp.dot(gated, out_weight, preferred_element_type=jnp.float32).astype(jnp.bfloat16)
     product, late = lax.optimization_barrier((product, late))
-    late = spread(late, side, 1)
+    late = spread(late, side, 2)
     product = lax.all_to_all(in_blocks(product, 0, split_count), "tp", 0, 0, tiled=True)
     projected = jnp.sum(product.astype(jnp.float32), axis=0)
     residual = lax.optimization_barrier(lax.dynamic_slice_in_dim(residual_in, first, rows, 0))

time: 199 us -> 199 us (level)
  no operation moved by 1% of the time
where the time goes in v12:
time: 199 us; the launch traced here: 195 us
  waiting for transfers between devices  58 us (29%)
  blocking collectives  55 us (28%)
  starting transfers between devices  53.5 us (27%)
  Pallas kernels  16.5 us (8%)
  local copies, waits for them, and re-layouts  5.37 us (3%)
  matrix products  4.31 us (2%)
    ppermute x4, waiting for transfers between devices, spread(): out.append(lax.ppermute(part, 'tp', pairs))  23.2 us
    all_to_all x1, blocking collectives, in_plane(): return lax.all_to_all(x, PLANE, 0, 0, tiled=True)  22.7 us
    all_to_all x1, blocking collectives, copy_for_each(): lax.all_to_all(jnp.broadcast_to(x[None], (length, *x.shape)), axis, 0, 0,...  13 us
    ppermute x4, starting transfers between devices, spread(): out.append(lax.ppermute(part, 'tp', pairs))  13 us
    all_gather x1, blocking collectives, entering(): near = lax.all_gather(own, ('zl', 'c')).astype(jnp.float32)  12.5 us
    all_to_all x1, waiting for transfers between devices, along_z(): out = lax.all_to_all(x.reshape(chips, 2, width), Z, 0, 0, tiled=True)  11.9 us
    all_to_all x1, starting transfers between devices, along_z(): out = lax.all_to_all(x.reshape(chips, 2, width), Z, 0, 0, tiled=True)  11.5 us
    all_to_all x1, waiting for transfers between devices, per_device(): lax.all_to_all(in_blocks(product, 0, split_count), 'tp', 0, 0, tiled=True)  9.8 us
  transfers between devices with their start and end apart: 9, of which 8 were waited for; matrix products, arithmetic and copies ran while one was open for 1% of the time, Pallas kernels for 3%

profile of v12, /device:TPU:1, one launch (start us, length us, event | category | flops | bytes accessed | tf_op | source)
XLA Modules:
  0.0 195.2 jit_solution(9557602808422355801)
XLA Ops:
  0.7 2.7 %local_span.1 = (bf16[256,128]{1,0:T(8,128)(2,1)S(1)}, f32[128,128]{1,0:T(8,128)S(1)}, f32[128,128]{1,0:T(8,128)S(1)}) custom-call(bf16[128,128]{1,0:T(8,128)(2,1)} %q_ref.1, bf16[128,128]{1,0:T(8,128)(2,1)} %k_ref.1, bf16[128,128]{1,0:T(8,128)(2,1)} %v_ref.1, bf16[1,128]{1,0:T(2,128)(2,1)} %beta_ref.1, bf16[1,128]{1,0:T(2,128)(2,1)} %decay_ref.1, ...), custom_call_target="tpu_custom_call" | custom-call | tf_op jit(solution)/shard_map/local_span/pallas_call | solution.py:293
  3.4 12.5 %all-gather = bf16[1024,128]{1,0:T(8,128)(2,1)S(1)} all-gather(bf16[256,128]{1,0:T(8,128)(2,1)S(1)} %get-tuple-element.21), channel_id=2, replica_groups=mesh['zh'=8,'zl'=2,'c'=2,'tp'=16] {'zl','c'}, dimensions={0}, use_global_device_ids=true | all-gather | bytes 327680 | tf_op jit(solution)/shard_map/all_gather | solution.py:106
  17.1 0.8 broadcast_in_dim.6
  17.8 9.6 %all-to-all-start = ((bf16[16,64,128]{2,1,0:T(8,128)(2,1)}), bf16[16,64,128]{2,1,0:T(8,128)(2,1)S(1)}, u32[]{:S(2)}, u32[]{:S(2)}) async-start(bf16[16,64,128]{2,1,0:T(8,128)(2,1)} %broadcast_in_dim.6), calls=%async_computation | async-start | bytes 524288 | tf_op jit(solution)/shard_map/all_to_all | solution.py:124
  27.4 5.7 %pack_experts.1 = (bf16[4608,128]{1,0:T(8,128)(2,1)}, bf16[4608,128]{1,0:T(8,128)(2,1)}, bf16[4608,128]{1,0:T(8,128)(2,1)}, bf16[4608,128]{1,0:T(8,128)(2,1)}) custom-call(bf16[2048,384]{1,0:T(8,128)(2,1)} %bitcast.160, bf16[2048,384]{1,0:T(8,128)(2,1)} %bitcast.162, bf16[384,2048]{1,0:T(8,128)(2,1)} %bitcast.164), custom_call_target="tpu_custom_call" | custom-call | tf_op jit(solution)/shard_map/pack_experts/pallas_call | solution.py:78
  33.1 8.4 %all-to-all-done = bf16[16,64,128]{2,1,0:T(8,128)(2,1)S(1)} async-done(((bf16[16,64,128]{2,1,0:T(8,128)(2,1)}), bf16[16,64,128]{2,1,0:T(8,128)(2,1)S(1)}, u32[]{:S(2)}, u32[]{:S(2)}) %all-to-all-start) | async-done | bytes 262176 | tf_op jit(solution)/shard_map/all_to_all | solution.py:124
  41.6 6.8 %all-gather.1 = bf16[32,64,128]{2,1,0:T(8,128)(2,1)S(1)} all-gather(bf16[16,64,128]{2,1,0:T(8,128)(2,1)S(1)} %all-to-all-done), channel_id=3, replica_groups=mesh['zh'=8,'zl'=2,'c'=2,'tp'=16] {'c'}, dimensions={0}, use_global_device_ids=true | all-gather | bytes 786432 | tf_op jit(solution)/shard_map/all_gather | solution.py:125
  50.0 0.3 multiply_reduce_fusion.2
  50.4 1.1 convolution_convert_fusion
  51.5 6.9 %all-to-all-start.1 = ((bf16[16,8,2048]{2,1,0:T(8,128)(2,1)}), bf16[16,8,2048]{2,1,0:T(8,128)(2,1)S(1)}, u32[]{:S(2)}, u32[]{:S(2)}) async-start(bf16[16,8,2048]{2,1,0:T(8,128)(2,1)} %bitcast.31), calls=%async_computation.1 | async-start | bytes 1048576 | tf_op jit(solution)/shard_map/all_to_all | solution.py:314
  58.4 0.8 constant_dynamic-slice_fusion.2
  59.3 9.8 %all-to-all-done.1 = bf16[16,8,2048]{2,1,0:T(8,128)(2,1)S(1)} async-done(((bf16[16,8,2048]{2,1,0:T(8,128)(2,1)}), bf16[16,8,2048]{2,1,0:T(8,128)(2,1)S(1)}, u32[]{:S(2)}, u32[]{:S(2)}) %all-to-all-start.1) | async-done | bytes 524320 | tf_op jit(solution)/shard_map/all_to_all | solution.py:314
  69.9 0.7 reshape.122
  70.6 5.7 %all-to-all-start.2 = ((bf16[16,16,256]{2,1,0:T(8,128)(2,1)}), bf16[16,16,256]{2,1,0:T(8,128)(2,1)S(1)}, u32[]{:S(2)}, u32[]{:S(2)}) async-start(bf16[16,16,256]{2,1,0:T(8,128)(2,1)} %reshape.122), calls=%async_computation.2 | async-start | bytes 262144 | tf_op jit(solution)/shard_map/all_to_all | solution.py:336
  76.3 2.2 %collective-permute-start = (bf16[4608,128]{1,0:T(8,128)(2,1)}, bf16[4608,128]{1,0:T(8,128)(2,1)}, u32[]{:S(2)}, u32[]{:S(2)}) collective-permute-start(bf16[4608,128]{1,0:T(8,128)(2,1)} %get-tuple-element.29), channel_id=1, source_target_pairs={{0,1},{1,2},{2,3},{3,0},{4,5},{5,6},{6,7},{7,4},{8,9},{9,10},{10,1... | collective-permute-start | bytes 3538952 | tf_op jit(solution)/shard_map/ppermute | solution.py:99
  78.5 4.3 %collective-permute-start.1 = (bf16[4608,128]{1,0:T(8,128)(2,1)}, bf16[4608,128]{1,0:T(8,128)(2,1)}, u32[]{:S(2)}, u32[]{:S(2)}) collective-permute-start(bf16[4608,128]{1,0:T(8,128)(2,1)} %get-tuple-element.30), channel_id=1, source_target_pairs={{0,3},{1,0},{2,1},{3,2},{4,7},{5,4},{6,5},{7,6},{8,11},{9,8},{10,9... | collective-permute-start | bytes 3538952 | tf_op jit(solution)/shard_map/ppermute | solution.py:99
  82.8 1.9 collective-permute-start.2
  84.8 4.6 %collective-permute-start.3 = (bf16[4608,128]{1,0:T(8,128)(2,1)}, bf16[4608,128]{1,0:T(8,128)(2,1)}, u32[]{:S(2)}, u32[]{:S(2)}) collective-permute-start(bf16[4608,128]{1,0:T(8,128)(2,1)} %get-tuple-element.32), channel_id=1, source_target_pairs={{0,12},{1,13},{2,14},{3,15},{4,0},{5,1},{6,2},{7,3},{8,4},{9,5},{1... | collective-permute-start | bytes 3538952 | tf_op jit(solution)/shard_map/ppermute | solution.py:99
  89.6 1.1 broadcast_in_dim.7
  90.7 6.8 %all-to-all-start.3 = ((bf16[32,8,2048]{2,1,0:T(8,128)(2,1)}), bf16[32,8,2048]{2,1,0:T(8,128)(2,1)S(1)}, u32[]{:S(2)}, u32[]{:S(2)}) async-start(bf16[32,8,2048]{2,1,0:T(8,128)(2,1)} %bitcast.36), calls=%async_computation.3 | async-start | bytes 2097152 | tf_op jit(solution)/shard_map/all_to_all | solution.py:333
  97.5 8.1 %collective-permute-done.refs_3_ = bf16[4608,128]{1,0:T(8,128)(2,1)} collective-permute-done((bf16[4608,128]{1,0:T(8,128)(2,1)}, bf16[4608,128]{1,0:T(8,128)(2,1)}, u32[]{:S(2)}, u32[]{:S(2)}) %collective-permute-start) | collective-permute-done | bytes 1179680 | tf_op jit(solution)/shard_map/ppermute | solution.py:99
  105.6 0.6 collective-permute-done.1.refs_4_
  106.2 13.5 %collective-permute-done.2.refs_5_ = bf16[4608,128]{1,0:T(8,128)(2,1)} collective-permute-done((bf16[4608,128]{1,0:T(8,128)(2,1)}, bf16[4608,128]{1,0:T(8,128)(2,1)}, u32[]{:S(2)}, u32[]{:S(2)}) %collective-permute-start.2) | collective-permute-done | bytes 1179680 | tf_op jit(solution)/shard_map/ppermute | solution.py:99
  119.6 1.1 collective-permute-done.3.refs_6_
  120.7 4.6 %all-to-all-done.3 = bf16[32,8,2048]{2,1,0:T(8,128)(2,1)S(1)} async-done(((bf16[32,8,2048]{2,1,0:T(8,128)(2,1)}), bf16[32,8,2048]{2,1,0:T(8,128)(2,1)S(1)}, u32[]{:S(2)}, u32[]{:S(2)}) %all-to-all-start.3) | async-done | bytes 1048608 | tf_op jit(solution)/shard_map/all_to_all | solution.py:333
  125.4 8.1 %run_experts.1 = bf16[256,2048]{1,0:T(8,128)(2,1)S(1)} custom-call(bf16[256,2048]{1,0:T(8,128)(2,1)S(1)} %bitcast.158, bf16[2048,384]{1,0:T(8,128)(2,1)} %bitcast.161, bf16[2048,384]{1,0:T(8,128)(2,1)} %bitcast.163, bf16[384,2048]{1,0:T(8,128)(2,1)} %bitcast.165, bf16[4608,128]{1,0:T(8,128)(2,1)} %collective-permute-done.refs_3_, ...), custom_call_target="tpu_custom_call" | custom-call | tf_op jit(solution)/shard_map/run_experts/pallas_call | solution.py:343
  133.5 22.7 %all_to_all.35 = bf16[32,8,2048]{2,1,0:T(8,128)(2,1)S(1)} all-to-all(bf16[32,8,2048]{2,1,0:T(8,128)(2,1)S(1)} %bitcast.159), channel_id=1, replica_groups=mesh['zh'=8,'zl'=2,'c'=2,'tp'=16] {'c','tp'}, dimensions={0} | all-to-all | bytes 2097152 | tf_op jit(solution)/shard_map/all_to_all | solution.py:333
  156.4 0.8 copy.46
  157.2 11.5 %all-to-all-start.5 = ((bf16[16,2,2048]{2,1,0:T(2,128)(2,1)}), bf16[16,2,2048]{2,1,0:T(2,128)(2,1)S(1)}, u32[]{:S(2)}, u32[]{:S(2)}) async-start(bf16[16,2,2048]{2,1,0:T(2,128)(2,1)} %copy.46), calls=%async_computation.5 | async-start | bytes 262144 | tf_op jit(solution)/shard_map/all_to_all | solution.py:329
  168.7 11.9 %all-to-all-done.5 = bf16[16,2,2048]{2,1,0:T(2,128)(2,1)S(1)} async-done(((bf16[16,2,2048]{2,1,0:T(2,128)(2,1)}), bf16[16,2,2048]{2,1,0:T(2,128)(2,1)S(1)}, u32[]{:S(2)}, u32[]{:S(2)}) %all-to-all-start.5) | async-done | bytes 131104 | tf_op jit(solution)/shard_map/all_to_all | solution.py:329
  181.4 13.0 %all_to_all.36 = bf16[16,8,2048]{2,1,0:T(8,128)(2,1)S(1)} all-to-all(bf16[16,8,2048]{2,1,0:T(8,128)(2,1)S(1)} %broadcast_in_dim.8), channel_id=1, replica_groups=mesh['zh'=8,'zl'=2,'c'=2,'tp'=16] {'tp'}, dimensions={0} | all-to-all | bytes 1048576 | tf_op jit(solution)/shard_map/all_to_all | solution.py:142
  194.4 0.8 copy.53
  (61 shorter events, 4.8 us)
Async XLA Ops:
  0.0 50.4 %copy-start = (bf16[128,2048]{1,0:T(8,128)(2,1)S(1)}, bf16[128,2048]{1,0:T(8,128)(2,1)}, u32[]{:S(2)}) copy-start(bf16[128,2048]{1,0:T(8,128)(2,1)} %param.26) | copy-start | bytes 1572868
  17.8 23.7 %all-to-all-start = ((bf16[16,64,128]{2,1,0:T(8,128)(2,1)}), bf16[16,64,128]{2,1,0:T(8,128)(2,1)S(1)}, u32[]{:S(2)}, u32[]{:S(2)}) async-start(bf16[16,64,128]{2,1,0:T(8,128)(2,1)} %broadcast_in_dim.6), calls=%async_computation | async-start | bytes 524288 | tf_op jit(solution)/shard_map/all_to_all | solution.py:124
  48.5 1.9 copy-start.1
  48.5 1.9 copy-start.6
  50.3 8.9 %copy-start.4 = (s32[128,2]{0,1:T(2,128)S(1)}, s32[128,2]{0,1:T(2,128)}, u32[]{:S(2)}) copy-start(s32[128,2]{0,1:T(2,128)} %param.29) | copy-start | bytes 3076
  51.5 18.0 %copy-start.2 = (f32[2048]{0:T(1024)S(1)}, f32[2048]{0:T(1024)}, u32[]{:S(2)}) copy-start(f32[2048]{0:T(1024)} %param.27) | copy-start | bytes 24580
  51.5 17.6 %all-to-all-start.1 = ((bf16[16,8,2048]{2,1,0:T(8,128)(2,1)}), bf16[16,8,2048]{2,1,0:T(8,128)(2,1)S(1)}, u32[]{:S(2)}, u32[]{:S(2)}) async-start(bf16[16,8,2048]{2,1,0:T(8,128)(2,1)} %bitcast.31), calls=%async_computation.1 | async-start | bytes 1048576 | tf_op jit(solution)/shard_map/all_to_all | solution.py:314
  70.6 18.8 %all-to-all-start.2 = ((bf16[16,16,256]{2,1,0:T(8,128)(2,1)}), bf16[16,16,256]{2,1,0:T(8,128)(2,1)S(1)}, u32[]{:S(2)}, u32[]{:S(2)}) async-start(bf16[16,16,256]{2,1,0:T(8,128)(2,1)} %reshape.122), calls=%async_computation.2 | async-start | bytes 262144 | tf_op jit(solution)/shard_map/all_to_all | solution.py:336
  76.3 29.3 %collective-permute-start = (bf16[4608,128]{1,0:T(8,128)(2,1)}, bf16[4608,128]{1,0:T(8,128)(2,1)}, u32[]{:S(2)}, u32[]{:S(2)}) collective-permute-start(bf16[4608,128]{1,0:T(8,128)(2,1)} %get-tuple-element.29), channel_id=1, source_target_pairs={{0,1},{1,2},{2,3},{3,0},{4,5},{5,6},{6,7},{7,4},{8,9},{9,10},{10,1... | collective-permute-start | bytes 3538952 | tf_op jit(solution)/shard_map/ppermute | solution.py:99
  78.5 27.6 %collective-permute-start.1 = (bf16[4608,128]{1,0:T(8,128)(2,1)}, bf16[4608,128]{1,0:T(8,128)(2,1)}, u32[]{:S(2)}, u32[]{:S(2)}) collective-permute-start(bf16[4608,128]{1,0:T(8,128)(2,1)} %get-tuple-element.30), channel_id=1, source_target_pairs={{0,3},{1,0},{2,1},{3,2},{4,7},{5,4},{6,5},{7,6},{8,11},{9,8},{10,9... | collective-permute-start | bytes 3538952 | tf_op jit(solution)/shard_map/ppermute | solution.py:99
  82.8 36.8 %collective-permute-start.2 = (bf16[4608,128]{1,0:T(8,128)(2,1)}, bf16[4608,128]{1,0:T(8,128)(2,1)}, u32[]{:S(2)}, u32[]{:S(2)}) collective-permute-start(bf16[4608,128]{1,0:T(8,128)(2,1)} %get-tuple-element.31), channel_id=1, source_target_pairs={{0,4},{1,5},{2,6},{3,7},{4,8},{5,9},{6,10},{7,11},{8,12},{9,13},{1... | collective-permute-start | bytes 3538952 | tf_op jit(solution)/shard_map/ppermute | solution.py:99
  84.8 36.0 %collective-permute-start.3 = (bf16[4608,128]{1,0:T(8,128)(2,1)}, bf16[4608,128]{1,0:T(8,128)(2,1)}, u32[]{:S(2)}, u32[]{:S(2)}) collective-permute-start(bf16[4608,128]{1,0:T(8,128)(2,1)} %get-tuple-element.32), channel_id=1, source_target_pairs={{0,12},{1,13},{2,14},{3,15},{4,0},{5,1},{6,2},{7,3},{8,4},{9,5},{1... | collective-permute-start | bytes 3538952 | tf_op jit(solution)/shard_map/ppermute | solution.py:99
  90.7 34.7 %all-to-all-start.3 = ((bf16[32,8,2048]{2,1,0:T(8,128)(2,1)}), bf16[32,8,2048]{2,1,0:T(8,128)(2,1)S(1)}, u32[]{:S(2)}, u32[]{:S(2)}) async-start(bf16[32,8,2048]{2,1,0:T(8,128)(2,1)} %bitcast.36), calls=%async_computation.3 | async-start | bytes 2097152 | tf_op jit(solution)/shard_map/all_to_all | solution.py:333
  156.1 12.5 %copy-start.5 = (f32[128,2]{0,1:T(2,128)S(1)}, f32[128,2]{0,1:T(2,128)}, u32[]{:S(2)}) copy-start(f32[128,2]{0,1:T(2,128)} %param.30) | copy-start | bytes 3076
  156.3 24.9 %copy-start.3 = (f32[2048]{0:T(1024)S(1)}, f32[2048]{0:T(1024)}, u32[]{:S(2)}) copy-start(f32[2048]{0:T(1024)} %param.28) | copy-start | bytes 24580
  157.2 23.5 %all-to-all-start.5 = ((bf16[16,2,2048]{2,1,0:T(2,128)(2,1)}), bf16[16,2,2048]{2,1,0:T(2,128)(2,1)S(1)}, u32[]{:S(2)}, u32[]{:S(2)}) async-start(bf16[16,2,2048]{2,1,0:T(2,128)(2,1)} %copy.46), calls=%async_computation.5 | async-start | bytes 262144 | tf_op jit(solution)/shard_map/all_to_all | solution.py:329
